TPU v7x, 512 devices: a 4x2x32 block of a 4x8x32 slice. The times are simulated.
512 devices in a mesh: grp: 2 (over y), sp: 64 (over z, core), tp: 4 (over x).
Axes of the slice: x: 4, y: 2, z: 32, core: 2. Of those that a mesh axis runs over, the one named last changes fastest.
The devices are a block of a 4x8x32 slice.
Arguments:
- tokens: bfloat16 [131072, 2048], P(('grp', 'sp', 'tp')), parts along dimension 0, may hold values from -6 to 6
- step: float32 [131072], P(('grp', 'sp')), parts along dimension 0, may hold values from 0.2 to 3.75
- in_gain: float32 [2048], replicated, may hold values from 0.1 to 1.9
- in_proj: bfloat16 [2048, 512], P(None, 'tp'), may hold values from -0.125 to 0.125
- decay_rate: float32 [32, 64], P('tp'), may hold values from 1.5258789e-06 to 0.04
- frequency: float32 [32, 64], P('tp'), may hold values from 0.2 to 3
- input_map: float32 [2, 32, 64, 16], P(None, 'tp'), may hold values from -1 to 1
- readout: float32 [2, 32, 16, 64], P(None, 'tp'), may hold values from -0.75 to 0.75
- out_gain: float32 [512], replicated, may hold values from 0.1 to 1.9
- out_proj: bfloat16 [512, 2048], replicated, may hold values from -0.25 to 0.25
Outputs:
- mixed: bfloat16 [131072, 2048], P(('grp', 'sp', 'tp')), parts along dimension 0
There are 2 independent parts, one for each index of `grp`. A program takes and returns all parts, laid end to end along the dimension named above; an argument that names none is the same for every part. Nothing has to cross between parts.
All inputs are finite; a program needn't handle non-finite values.
Results may differ from a plain program's by a relative error of at most 0.01.
Values may be sent and summed in bfloat16 or wider, within the bound.
No kernel may reach another device: no remote copies, remote signals or barrier semaphores. Data moves between devices by JAX's collectives and lax.ppermute only.
A program may use at most 64 MiB of HBM per device.

v0:
```python
from functools import partial

import jax
import jax.numpy as jnp
from jax import lax
from jax.sharding import PartitionSpec as P

SPAN = 64


HIGHEST = lax.Precision.HIGHEST


def gathered_once(array, axis):
    leaves = jax.tree.leaves(array)
    sequence = sorted(range(len(leaves)), key=lambda k: -leaves[k].size)
    width = (1, *leaves[sequence[0]].shape)[-1]
    lines = [
        jnp.pad(leaves[k].reshape(-1), (0, -leaves[k].size % width)).reshape(-1, width)
        for k in sequence
    ]
    both, at, found = (lax.all_gather(jnp.concatenate(lines), axis), 0, {})
    for k, line in zip(sequence, lines):
        section = both[:, at : at + len(line)].reshape(len(both), -1)
        found[k] = section[:, : leaves[k].size].reshape(-1, *leaves[k].shape)
        at += len(line)
    numbers = iter(range(len(leaves)))
    return jax.tree.map(lambda _: found[next(numbers)], array)


def entering(value, axis, join, neutral):
    count, mine = (lax.axis_size(axis), lax.axis_index(axis))
    pieces = gathered_once(value, axis)
    so_far = jax.tree.map(
        lambda part, zero: jnp.full_like(part, 0) + jnp.asarray(zero, part.dtype), value, neutral
    )

    def lap(position, so_far):
        longer = join(so_far, jax.tree.map(lambda part: part[position], pieces))
        return jax.tree.map(lambda new, old: jnp.where(position < mine, new, old), longer, so_far)

    return lax.fori_loop(0, count - 1, lap, so_far)


def compose(earlier, later):
    a_re, a_im, b_re, b_im = earlier
    c_re, c_im, d_re, d_im = later
    return (
        c_re * a_re - c_im * a_im,
        c_re * a_im + c_im * a_re,
        c_re * b_re - c_im * b_im + d_re,
        c_re * b_im + c_im * b_re + d_im,
    )


def rms_rows(values, gain):
    values = values.astype(jnp.float32)
    scaled = values * lax.rsqrt(jnp.mean(values * values, axis=-1, keepdims=True) + 1e-06)
    return (scaled * gain).astype(jnp.bfloat16)


def block_tables(input_map, readout):
    groups = input_map.shape[1]
    unit = jnp.eye(groups, dtype=jnp.float32)
    push_re = jnp.einsum("gph,gk->ghkp", input_map[0], unit, precision=HIGHEST)
    push_im = jnp.einsum("gph,gk->ghkp", input_map[1], unit, precision=HIGHEST)
    read_re = jnp.einsum("ghp,gk->gpkh", readout[0], unit, precision=HIGHEST)
    read_im = jnp.einsum("ghp,gk->gpkh", readout[1], unit, precision=HIGHEST)
    inner = push_re.shape[0] * push_re.shape[1]
    flat = push_re.shape[2] * push_re.shape[3]
    return (
        push_re.reshape(inner, flat),
        push_im.reshape(inner, flat),
        read_re.reshape(flat, inner),
        read_im.reshape(flat, inner),
    )


def response(s_re, s_im, read_re, read_im):
    value = jnp.dot(s_re, read_re, precision=HIGHEST) - jnp.dot(s_im, read_im, precision=HIGHEST)
    return jax.nn.gelu(value, approximate=True).astype(jnp.bfloat16)


def advance(carry, piece, rates, freqs, tables, lower, keep):
    drive_part, time_part = piece
    push_re, push_im, read_re, read_im = tables
    own = time_part[:, None]
    magnitude = jnp.exp(-rates[None] * own)
    a_re = magnitude * jnp.cos(freqs[None] * own)
    a_im = magnitude * jnp.sin(freqs[None] * own)
    lam_re = -rates
    denom = lam_re * lam_re + freqs * freqs
    n_re = a_re - 1.0
    z_re = (n_re * lam_re + a_im * freqs) / denom
    z_im = (a_im * lam_re - n_re * freqs) / denom
    grouped = drive_part.astype(jnp.float32)
    in_re = jnp.dot(grouped, push_re, precision=HIGHEST)
    in_im = jnp.dot(grouped, push_im, precision=HIGHEST)
    i_re = z_re * in_re - z_im * in_im
    i_im = z_re * in_im + z_im * in_re
    elapsed = jnp.dot(lower, time_part, precision=HIGHEST)[:, None]
    grow = jnp.exp(rates[None] * elapsed)
    angle = freqs[None] * elapsed
    cosine = jnp.cos(angle)
    sine = jnp.sin(angle)
    w_re = grow * (cosine * i_re + sine * i_im)
    w_im = grow * (cosine * i_im - sine * i_re)
    acc_re = jnp.dot(lower, w_re, precision=HIGHEST)
    acc_im = jnp.dot(lower, w_im, precision=HIGHEST)
    shrink = jnp.exp(-rates[None] * elapsed)
    c_re = shrink * cosine
    c_im = shrink * sine
    s_re = c_re * acc_re - c_im * acc_im
    s_im = c_re * acc_im + c_im * acc_re
    d_re, d_im, e_re, e_im = carry
    full_re = s_re + c_re * e_re - c_im * e_im
    full_im = s_im + c_re * e_im + c_im * e_re
    cum_re = c_re * d_re - c_im * d_im
    cum_im = c_re * d_im + c_im * d_re
    ends = (cum_re[-1], cum_im[-1], full_re[-1], full_im[-1])
    return (ends, (cum_re, cum_im, full_re, full_im))


def on_device(
    tokens, step, in_gain, in_proj, decay_rate, frequency, input_map, readout, out_gain, out_proj
):
    normed = rms_rows(tokens, in_gain)
    rates, freqs, maps, reads = (decay_rate, frequency, input_map, readout)
    drive = jnp.dot(
        lax.all_gather(normed, "tp", axis=0, tiled=True),
        in_proj,
        preferred_element_type=jnp.float32,
    ).astype(jnp.bfloat16)
    tables = block_tables(maps, reads)
    flat_rates = rates.reshape(-1)
    flat_freqs = freqs.reshape(-1)
    seq_rows = drive.shape[0]
    block_count = seq_rows // SPAN
    drive_blocks = drive.reshape(block_count, SPAN, -1)
    time_blocks = step.reshape(block_count, SPAN)
    rows_index = lax.broadcasted_iota(jnp.int32, (SPAN, SPAN), 0)
    cols_index = lax.broadcasted_iota(jnp.int32, (SPAN, SPAN), 1)
    lower = (cols_index <= rows_index).astype(jnp.float32)
    zeros = jnp.zeros(flat_rates.shape, jnp.float32)
    ones = jnp.ones(flat_rates.shape, jnp.float32)
    start_carry = (ones, zeros, zeros, zeros)
    keep_first = "states"
    ends, stored = lax.scan(
        partial(
            advance, rates=flat_rates, freqs=flat_freqs, tables=tables, lower=lower, keep=keep_first
        ),
        start_carry,
        (drive_blocks, time_blocks),
    )
    incoming = entering(ends, "sp", compose, start_carry)
    cum_re, cum_im, full_re, full_im = stored
    width = flat_rates.shape[0]
    cum_re = cum_re.reshape(seq_rows, width)
    cum_im = cum_im.reshape(seq_rows, width)
    state_re = full_re.reshape(seq_rows, width) + cum_re * incoming[2] - cum_im * incoming[3]
    state_im = full_im.reshape(seq_rows, width) + cum_re * incoming[3] + cum_im * incoming[2]
    answer = response(state_re, state_im, tables[2], tables[3])
    gathered = lax.all_to_all(answer, "tp", split_axis=0, concat_axis=1, tiled=True)
    shaped = rms_rows(gathered, out_gain)
    return jnp.dot(shaped, out_proj, preferred_element_type=jnp.float32).astype(jnp.bfloat16)


def solution(mesh):
    placed = (
        P(("grp", "sp", "tp"), None),
        P(("grp", "sp")),
        P(),
        P(None, "tp"),
        P("tp", None),
        P("tp", None),
        P(None, "tp", None, None),
        P(None, "tp", None, None),
        P(),
        P(),
    )
    return jax.shard_map(
        on_device,
        mesh=mesh,
        in_specs=placed,
        out_specs=P(("grp", "sp", "tp"), None),
        check_vma=False,
    )
```

profile of v0, /device:TPU:33, one launch (start us, length us, event | category | flops | bytes accessed | tf_op | source)
XLA Modules:
  0.0 373.2 jit_solution(620879934638658215)
XLA Ops:
  8.3 2.5 fusion.46
  15.7 85.1 %all-gather.4.cloned.1.call-done = bf16[1024,2048]{1,0:T(8,128)(2,1)} async-done(((bf16[256,2048]{1,0:T(8,128)(2,1)}), bf16[1024,2048]{1,0:T(8,128)(2,1)}) %all-gather.4.cloned.1.call-update) | async-done | bytes 4194320 | tf_op jit(solution)/shard_map/all_gather | solution.py:130
  100.8 4.3 %convolution_convert_fusion.1 = bf16[1024,128]{1,0:T(8,128)(2,1)} fusion(bf16[1024,2048]{1,0:T(8,128)(2,1)} %all-gather.4.cloned.1.call-done, bf16[2048,128]{1,0:T(8,128)(2,1)} %param.17), kind=kOutput, calls=%fused_computation.81 | convolution fusion | flops 537001984 | bytes 4980736 | tf_op jit(solution)/shard_map/dot_general | solution.py:129
  106.2 173.9 %while.48 = (s32[]{:T(128)}, f32[512]{0:T(512)S(1)}, f32[512]{0:T(512)S(1)}, f32[512]{0:T(512)}, f32[512]{0:T(512)}, /*index=5*/f32[16,64,512]{2,1,0:T(8,128)}, ...) while((s32[]{:T(128)}, f32[512]{0:T(512)S(1)}, ...), condition=%wide.wide.region_2.3_spmd.clone.clone.clone, body=%wide.wide.region_1.2_spmd.clone.clone.clone.sunk | while | flops 153889792 | bytes 4405837 | solution.py:148
  112.3 3.0 add_dynamic-update-slice_fusion.3
  123.2 3.0 add_dynamic-update-slice_fusion.3
  134.1 3.0 add_dynamic-update-slice_fusion.3
  144.9 3.0 add_dynamic-update-slice_fusion.3
  155.8 3.0 add_dynamic-update-slice_fusion.3
  166.7 3.0 add_dynamic-update-slice_fusion.3
  177.6 3.0 add_dynamic-update-slice_fusion.3
  188.4 3.0 add_dynamic-update-slice_fusion.3
  199.3 3.0 add_dynamic-update-slice_fusion.3
  210.2 3.0 add_dynamic-update-slice_fusion.3
  221.0 3.0 add_dynamic-update-slice_fusion.3
  231.9 3.0 add_dynamic-update-slice_fusion.3
  242.8 3.0 add_dynamic-update-slice_fusion.3
  253.6 3.0 add_dynamic-update-slice_fusion.3
  264.5 3.0 add_dynamic-update-slice_fusion.3
  275.4 3.0 add_dynamic-update-slice_fusion.3
  280.9 60.4 %all-gather.1 = f32[64,4,512]{2,1,0:T(4,128)S(1)} all-gather(f32[1,4,512]{2,1,0:T(4,128)S(1)} %maximum_bitcast_fusion), channel_id=2, replica_groups=mesh['grp'=2,'sp'=64,'tp'=4] {'sp'}, dimensions={0}, use_global_device_ids=true | all-gather | bytes 532480 | tf_op jit(solution)/shard_map/all_gather | solution.py:22
  341.7 5.1 %while.47 = (s32[]{:T(128)}, f32[512]{0:T(512)S(1)}, f32[512]{0:T(512)S(1)}, s32[]{:T(128)}, f32[64,512]{1,0:T(8,128)S(1)}, /*index=5*/f32[64,512]{1,0:T(8,128)S...) while((s32[]{:T(128)}, f32[512]{0:T(512)S(1)}, f32[512]{0:T(512)S(1)}, ...), condition=%wide.region_4.5_spmd.clone, body=%wide.region_3.4_spmd.clone.sunk | while | flops 6148 | bytes 32897 | solution.py:42
  346.8 4.6 %multiply_add_fusion.5 = (f32[16,64,512]{2,1,0:T(8,128)S(1)}, f32[16,64,512]{2,1,0:T(8,128)S(1)}) fusion(f32[16,64,512]{2,1,0:T(8,128)} %get-tuple-element.435, f32[16,64,512]{2,1,0:T(8,128)} %get-tuple-element.437, f32[16,64,512]{2,1,0:T(8,128)} %get-tuple-element.429, f32[512]{0:T(512)S(1)} %get-tuple-element.436, f32[512]{0:T(512)S(1)} %get-tuple-element.434, ...), kind=kLoop, calls=%fused_computation.78 | loop fusion | flops 4194304 | bytes 12587008 | tf_op jit(solution)/shard_map/add | solution.py:161
  355.2 9.2 %all_to_all.13 = bf16[4,256,128]{1,2,0:T(8,128)(2,1)S(1)} all-to-all(bf16[4,256,128]{1,2,0:T(8,128)(2,1)S(1)} %copy.20), channel_id=1, replica_groups=mesh['grp'=2,'sp'=64,'tp'=4] {'tp'}, dimensions={0} | all-to-all | bytes 524288 | tf_op jit(solution)/shard_map/all_to_all | solution.py:163
  (635 shorter events, 140.3 us)
Async XLA Ops:
  6.5 358.1 %copy-start = (bf16[512,2048]{1,0:T(8,128)(2,1)S(1)}, bf16[512,2048]{1,0:T(8,128)(2,1)}, u32[]{:S(2)}) copy-start(bf16[512,2048]{1,0:T(8,128)(2,1)} %param.23) | copy-start | bytes 6291460
  6.6 6.4 %copy-start.12 = (f32[1024]{0:T(1024)S(1)}, f32[1024]{0:T(1024)}, u32[]{:S(2)}) copy-start(f32[1024]{0:T(1024)} %param.15) | copy-start | bytes 12292
  6.6 7.0 %copy-start.3 = (f32[2,8,16,64]{3,2,1,0:T(8,128)S(1)}, f32[2,8,16,64]{3,2,1,0:T(8,128)}, u32[]{:S(2)}) copy-start(f32[2,8,16,64]{3,2,1,0:T(8,128)} %param.21) | copy-start | bytes 196612
  6.6 94.2 %all-gather.4.cloned.1.call-start = ((), (), s32[]{:S(2)}) async-start(), calls=%async_computation.1 | async-start | bytes 5242880 | tf_op jit(solution)/shard_map/all_gather | solution.py:130
  128.3 5.7 %copy-start.5 = (f32[1,512]{1,0:T(1,128)S(1)}, f32[1,512]{1,0:T(1,128)}, u32[]{:S(2)}) copy-start(f32[1,512]{1,0:T(1,128)} %get-tuple-element.1028) | copy-start | bytes 6148 | tf_op jit(solution)/shard_map/while
  128.3 5.7 %copy-start.10 = (f32[512]{0:T(512)S(1)}, f32[512]{0:T(512)}, u32[]{:S(2)}) copy-start(f32[512]{0:T(512)} %get-tuple-element.1001) | copy-start | bytes 6148 | tf_op jit(solution)/shard_map/while
  128.3 5.7 %copy-start.11 = (f32[512]{0:T(512)S(1)}, f32[512]{0:T(512)}, u32[]{:S(2)}) copy-start(f32[512]{0:T(512)} %get-tuple-element.1002) | copy-start | bytes 6148 | tf_op jit(solution)/shard_map/while
  128.3 5.7 %copy-start.14 = (f32[512]{0:T(512)S(1)}, f32[512]{0:T(512)}, u32[]{:S(2)}) copy-start(f32[512]{0:T(512)} %get-tuple-element.1038) | copy-start | bytes 6148 | tf_op jit(solution)/shard_map/while
  128.3 5.7 %copy-start.15 = (f32[1,512]{1,0:T(1,128)S(1)}, f32[1,512]{1,0:T(1,128)}, u32[]{:S(2)}) copy-start(f32[1,512]{1,0:T(1,128)} %get-tuple-element.1032) | copy-start | bytes 6148 | tf_op jit(solution)/shard_map/while
  139.1 5.7 %copy-start.5 = (f32[1,512]{1,0:T(1,128)S(1)}, f32[1,512]{1,0:T(1,128)}, u32[]{:S(2)}) copy-start(f32[1,512]{1,0:T(1,128)} %get-tuple-element.1028) | copy-start | bytes 6148 | tf_op jit(solution)/shard_map/while
  139.2 5.7 %copy-start.10 = (f32[512]{0:T(512)S(1)}, f32[512]{0:T(512)}, u32[]{:S(2)}) copy-start(f32[512]{0:T(512)} %get-tuple-element.1001) | copy-start | bytes 6148 | tf_op jit(solution)/shard_map/while
  139.2 5.7 %copy-start.11 = (f32[512]{0:T(512)S(1)}, f32[512]{0:T(512)}, u32[]{:S(2)}) copy-start(f32[512]{0:T(512)} %get-tuple-element.1002) | copy-start | bytes 6148 | tf_op jit(solution)/shard_map/while
  139.2 5.7 %copy-start.14 = (f32[512]{0:T(512)S(1)}, f32[512]{0:T(512)}, u32[]{:S(2)}) copy-start(f32[512]{0:T(512)} %get-tuple-element.1038) | copy-start | bytes 6148 | tf_op jit(solution)/shard_map/while
  139.2 5.7 %copy-start.15 = (f32[1,512]{1,0:T(1,128)S(1)}, f32[1,512]{1,0:T(1,128)}, u32[]{:S(2)}) copy-start(f32[1,512]{1,0:T(1,128)} %get-tuple-element.1032) | copy-start | bytes 6148 | tf_op jit(solution)/shard_map/while
  150.0 5.7 %copy-start.5 = (f32[1,512]{1,0:T(1,128)S(1)}, f32[1,512]{1,0:T(1,128)}, u32[]{:S(2)}) copy-start(f32[1,512]{1,0:T(1,128)} %get-tuple-element.1028) | copy-start | bytes 6148 | tf_op jit(solution)/shard_map/while
  150.0 5.7 %copy-start.10 = (f32[512]{0:T(512)S(1)}, f32[512]{0:T(512)}, u32[]{:S(2)}) copy-start(f32[512]{0:T(512)} %get-tuple-element.1001) | copy-start | bytes 6148 | tf_op jit(solution)/shard_map/while
  150.0 5.7 %copy-start.11 = (f32[512]{0:T(512)S(1)}, f32[512]{0:T(512)}, u32[]{:S(2)}) copy-start(f32[512]{0:T(512)} %get-tuple-element.1002) | copy-start | bytes 6148 | tf_op jit(solution)/shard_map/while
  150.0 5.7 %copy-start.14 = (f32[512]{0:T(512)S(1)}, f32[512]{0:T(512)}, u32[]{:S(2)}) copy-start(f32[512]{0:T(512)} %get-tuple-element.1038) | copy-start | bytes 6148 | tf_op jit(solution)/shard_map/while
  150.1 5.7 %copy-start.15 = (f32[1,512]{1,0:T(1,128)S(1)}, f32[1,512]{1,0:T(1,128)}, u32[]{:S(2)}) copy-start(f32[1,512]{1,0:T(1,128)} %get-tuple-element.1032) | copy-start | bytes 6148 | tf_op jit(solution)/shard_map/while
  160.9 5.7 %copy-start.5 = (f32[1,512]{1,0:T(1,128)S(1)}, f32[1,512]{1,0:T(1,128)}, u32[]{:S(2)}) copy-start(f32[1,512]{1,0:T(1,128)} %get-tuple-element.1028) | copy-start | bytes 6148 | tf_op jit(solution)/shard_map/while
  160.9 5.7 %copy-start.10 = (f32[512]{0:T(512)S(1)}, f32[512]{0:T(512)}, u32[]{:S(2)}) copy-start(f32[512]{0:T(512)} %get-tuple-element.1001) | copy-start | bytes 6148 | tf_op jit(solution)/shard_map/while
  280.2 61.5 %copy-start.6 = (f32[512]{0:T(512)S(1)}, f32[512]{0:T(512)}, u32[]{:S(2)}) copy-start(f32[512]{0:T(512)} %custom-call) | copy-start | bytes 6148
  280.2 61.5 %copy-start.7 = (f32[512]{0:T(512)S(1)}, f32[512]{0:T(512)}, u32[]{:S(2)}) copy-start(f32[512]{0:T(512)} %custom-call.1) | copy-start | bytes 6148
  353.2 11.3 %copy-start.13 = (f32[512]{0:T(512)S(1)}, f32[512]{0:T(512)}, u32[]{:S(2)}) copy-start(f32[512]{0:T(512)} %param.22) | copy-start | bytes 6148
  (68 other events, 381.6 us)
Sparse Core Ops, SparseCore 0:
  11.0 89.7 all-gather.3
where the time goes:
time: 378 us; the launch traced here: 373 us
  matrix products  134 us (35%)
  waiting for transfers between devices  85.1 us (23%)
  blocking collectives  69.5 us (18%)
  local copies, waits for them, and re-layouts  43.1 us (11%)
  other arithmetic  22.5 us (6%)
  between operations  13.7 us (4%)
  loops' own time  5.22 us (1%)
    all_gather x1, waiting for transfers between devices, on_device(): lax.all_gather(normed, 'tp', axis=0, tiled=True)  85.1 us
    all_gather x1, blocking collectives, gathered_once(): both, at, found = (lax.all_gather(jnp.concatenate(lines), axis), 0, {})  60.4 us
    dot_general x16, matrix products, advance(): acc_im = jnp.dot(lower, w_im, precision=HIGHEST)  48.1 us
    dot_general x16, matrix products, advance(): acc_re = jnp.dot(lower, w_re, precision=HIGHEST)  32.4 us
    slice x32, local copies, waits for them, and re-layouts, advance(): ends = (cum_re[-1], cum_im[-1], full_re[-1], full_im[-1])  18.8 us
    dot_general x16, matrix products, advance(): in_im = jnp.dot(grouped, push_im, precision=HIGHEST)  15.3 us
    dot_general x16, matrix products, advance(): in_re = jnp.dot(grouped, push_re, precision=HIGHEST)  15.3 us
    dot_general x16, matrix products, advance(): elapsed = jnp.dot(lower, time_part, precision=HIGHEST)[:, None]  13.3 us
  transfers between devices with their start and end apart: 1, of which 1 were waited for; matrix products, arithmetic and copies ran while one was open for 1% of the time, Pallas kernels for 0%

commit v1 on v0

v1 whole, which is shorter than its diff:
```python
from functools import partial

import jax
import jax.numpy as jnp
from jax import lax
from jax.experimental import pallas as pl
from jax.experimental.pallas import tpu as pltpu
from jax.sharding import Mesh, PartitionSpec as P

CHUNK = 128
LANES = 128
F32 = jnp.float32
BF16 = jnp.bfloat16
TWO_PI_HIGH = 6.28125
TWO_PI_LOW = 0.0019353071795864769
INV_TWO_PI = 0.15915494309189535
SIN = (6.2831854820251465, -41.3416862487793, 81.60456085205078, -76.69428253173828,
       41.96574020385742, -14.708574295043945, 3.0096182823181152)
COS = (1.0, -19.739208221435547, 64.9393539428711, -85.45588684082031, 60.23442077636719,
       -26.364990234375, 7.6985273361206055, -1.3503994941711426)
HIGHEST = lax.Precision.HIGHEST


def polynomial(x, factors):
    total = factors[-1] * x + factors[-2]
    for factor in factors[-3::-1]:
        total = total * x + factor
    return total


def split_turns(freq):
    plain = freq * INV_TWO_PI
    high = jnp.round(plain * 8192.0) * (1.0 / 8192.0)
    rest = (freq - high * TWO_PI_HIGH) - high * TWO_PI_LOW
    return high, rest * INV_TWO_PI, plain


def rotation(coarse, fine, turns, again=False):
    high, rest, plain = turns
    whole = coarse * high
    part = (whole - jnp.round(whole)) + (coarse * rest + fine * plain)
    if again:
        part = part - jnp.round(part)
    square = part * part
    return polynomial(square, COS), part * polynomial(square, SIN)


def decayed(coarse, fine, rate, turns):
    cosine, sine = rotation(coarse, fine, turns, again=True)
    magnitude = jnp.exp(-rate * (coarse + fine))
    return magnitude * cosine, magnitude * sine


def high_low(x):
    high = x.astype(BF16)
    return high, (x - high.astype(F32)).astype(BF16)


def dot_t(a, b):
    return lax.dot_general(a, b, (((1,), (1,)), ((), ())), preferred_element_type=F32)


def tables_kernel(coarse_ref, fine_ref, rate_ref, freq_ref, w_re, w_im, c_re, c_im):
    coarse, fine = coarse_ref[...], fine_ref[...]
    elapsed = coarse + fine
    first = lax.broadcasted_iota(jnp.int32, (CHUNK, LANES), 0) == 0
    for b in range(rate_ref.shape[1] // LANES):
        cols = slice(b * LANES, (b + 1) * LANES)
        rate = rate_ref[:, cols]
        cosine, sine = rotation(coarse, fine, split_turns(freq_ref[:, cols]))
        exponent = rate * elapsed
        shrink = jnp.exp(-exponent)
        c_re[:, cols] = shrink * cosine
        c_im[:, cols] = shrink * sine
        grow = jnp.exp(exponent)
        g_re = grow * cosine
        g_im = -(grow * sine)
        w_re[:, cols] = jnp.where(first, 1.0, pltpu.roll(g_re, 1, 0)) - g_re
        w_im[:, cols] = jnp.where(first, 0.0, pltpu.roll(g_im, 1, 0)) - g_im


def tables(coarse, fine, rate, freq):
    rows, width = coarse.shape[0], rate.shape[1]
    column = pl.BlockSpec((CHUNK, 1), lambda c: (c, 0))
    whole = pl.BlockSpec((1, width), lambda c: (0, 0))
    block = pl.BlockSpec((CHUNK, width), lambda c: (c, 0))
    out = jax.ShapeDtypeStruct((rows, width), F32)
    return pl.pallas_call(
        tables_kernel, grid=(rows // CHUNK,), in_specs=[column, column, whole, whole],
        out_specs=[block] * 4, out_shape=[out] * 4, name="tables",
        cost_estimate=pl.CostEstimate(flops=rows * width * 60, transcendentals=0, bytes_accessed=rows * width * 16),
    )(coarse, fine, rate, freq)


def sums_kernel(at_ref, d0, d1, d2, d3, w_re, w_im, c_re, c_im, push_re, push_im, shift_ref,
                rate4, freq4, acc_re, acc_im, own_ref, sent_ref, push, carry):
    chunk = pl.program_id(0)
    blocks = push_re.shape[0] // LANES

    @pl.when(chunk == 0)
    def _():
        carry[...] = jnp.zeros_like(carry)
        for b in range(blocks):
            rows = slice(b * LANES, (b + 1) * LANES)
            re_high, re_low = high_low(push_re[rows, :])
            im_high, im_low = high_low(push_im[rows, :])
            push[b, :LANES, :LANES] = re_high
            push[b, :LANES, LANES:] = re_low
            push[b, LANES:, :LANES] = im_high
            push[b, LANES:, LANES:] = im_low

    per_slot = d0.shape[0] // CHUNK
    slot = (chunk // per_slot - at_ref[0] + 4) % 4
    start = (chunk % per_slot) * CHUNK
    rows = pl.ds(pl.multiple_of(start, CHUNK), CHUNK)
    drive = jnp.where(slot == 0, d0[rows, :], jnp.where(slot == 1, d1[rows, :],
                      jnp.where(slot == 2, d2[rows, :], d3[rows, :])))
    twice = jnp.concatenate([drive, drive], axis=1)
    row = lax.broadcasted_iota(jnp.int32, (CHUNK, 2 * CHUNK), 0)
    col = lax.broadcasted_iota(jnp.int32, (CHUNK, 2 * CHUNK), 1)
    lower = jnp.where((col % CHUNK) <= row, 1.0, 0.0).astype(BF16)
    for b in range(blocks):
        cols = slice(b * LANES, (b + 1) * LANES)
        pushed = dot_t(twice, push[b])
        p_re, p_im = pushed[:, :LANES], pushed[:, LANES:]
        wr, wi = w_re[:, cols], w_im[:, cols]
        xr_high, xr_low = high_low(wr * p_re - wi * p_im)
        xi_high, xi_low = high_low(wr * p_im + wi * p_re)
        stacked = jnp.concatenate([jnp.concatenate([xr_high, xi_high], axis=1),
                                   jnp.concatenate([xr_low, xi_low], axis=1)], axis=0)
        acc = jnp.dot(lower, stacked, preferred_element_type=F32)
        acc_re[:, cols] = acc[:, :LANES]
        acc_im[:, cols] = acc[:, LANES:]
        cr, ci = c_re[7:8, cols], c_im[7:8, cols]
        tr = acc[CHUNK - 1:, :LANES] + carry[b:b + 1, :]
        ti = acc[CHUNK - 1:, LANES:] + carry[blocks + b:blocks + b + 1, :]
        carry[b:b + 1, :] = cr * tr - ci * ti
        carry[blocks + b:blocks + b + 1, :] = cr * ti + ci * tr

    @pl.when(chunk == pl.num_programs(0) - 1)
    def _():
        own = carry[...]
        own_ref[...] = own
        coarse = shift_ref[0:1, 0:1]
        fine = shift_ref[0:1, 1:2]
        dr, di = decayed(coarse, fine, rate4[...], split_turns(freq4[...]))
        sr, si = own[:blocks], own[blocks:]
        times = shift_ref[...][:, :LANES]
        parts = [times[:, 2:3], times[:, 3:4]]
        lane = lax.broadcasted_iota(jnp.int32, (8, LANES), 1)
        packed = jnp.zeros((8, LANES), F32)
        for k in range(2):
            left = parts[k]
            for j in range(3):
                piece = left.astype(BF16).astype(F32)
                packed = jnp.where(lane == 3 * k + j, piece, packed)
                left = left - piece
        message = jnp.concatenate([dr * sr - di * si, dr * si + di * sr, packed], axis=0).astype(BF16)
        for k in range(sent_ref.shape[0]):
            sent_ref[k] = message


def sums(at, drives, table, push_re, push_im, shift, rate4, freq4, peers):
    w_re, w_im, c_re, c_im = table
    rows, width = w_re.shape
    blocks = width // LANES
    block = pl.BlockSpec((CHUNK, width), lambda c, at: (c, 0))
    last = pl.BlockSpec((8, width), lambda c, at: ((c + 1) * (CHUNK // 8) - 1, 0))

    def whole(array):
        return pl.BlockSpec(array.shape, lambda c, at: (0,) * array.ndim)

    big = jax.ShapeDtypeStruct((rows, width), F32)
    own = jax.ShapeDtypeStruct((2 * blocks, LANES), F32)
    sent = jax.ShapeDtypeStruct((peers, 2 * blocks + 8, LANES), BF16)
    return pl.pallas_call(
        sums_kernel,
        grid_spec=pltpu.PrefetchScalarGridSpec(
            num_scalar_prefetch=1, grid=(rows // CHUNK,),
            in_specs=[whole(d) for d in drives] + [block, block, last, last]
            + [whole(x) for x in (push_re, push_im, shift, rate4, freq4)],
            out_specs=[block, block, pl.BlockSpec(own.shape, lambda c, at: (0, 0)),
                       pl.BlockSpec(sent.shape, lambda c, at: (0, 0, 0))],
            scratch_shapes=[pltpu.VMEM((blocks, 2 * LANES, 2 * push_re.shape[1]), BF16),
                            pltpu.VMEM((2 * blocks, LANES), F32)],
        ),
        out_shape=[big, big, own, sent], name="sums",
        cost_estimate=pl.CostEstimate(flops=rows * width * 1500, transcendentals=0, bytes_accessed=rows * width * 16),
    )(at, *drives, w_re, w_im, c_re, c_im, push_re, push_im, shift, rate4, freq4)


def before_kernel(at_ref, heard_ref, rate4, freq4, own_ref, out_ref):
    rate = rate4[...]
    turns = split_turns(freq4[...])
    blocks = rate.shape[0]
    sr = jnp.zeros(rate.shape, F32)
    si = jnp.zeros(rate.shape, F32)
    for k in range(heard_ref.shape[0] - 1):
        heard = heard_ref[k].astype(F32)
        times = heard[2 * blocks:2 * blocks + 1]
        coarse = (times[:, 0:1] + times[:, 1:2]) + times[:, 2:3]
        fine = (times[:, 3:4] + times[:, 4:5]) + times[:, 5:6]
        dr, di = decayed(coarse, fine, rate, turns)
        nr = dr * sr - di * si + heard[:blocks]
        ni = dr * si + di * sr + heard[blocks:2 * blocks]
        earlier = k < at_ref[1]
        sr = jnp.where(earlier, nr, sr)
        si = jnp.where(earlier, ni, si)
    out_ref[:blocks] = sr
    out_ref[blocks:2 * blocks] = si
    out_ref[2 * blocks:] = own_ref[...]


def before(at, heard, rate4, freq4, own):
    def whole(array):
        return pl.BlockSpec(array.shape, lambda c, at: (0,) * array.ndim)

    out = jax.ShapeDtypeStruct((2 * own.shape[0], LANES), F32)
    return pl.pallas_call(
        before_kernel,
        grid_spec=pltpu.PrefetchScalarGridSpec(
            num_scalar_prefetch=1, grid=(1,), in_specs=[whole(x) for x in (heard, rate4, freq4, own)],
            out_specs=pl.BlockSpec(out.shape, lambda c, at: (0, 0)),
        ),
        out_shape=out, name="before",
    )(at, heard, rate4, freq4, own)


def answer_kernel(at_ref, mine_ref, other_ref, acc_re, acc_im, c_re, c_im, read_re, read_im,
                  shift_ref, rate4, freq4, out_ref, read, carry):
    chunk = pl.program_id(0)
    blocks = rate4.shape[0]

    @pl.when(chunk == 0)
    def _():
        for b in range(blocks):
            cols = slice(b * LANES, (b + 1) * LANES)
            re_high, re_low = high_low(read_re[:, cols])
            im_high, im_low = high_low(-read_im[:, cols])
            read[b, :LANES, :LANES] = re_high
            read[b, :LANES, LANES:] = im_high
            read[b, LANES:, :LANES] = re_low
            read[b, LANES:, LANES:] = im_low
        both = mine_ref[:2 * blocks] + other_ref[:2 * blocks]
        sr, si = both[:blocks], both[blocks:]
        dr, di = decayed(shift_ref[0:1, 4:5], shift_ref[0:1, 5:6], rate4[...], split_turns(freq4[...]))
        second = at_ref[2] == 1
        carry[:blocks] = jnp.where(second, dr * sr - di * si + other_ref[2 * blocks:3 * blocks], sr)
        carry[blocks:] = jnp.where(second, dr * si + di * sr + other_ref[3 * blocks:], si)

    total = jnp.zeros((CHUNK, 2 * LANES), F32)
    for b in range(blocks):
        cols = slice(b * LANES, (b + 1) * LANES)
        tr = acc_re[:, cols] + carry[b:b + 1, :]
        ti = acc_im[:, cols] + carry[blocks + b:blocks + b + 1, :]
        cr, ci = c_re[:, cols], c_im[:, cols]
        sr = cr * tr - ci * ti
        si = cr * ti + ci * tr
        carry[b:b + 1, :] = sr[CHUNK - 1:]
        carry[blocks + b:blocks + b + 1, :] = si[CHUNK - 1:]
        r_high, r_low = high_low(sr)
        i_high, i_low = high_low(si)
        high = jnp.concatenate([r_high, i_high], axis=1)
        low = jnp.concatenate([r_low, i_low], axis=1)
        total = total + dot_t(high, read[b])
        total = total + jnp.concatenate(
            [dot_t(low, read[b, :LANES]), jnp.zeros((CHUNK, LANES), F32)], axis=1)
    value = total[:, :LANES] + total[:, LANES:]
    inner = 0.7978845608 * (value + 0.044715 * (value * value * value))
    out_ref[...] = (0.5 * value * (1.0 + jnp.tanh(inner))).astype(BF16)


def answers(at, mine, other, acc_re, acc_im, c_re, c_im, read_re, read_im, shift, rate4, freq4):
    rows, width = acc_re.shape
    blocks = width // LANES
    block = pl.BlockSpec((CHUNK, width), lambda c, at: (c, 0))

    def whole(array):
        return pl.BlockSpec(array.shape, lambda c, at: (0,) * array.ndim)

    return pl.pallas_call(
        answer_kernel,
        grid_spec=pltpu.PrefetchScalarGridSpec(
            num_scalar_prefetch=1, grid=(rows // CHUNK,),
            in_specs=[whole(mine), whole(other)] + [block] * 4
            + [whole(x) for x in (read_re, read_im, shift, rate4, freq4)],
            out_specs=pl.BlockSpec((CHUNK, LANES), lambda c, at: (c, 0)),
            scratch_shapes=[pltpu.VMEM((blocks, 2 * LANES, 2 * LANES), BF16),
                            pltpu.VMEM((2 * blocks, LANES), F32)],
        ),
        out_shape=jax.ShapeDtypeStruct((rows, LANES), BF16), name="answers",
        cost_estimate=pl.CostEstimate(flops=rows * width * 1000, transcendentals=0, bytes_accessed=rows * width * 16),
    )(at, mine, other, acc_re, acc_im, c_re, c_im, read_re, read_im, shift, rate4, freq4)


def rms_rows(values, gain):
    values = values.astype(F32)
    scaled = values * lax.rsqrt(jnp.mean(values * values, axis=-1, keepdims=True) + 1e-06)
    return (scaled * gain).astype(BF16)


def elapsed_parts(step):
    times = step.reshape(-1, CHUNK)
    grid = jnp.round(times * 8192.0) * (1.0 / 8192.0)
    rows = lax.broadcasted_iota(jnp.int32, (CHUNK, CHUNK), 0)
    cols = lax.broadcasted_iota(jnp.int32, (CHUNK, CHUNK), 1)
    upper = (rows <= cols).astype(F32)
    run = jnp.dot(grid, upper, precision=HIGHEST)
    rest = jnp.dot(times - grid, upper, precision=HIGHEST)
    coarse = jnp.round(run * 8.0) * 0.125
    fine = (run - coarse) + rest
    whole = jnp.sum(coarse[:, -1])
    left = jnp.sum(fine[:, -1])
    return coarse.reshape(-1, 1), fine.reshape(-1, 1), whole, left


def settle(whole, left):
    coarse = jnp.round(whole * 0.5) * 2.0
    return coarse, (whole - coarse) + left


def ring(count, by):
    return [(k, (k + by) % count) for k in range(count)]


def on_device(
    tokens, step, in_gain, in_proj, decay_rate, frequency, input_map, readout, out_gain, out_proj
):
    peers = lax.axis_size("z")
    ways = lax.axis_size("tp")
    core = lax.axis_index("core")
    at = jnp.stack([lax.axis_index("tp"), lax.axis_index("z"), core]).astype(jnp.int32)
    weights = {shift: lax.ppermute(in_proj, "tp", ring(ways, shift)) for shift in (2, 1, 3)}

    coarse, fine, whole, left = elapsed_parts(step)
    times = jnp.zeros((8, LANES), F32).at[0, 0].set(whole).at[0, 1].set(left)
    partner = lax.ppermute(times, "core", [(0, 1), (1, 0)])
    near_whole, near_left = partner[0, 0], partner[0, 1]
    near = settle(near_whole, near_left)
    chip = settle(whole + near_whole, left + near_left)
    first = (core == 0).astype(F32)
    shift = jnp.stack([near[0] * first, near[1] * first, *chip, *near])
    shift = jnp.broadcast_to(jnp.pad(shift, (0, LANES - 6))[None], (8, LANES))

    rate = decay_rate.reshape(1, -1)
    freq = frequency.reshape(1, -1)
    rate4 = decay_rate.reshape(-1, LANES)
    freq4 = frequency.reshape(-1, LANES)
    table = tables(coarse, fine, rate, freq)

    groups, entries = decay_rate.shape
    members = input_map.shape[-1]
    unit = jnp.eye(groups, dtype=F32)
    denom = decay_rate * decay_rate + frequency * frequency
    lam_re = (-decay_rate / denom)[..., None]
    lam_im = (-frequency / denom)[..., None]
    push_re = lam_re * input_map[0] - lam_im * input_map[1]
    push_im = lam_re * input_map[1] + lam_im * input_map[0]

    def spread(small):
        return (small[:, :, None, :] * unit[:, None, :, None]).reshape(groups * entries, groups * members)

    def spread_read(small):
        return (small[:, :, None, :] * unit[:, None, :, None]).reshape(groups * members, groups * entries)

    normed = rms_rows(tokens, in_gain)

    def driven(proj):
        return jnp.dot(normed, proj, preferred_element_type=F32).astype(BF16)

    drives = [driven(in_proj)] + [
        lax.ppermute(driven(weights[k]), "tp", ring(ways, -k)) for k in range(1, ways)
    ]
    acc_re, acc_im, own, sent = sums(
        at, drives, table, spread(push_re), spread(push_im), shift, rate4, freq4, peers
    )
    heard = lax.all_to_all(sent, "z", 0, 0, tiled=True)
    mine = before(at, heard, rate4, freq4, own)
    other = lax.ppermute(mine, "core", [(0, 1), (1, 0)])
    answer = answers(
        at, mine, other, acc_re, acc_im, table[2], table[3],
        spread_read(readout[0]), spread_read(readout[1]), shift, rate4, freq4,
    )
    gathered = lax.all_to_all(answer, "tp", split_axis=0, concat_axis=1, tiled=True)
    shaped = rms_rows(gathered, out_gain)
    return jnp.dot(shaped, out_proj, preferred_element_type=F32).astype(BF16)


def solution(mesh):
    shape = mesh.shape
    devices = mesh.devices.reshape(shape["grp"], shape["sp"] // 2, 2, shape["tp"])
    fine_mesh = Mesh(devices, ("grp", "z", "core", "tp"))
    rows = ("grp", "z", "core", "tp")
    placed = (
        P(rows, None),
        P(("grp", "z", "core")),
        P(),
        P(None, "tp"),
        P("tp", None),
        P("tp", None),
        P(None, "tp", None, None),
        P(None, "tp", None, None),
        P(),
        P(),
    )
    return jax.shard_map(
        on_device,
        mesh=fine_mesh,
        in_specs=placed,
        out_specs=P(rows, None),
        check_vma=False,
    )
```

time: 378 us -> 183 us (0.48)
  matrix products: 134 us -> 10.5 us
  starting transfers between devices: 0.06 us -> 73.7 us
  blocking collectives: 69.5 us -> 10.3 us
  waiting for transfers between devices: 85.1 us -> 28.7 us
  Pallas kernels: 0 us -> 32.5 us
  local copies, waits for them, and re-layouts: 43.1 us -> 15.4 us
  other arithmetic: 22.5 us -> 5.66 us
  between operations: 13.7 us -> 4.44 us
  loops' own time: 5.22 us -> 0 us
    dot_general x84 -> x7, matrix products: 134 us -> 10.5 us  [the longest x4 7.12 us: driven(): return jnp.dot(normed, proj, preferred_element_type=F32).astype(BF16)]
    all_gather x1 -> x0, waiting for transfers between devices: 85.1 us -> none  [on_device(): lax.all_gather(normed, 'tp', axis=0, tiled=True)]
    ppermute x0 -> x8, starting transfers between devices: none -> 66.7 us  [the longest x1 40.7 us: on_device(): partner = lax.ppermute(times, 'core', [(0, 1), (1, 0)])]
    all_gather x1 -> x0, blocking collectives: 60.4 us -> none  [gathered_once(): both, at, found = (lax.all_gather(jnp.concatenate(lines), axis), 0, {})]
    pallas_call x0 -> x4, Pallas kernels: none -> 32.5 us  [the longest x1 12.6 us: sums(): pl.pallas_call(sums_kernel, grid_spec=pltpu.PrefetchScalarGridSpec(num_sc...]
    all_to_all x0 -> x1, waiting for transfers between devices: none -> 28.7 us  [on_device(): heard = lax.all_to_all(sent, 'z', 0, 0, tiled=True)]
    slice x33 -> x1, local copies, waits for them, and re-layouts: 19.1 us -> 0.58 us  [on_device(): near_whole, near_left = (partner[0, 0], partner[0, 1])]
    squeeze x20 -> x0, local copies, waits for them, and re-layouts: 11.6 us -> none  [the longest x16 11.6 us: on_device(): lax.scan(partial(advance, rates=flat_rates, freqs=flat_freqs, tables=tabl...]
  transfers between devices with their start and end apart: 1 -> 9, of which waited for: 1 -> 1; matrix products, arithmetic and copies ran while one was open for 1% -> 15% of each run, Pallas kernels for 0% -> 5%
where the time goes in v1:
time: 183 us; the launch traced here: 181 us
  starting transfers between devices  73.7 us (40%)
  Pallas kernels  32.5 us (18%)
  waiting for transfers between devices  28.7 us (16%)
  local copies, waits for them, and re-layouts  15.4 us (8%)
  matrix products  10.5 us (6%)
  blocking collectives  10.3 us (6%)
  other arithmetic  5.66 us (3%)
  between operations  4.44 us (2%)
    ppermute x1, starting transfers between devices, on_device(): partner = lax.ppermute(times, 'core', [(0, 1), (1, 0)])  40.7 us
    all_to_all x1, waiting for transfers between devices, on_device(): heard = lax.all_to_all(sent, 'z', 0, 0, tiled=True)  28.7 us
    pallas_call x1, Pallas kernels, sums(): pl.pallas_call(sums_kernel, grid_spec=pltpu.PrefetchScalarGridSpec(num_sc...  12.6 us
    ppermute x3, starting transfers between devices, on_device(): lax.ppermute(in_proj, 'tp', ring(ways, shift))  11.9 us
    all_to_all x1, blocking collectives, on_device(): lax.all_to_all(answer, 'tp', split_axis=0, concat_axis=1, tiled=True)  10.3 us
    ppermute x3, starting transfers between devices, on_device(): lax.ppermute(driven(weights[k]), 'tp', ring(ways, -k))  9.31 us
    pallas_call x1, Pallas kernels, answers(): pl.pallas_call(answer_kernel, grid_spec=pltpu.PrefetchScalarGridSpec(num_...  9.05 us
    pallas_call x1, Pallas kernels, tables(): pl.pallas_call(tables_kernel, grid=(rows // CHUNK,), in_specs=[column, co...  8.21 us
  transfers between devices with their start and end apart: 9, of which 1 were waited for; matrix products, arithmetic and copies ran while one was open for 15% of the time, Pallas kernels for 5%

profile of v1, /device:TPU:33, one launch (start us, length us, event | category | flops | bytes accessed | tf_op | source)
XLA Modules:
  0.0 181.2 jit_solution(7789018188698063615)
XLA Ops:
  0.0 4.2 %collective-permute-start = (bf16[2048,128]{1,0:T(8,128)(2,1)}, bf16[2048,128]{1,0:T(8,128)(2,1)}, u32[]{:S(2)}, u32[]{:S(2)}) collective-permute-start(bf16[2048,128]{1,0:T(8,128)(2,1)} %param.17), channel_id=1, source_target_pairs={{0,1},{1,2},{2,3},{3,0},{4,5},{5,6},{6,7},{7,4},{8,9},{9,10},{10,1... | collective-permute-start | bytes 1572872 | tf_op jit(solution)/shard_map/ppermute | solution.py:333
  4.3 4.7 %collective-permute-start.2 = (bf16[2048,128]{1,0:T(8,128)(2,1)}, bf16[2048,128]{1,0:T(8,128)(2,1)}, u32[]{:S(2)}, u32[]{:S(2)}) collective-permute-start(bf16[2048,128]{1,0:T(8,128)(2,1)} %param.17), channel_id=1, source_target_pairs={{0,2},{1,3},{2,0},{3,1},{4,6},{5,7},{6,4},{7,5},{8,10},{9,11},{10,... | collective-permute-start | bytes 1572872 | tf_op jit(solution)/shard_map/ppermute | solution.py:333
  8.9 3.0 %collective-permute-start.4 = (bf16[2048,128]{1,0:T(8,128)(2,1)}, bf16[2048,128]{1,0:T(8,128)(2,1)}, u32[]{:S(2)}, u32[]{:S(2)}) collective-permute-start(bf16[2048,128]{1,0:T(8,128)(2,1)} %param.17), channel_id=1, source_target_pairs={{0,3},{1,0},{2,1},{3,2},{4,7},{5,4},{6,5},{7,6},{8,11},{9,8},{10,9... | collective-permute-start | bytes 1572872 | tf_op jit(solution)/shard_map/ppermute | solution.py:333
  16.2 2.0 %scatter.9 = f32[8,128]{1,0:T(8,128)S(1)} dynamic-update-slice(f32[8,128]{1,0:T(8,128)S(1)} %scatter.6, f32[1,1]{1,0:T(1,128)} %bitcast.9, s32[]{:T(128)} %bitcast.10, s32[]{:T(128)} %bitcast.11) | dynamic-update-slice | bytes 12 | tf_op jit(solution)/shard_map/scatter | solution.py:336
  18.1 40.7 %collective-permute-start.6 = (f32[8,128]{1,0:T(8,128)S(1)}, f32[8,128]{1,0:T(8,128)S(1)}, u32[]{:S(2)}, u32[]{:S(2)}) collective-permute-start(f32[8,128]{1,0:T(8,128)S(1)} %scatter.9), channel_id=1, source_target_pairs={{0,4},{4,0},{1,5},{5,1},{2,6},{6,2},{3,7},{7,3},{8,12},{12,8},{9,1... | collective-permute-start | bytes 12296 | tf_op jit(solution)/shard_map/ppermute | solution.py:337
  60.5 1.5 fusion
  65.4 1.1 copy.14.fine_ref
  69.5 8.2 %tables.1 = (f32[1024,512]{1,0:T(8,128)}, f32[1024,512]{1,0:T(8,128)}, f32[1024,512]{1,0:T(8,128)}, f32[1024,512]{1,0:T(8,128)}) custom-call(f32[1024,1]{1,0:T(8,128)} %copy.13.coarse_ref, f32[1024,1]{1,0:T(8,128)} %copy.14.fine_ref, f32[1,512]{1,0:T(1,128)} %reshape.160.rate_ref, f32[1,512]{1,0:T(1,128)} %reshape.161.freq_ref), custom_call_target="tpu_custom_call" | custom-call | flops 31457280 | bytes 8388608 | tf_op jit(solution)/shard_map/tables/pallas_call | solution.py:88
  77.7 2.5 %convolution_convert_fusion.4.d0 = bf16[256,128]{1,0:T(8,128)(2,1)} fusion(bf16[2048,128]{1,0:T(8,128)(2,1)} %param.17, bf16[256,2048]{1,0:T(8,128)(2,1)} %param.14, f32[2048]{0:T(1024)S(1)} %copy-done.11, f32[256]{0:T(256)S(1)} %add_rsqrt_fusion.1), kind=kOutput, calls=%fused_computation.9 | convolution fusion | flops 136347648 | bytes 1647616 | tf_op jit(solution)/shard_map/dot_general | solution.py:369
  80.2 1.5 convolution_convert_fusion.3
  81.7 2.5 %collective-permute-start.1 = (bf16[256,128]{1,0:T(8,128)(2,1)S(1)}, bf16[256,128]{1,0:T(8,128)(2,1)S(1)}, u32[]{:S(2)}, u32[]{:S(2)}) collective-permute-start(bf16[256,128]{1,0:T(8,128)(2,1)S(1)} %convolution_convert_fusion.3), channel_id=1, source_target_pairs={{0,3},{1,0},{2,1},{3,2},{4,7},{5,4},{6,5},{7,6},{8,11},{9,8},{10,9... | collective-permute-start | bytes 196616 | tf_op jit(solution)/shard_map/ppermute | solution.py:372
  84.3 1.5 convolution_convert_fusion.2
  85.8 4.0 %collective-permute-start.3 = (bf16[256,128]{1,0:T(8,128)(2,1)S(1)}, bf16[256,128]{1,0:T(8,128)(2,1)S(1)}, u32[]{:S(2)}, u32[]{:S(2)}) collective-permute-start(bf16[256,128]{1,0:T(8,128)(2,1)S(1)} %convolution_convert_fusion.2), channel_id=1, source_target_pairs={{0,2},{1,3},{2,0},{3,1},{4,6},{5,7},{6,4},{7,5},{8,10},{9,11},{10,... | collective-permute-start | bytes 196616 | tf_op jit(solution)/shard_map/ppermute | solution.py:372
  89.8 1.5 convolution_convert_fusion.1
  91.4 2.8 %collective-permute-start.5 = (bf16[256,128]{1,0:T(8,128)(2,1)S(1)}, bf16[256,128]{1,0:T(8,128)(2,1)S(1)}, u32[]{:S(2)}, u32[]{:S(2)}) collective-permute-start(bf16[256,128]{1,0:T(8,128)(2,1)S(1)} %convolution_convert_fusion.1), channel_id=1, source_target_pairs={{0,1},{1,2},{2,3},{3,0},{4,5},{5,6},{6,7},{7,4},{8,9},{9,10},{10,1... | collective-permute-start | bytes 196616 | tf_op jit(solution)/shard_map/ppermute | solution.py:372
  99.7 12.6 %sums.1 = (f32[1024,512]{1,0:T(8,128)}, f32[1024,512]{1,0:T(8,128)}, f32[8,128]{1,0:T(8,128)}, bf16[32,16,128]{2,1,0:T(8,128)(2,1)}) custom-call(s32[3]{0:T(128)} %pad_add_fusion.at_ref, bf16[256,128]{1,0:T(8,128)(2,1)} %convolution_convert_fusion.4.d0, bf16[256,128]{1,0:T(8,128)(2,1)} %copy-done.4, bf16[256,128]{1,0:T(8,128)(2,1)} %copy-done.5, ...), custom_call_target="tpu_custom_call" | custom-call | flops 786432000 | bytes 8388608 | tf_op jit(solution)/shard_map/sums/pallas_call | solution.py:176
  112.3 6.9 %all-to-all-start = ((bf16[32,16,128]{2,1,0:T(8,128)(2,1)}), bf16[32,16,128]{2,1,0:T(8,128)(2,1)S(1)}, u32[]{:S(2)}, u32[]{:S(2)}) async-start(bf16[32,16,128]{2,1,0:T(8,128)(2,1)} %get-tuple-element.41), calls=%async_computation | async-start | bytes 262144 | tf_op jit(solution)/shard_map/all_to_all | solution.py:377
  119.4 28.7 %all-to-all-done.heard_ref = bf16[32,16,128]{2,1,0:T(8,128)(2,1)S(1)} async-done(((bf16[32,16,128]{2,1,0:T(8,128)(2,1)}), bf16[32,16,128]{2,1,0:T(8,128)(2,1)S(1)}, u32[]{:S(2)}, u32[]{:S(2)}) %all-to-all-start) | async-done | bytes 131104 | tf_op jit(solution)/shard_map/all_to_all | solution.py:377
  148.7 2.7 %before.1.mine_ref = f32[16,128]{1,0:T(8,128)} custom-call(s32[3]{0:T(128)} %pad_add_fusion.at_ref, bf16[32,16,128]{2,1,0:T(8,128)(2,1)} %copy-done.2, f32[4,128]{1,0:T(4,128)} %reshape.166.rate4, f32[4,128]{1,0:T(4,128)} %reshape.167.freq4, f32[8,128]{1,0:T(8,128)} %get-tuple-element.42.own_ref), custom_call_target="tpu_custom_call" | custom-call | tf_op jit(solution)/shard_map/before/pallas_call | solution.py:219
  151.4 4.9 %collective-permute-start.7 = (f32[16,128]{1,0:T(8,128)}, f32[16,128]{1,0:T(8,128)S(1)}, u32[]{:S(2)}, u32[]{:S(2)}) collective-permute-start(f32[16,128]{1,0:T(8,128)} %before.1.mine_ref), channel_id=1, source_target_pairs={{0,4},{4,0},{1,5},{5,1},{2,6},{6,2},{3,7},{7,3},{8,12},{12,8},{9,1... | collective-permute-start | bytes 24584 | tf_op jit(solution)/shard_map/ppermute | solution.py:379
  158.8 9.0 %answers.1 = bf16[1024,128]{1,0:T(8,128)(2,1)} custom-call(s32[3]{0:T(128)} %pad_add_fusion.at_ref, f32[16,128]{1,0:T(8,128)} %before.1.mine_ref, f32[16,128]{1,0:T(8,128)} %copy-done.9, f32[1024,512]{1,0:T(8,128)} %get-tuple-element.43.acc_re, f32[1024,512]{1,0:T(8,128)} %get-tuple-element.44.acc_im, f32[1024,512]{1,0:T(8,128)} %get-tuple-element.39.c_re, ...), custom_call_target="tpu_custom_call" | custom-call | flops 524288000 | bytes 8388608 | tf_op jit(solution)/shard_map/answers/pallas_call | solution.py:281
  167.8 1.1 copy.20
  168.9 10.3 %all_to_all.18 = bf16[4,256,128]{1,2,0:T(8,128)(2,1)S(1)} all-to-all(bf16[4,256,128]{1,2,0:T(8,128)(2,1)S(1)} %copy.20), channel_id=1, replica_groups=mesh['grp'=2,'z'=32,'core'=2,'tp'=4] {'tp'}, dimensions={0} | all-to-all | bytes 524288 | tf_op jit(solution)/shard_map/all_to_all | solution.py:384
  179.5 1.7 convolution_convert_fusion
  (68 shorter events, 17.1 us)
Async XLA Ops:
  0.0 179.5 %copy-start = (bf16[512,2048]{1,0:T(8,128)(2,1)S(1)}, bf16[512,2048]{1,0:T(8,128)(2,1)}, u32[]{:S(2)}) copy-start(bf16[512,2048]{1,0:T(8,128)(2,1)} %param.23) | copy-start | bytes 6291460
  0.0 62.8 %copy-start.7 = (f32[8,64]{1,0:T(8,128)S(1)}, f32[8,64]{1,0:T(8,128)}, u32[]{:S(2)}) copy-start(f32[8,64]{1,0:T(8,128)} %param.18) | copy-start | bytes 6148
  0.0 63.5 %copy-start.8 = (f32[8,64]{1,0:T(8,128)S(1)}, f32[8,64]{1,0:T(8,128)}, u32[]{:S(2)}) copy-start(f32[8,64]{1,0:T(8,128)} %param.19) | copy-start | bytes 6148
  0.0 80.2 %collective-permute-start = (bf16[2048,128]{1,0:T(8,128)(2,1)}, bf16[2048,128]{1,0:T(8,128)(2,1)}, u32[]{:S(2)}, u32[]{:S(2)}) collective-permute-start(bf16[2048,128]{1,0:T(8,128)(2,1)} %param.17), channel_id=1, source_target_pairs={{0,1},{1,2},{2,3},{3,0},{4,5},{5,6},{6,7},{7,4},{8,9},{9,10},{10,1... | collective-permute-start | bytes 1572872 | tf_op jit(solution)/shard_map/ppermute | solution.py:333
  4.3 80.0 %collective-permute-start.2 = (bf16[2048,128]{1,0:T(8,128)(2,1)}, bf16[2048,128]{1,0:T(8,128)(2,1)}, u32[]{:S(2)}, u32[]{:S(2)}) collective-permute-start(bf16[2048,128]{1,0:T(8,128)(2,1)} %param.17), channel_id=1, source_target_pairs={{0,2},{1,3},{2,0},{3,1},{4,6},{5,7},{6,4},{7,5},{8,10},{9,11},{10,... | collective-permute-start | bytes 1572872 | tf_op jit(solution)/shard_map/ppermute | solution.py:333
  8.9 80.9 %collective-permute-start.4 = (bf16[2048,128]{1,0:T(8,128)(2,1)}, bf16[2048,128]{1,0:T(8,128)(2,1)}, u32[]{:S(2)}, u32[]{:S(2)}) collective-permute-start(bf16[2048,128]{1,0:T(8,128)(2,1)} %param.17), channel_id=1, source_target_pairs={{0,3},{1,0},{2,1},{3,2},{4,7},{5,4},{6,5},{7,6},{8,11},{9,8},{10,9... | collective-permute-start | bytes 1572872 | tf_op jit(solution)/shard_map/ppermute | solution.py:333
  18.1 76.1 %collective-permute-start.6 = (f32[8,128]{1,0:T(8,128)S(1)}, f32[8,128]{1,0:T(8,128)S(1)}, u32[]{:S(2)}, u32[]{:S(2)}) collective-permute-start(f32[8,128]{1,0:T(8,128)S(1)} %scatter.9), channel_id=1, source_target_pairs={{0,4},{4,0},{1,5},{5,1},{2,6},{6,2},{3,7},{7,3},{8,12},{12,8},{9,1... | collective-permute-start | bytes 12296 | tf_op jit(solution)/shard_map/ppermute | solution.py:337
  66.4 11.2 %copy-start.11 = (f32[2048]{0:T(1024)S(1)}, f32[2048]{0:T(1024)}, u32[]{:S(2)}) copy-start(f32[2048]{0:T(1024)} %param.16) | copy-start | bytes 24580
  69.5 10.7 %copy-start.1 = (bf16[256,2048]{1,0:T(8,128)(2,1)S(1)}, bf16[256,2048]{1,0:T(8,128)(2,1)}, u32[]{:S(2)}) copy-start(bf16[256,2048]{1,0:T(8,128)(2,1)} %param.14) | copy-start | bytes 3145732
  81.7 17.3 %collective-permute-start.1 = (bf16[256,128]{1,0:T(8,128)(2,1)S(1)}, bf16[256,128]{1,0:T(8,128)(2,1)S(1)}, u32[]{:S(2)}, u32[]{:S(2)}) collective-permute-start(bf16[256,128]{1,0:T(8,128)(2,1)S(1)} %convolution_convert_fusion.3), channel_id=1, source_target_pairs={{0,3},{1,0},{2,1},{3,2},{4,7},{5,4},{6,5},{7,6},{8,11},{9,8},{10,9... | collective-permute-start | bytes 196616 | tf_op jit(solution)/shard_map/ppermute | solution.py:372
  85.8 13.2 %collective-permute-start.3 = (bf16[256,128]{1,0:T(8,128)(2,1)S(1)}, bf16[256,128]{1,0:T(8,128)(2,1)S(1)}, u32[]{:S(2)}, u32[]{:S(2)}) collective-permute-start(bf16[256,128]{1,0:T(8,128)(2,1)S(1)} %convolution_convert_fusion.2), channel_id=1, source_target_pairs={{0,2},{1,3},{2,0},{3,1},{4,6},{5,7},{6,4},{7,5},{8,10},{9,11},{10,... | collective-permute-start | bytes 196616 | tf_op jit(solution)/shard_map/ppermute | solution.py:372
  91.4 7.7 %collective-permute-start.5 = (bf16[256,128]{1,0:T(8,128)(2,1)S(1)}, bf16[256,128]{1,0:T(8,128)(2,1)S(1)}, u32[]{:S(2)}, u32[]{:S(2)}) collective-permute-start(bf16[256,128]{1,0:T(8,128)(2,1)S(1)} %convolution_convert_fusion.1), channel_id=1, source_target_pairs={{0,1},{1,2},{2,3},{3,0},{4,5},{5,6},{6,7},{7,4},{8,9},{9,10},{10,1... | collective-permute-start | bytes 196616 | tf_op jit(solution)/shard_map/ppermute | solution.py:372
  99.0 0.7 copy-start.4
  99.0 0.7 copy-start.5
  99.1 0.7 copy-start.6
  99.7 19.6 %copy-start.3 = (f32[2,8,16,64]{3,2,1,0:T(8,128)S(1)}, f32[2,8,16,64]{3,2,1,0:T(8,128)}, u32[]{:S(2)}) copy-start(f32[2,8,16,64]{3,2,1,0:T(8,128)} %param.21) | copy-start | bytes 196612
  112.3 35.7 %all-to-all-start = ((bf16[32,16,128]{2,1,0:T(8,128)(2,1)}), bf16[32,16,128]{2,1,0:T(8,128)(2,1)S(1)}, u32[]{:S(2)}, u32[]{:S(2)}) async-start(bf16[32,16,128]{2,1,0:T(8,128)(2,1)} %get-tuple-element.41), calls=%async_computation | async-start | bytes 262144 | tf_op jit(solution)/shard_map/all_to_all | solution.py:377
  148.1 0.7 copy-start.2
  151.4 6.8 %collective-permute-start.7 = (f32[16,128]{1,0:T(8,128)}, f32[16,128]{1,0:T(8,128)S(1)}, u32[]{:S(2)}, u32[]{:S(2)}) collective-permute-start(f32[16,128]{1,0:T(8,128)} %before.1.mine_ref), channel_id=1, source_target_pairs={{0,4},{4,0},{1,5},{5,1},{2,6},{6,2},{3,7},{7,3},{8,12},{12,8},{9,1... | collective-permute-start | bytes 24584 | tf_op jit(solution)/shard_map/ppermute | solution.py:379
  158.2 0.6 copy-start.9
  158.8 20.5 %copy-start.10 = (f32[512]{0:T(512)S(1)}, f32[512]{0:T(512)}, u32[]{:S(2)}) copy-start(f32[512]{0:T(512)} %param.22) | copy-start | bytes 6148

commit v2 on v1

v2 whole, which is shorter than its diff:
```python
from functools import partial

import jax
import jax.numpy as jnp
from jax import lax
from jax.experimental import pallas as pl
from jax.experimental.pallas import tpu as pltpu
from jax.sharding import Mesh, PartitionSpec as P

CHUNK = 128
LANES = 128
BLOCK = 8
F32 = jnp.float32
BF16 = jnp.bfloat16
TWO_PI_HIGH = 6.28125
TWO_PI_LOW = 0.0019353071795864769
INV_TWO_PI = 0.15915494309189535
SIN = (6.2831854820251465, -41.3416862487793, 81.60456085205078, -76.69428253173828,
       41.96574020385742, -14.708574295043945, 3.0096182823181152)
COS = (1.0, -19.739208221435547, 64.9393539428711, -85.45588684082031, 60.23442077636719,
       -26.364990234375, 7.6985273361206055, -1.3503994941711426)


def polynomial(x, factors):
    total = factors[-1] * x + factors[-2]
    for factor in factors[-3::-1]:
        total = total * x + factor
    return total


def split_turns(freq):
    plain = freq * INV_TWO_PI
    high = jnp.round(plain * 8192.0) * (1.0 / 8192.0)
    rest = (freq - high * TWO_PI_HIGH) - high * TWO_PI_LOW
    return high, rest * INV_TWO_PI, plain


def rotation(coarse, fine, turns, again=False):
    high, rest, plain = turns
    whole = coarse * high
    part = (whole - jnp.round(whole)) + (coarse * rest + fine * plain)
    if again:
        part = part - jnp.round(part)
    square = part * part
    return polynomial(square, COS), part * polynomial(square, SIN)


def decayed(coarse, fine, rate, turns):
    cosine, sine = rotation(coarse, fine, turns, again=True)
    magnitude = jnp.exp(-rate * (coarse + fine))
    return magnitude * cosine, magnitude * sine


def high_low(x):
    high = x.astype(BF16)
    return high, (x - high.astype(F32)).astype(BF16)


def dot_t(a, b):
    return lax.dot_general(a, b, (((1,), (1,)), ((), ())), preferred_element_type=F32)


def whole(array):
    return pl.BlockSpec(array.shape, lambda *at: (0,) * array.ndim)


def iota(shape, dim):
    return lax.broadcasted_iota(jnp.int32, shape, dim)


def triangle(repeat=1):
    shape = (CHUNK, repeat * CHUNK)
    return jnp.where((iota(shape, 1) % CHUNK) <= iota(shape, 0), 1.0, 0.0).astype(BF16)


def tables_kernel(step_ref, rate_ref, freq_ref, map_ref, readout_ref, w_re, w_im, c_re, c_im,
                  push_ref, read_ref, modes_ref, times_ref):
    chunk = pl.program_id(0)
    blocks = modes_ref.shape[0] // 2
    per_block, entries = rate_ref.shape[0] // blocks, rate_ref.shape[1]

    @pl.when(chunk == 0)
    def _():
        times_ref[...] = jnp.zeros_like(times_ref)
        for b in range(blocks):
            mine = range(per_block * b, per_block * (b + 1))
            modes_ref[b:b + 1, :] = jnp.concatenate([rate_ref[g:g + 1, :] for g in mine], axis=1)
            modes_ref[blocks + b:blocks + b + 1, :] = jnp.concatenate([freq_ref[g:g + 1, :] for g in mine], axis=1)

    for b in range(blocks):
        @pl.when(chunk == b)
        def _(b=b):
            read_ref[b] = jnp.zeros(read_ref.shape[1:], BF16)
            for j in range(per_block):
                g = per_block * b + j
                members = map_ref.shape[-1]
                place = (iota((members, LANES), 1) == iota((members, LANES), 0) + members * g)
                place = jnp.where(place, 1.0, 0.0).astype(BF16)
                seat = (iota((entries, LANES), 1) == iota((entries, LANES), 0) + entries * j)
                seat = jnp.where(seat, 1.0, 0.0).astype(BF16)
                for part in range(2):
                    rows = slice(part * LANES + entries * j, part * LANES + entries * (j + 1))
                    for k, piece in enumerate(high_low(map_ref[part, g])):
                        spread = jnp.dot(piece, place, preferred_element_type=F32)
                        push_ref[b, rows, k * LANES:(k + 1) * LANES] = spread.astype(BF16)
                    sign = 1.0 if part == 0 else -1.0
                    for k, piece in enumerate(high_low(sign * readout_ref[part, g])):
                        spread = jnp.dot(piece, seat, preferred_element_type=F32)
                        first = k * LANES + members * g
                        read_ref[b, first:first + members, part * LANES:(part + 1) * LANES] = spread.astype(BF16)

    lower = triangle()
    steps = jnp.broadcast_to(step_ref[pl.ds(chunk, 1), :], (CHUNK, CHUNK))
    grid = jnp.round(steps * 8192.0) * (1.0 / 8192.0)

    def running(values):
        high, low = high_low(values)
        return dot_t(lower, high) + dot_t(lower, low)

    run = running(grid)
    coarse = jnp.round(run * 8.0) * 0.125
    fine = (run - coarse) + running(steps - grid)
    times_ref[0:1, :] += coarse[CHUNK - 1:]
    times_ref[1:2, :] += fine[CHUNK - 1:]
    elapsed = coarse + fine
    first = iota((CHUNK, LANES), 0) == 0
    for b in range(blocks):
        cols = slice(b * LANES, (b + 1) * LANES)
        rate = modes_ref[b:b + 1, :]
        freq = modes_ref[blocks + b:blocks + b + 1, :]
        cosine, sine = rotation(coarse, fine, split_turns(freq))
        exponent = rate * elapsed
        shrink = jnp.exp(-exponent)
        c_re[:, cols] = shrink * cosine
        c_im[:, cols] = shrink * sine
        grow = jnp.exp(exponent)
        g_re = grow * cosine
        g_im = -(grow * sine)
        d_re = jnp.where(first, 1.0, pltpu.roll(g_re, 1, 0)) - g_re
        d_im = jnp.where(first, 0.0, pltpu.roll(g_im, 1, 0)) - g_im
        scale = 1.0 / (rate * rate + freq * freq)
        l_re, l_im = -rate * scale, -freq * scale
        w_re[:, cols] = d_re * l_re - d_im * l_im
        w_im[:, cols] = d_re * l_im + d_im * l_re


def tables(step, rate, freq, input_map, readout):
    width = rate.size
    blocks = width // LANES
    chunks = step.shape[0]
    rows = chunks * CHUNK
    block = pl.BlockSpec((CHUNK, width), lambda c: (c, 0))
    big = jax.ShapeDtypeStruct((rows, width), F32)
    matrix = jax.ShapeDtypeStruct((blocks, 2 * LANES, 2 * LANES), BF16)
    modes = jax.ShapeDtypeStruct((2 * blocks, LANES), F32)
    times = jax.ShapeDtypeStruct((8, LANES), F32)
    small = [matrix, matrix, modes, times]
    return pl.pallas_call(
        tables_kernel, grid=(chunks,), in_specs=[whole(x) for x in (step, rate, freq, input_map, readout)],
        out_specs=[block] * 4 + [whole(x) for x in small], out_shape=[big] * 4 + small, name="tables",
        cost_estimate=pl.CostEstimate(flops=rows * width * 60, transcendentals=0, bytes_accessed=rows * width * 16),
    )(step, rate, freq, input_map, readout)


def project_kernel(at_ref, rows_ref, _, *refs):
    out_ref = refs[-1]
    ways = len(refs) - 1
    for back, proj in enumerate(refs[:-1]):
        owner = (at_ref[0] - back + ways) % ways
        out_ref[owner] = jnp.dot(rows_ref[...], proj[...], preferred_element_type=F32).astype(BF16)


def project(at, rows, after, projs):
    out = jax.ShapeDtypeStruct((len(projs), rows.shape[0], projs[0].shape[1]), BF16)
    return pl.pallas_call(
        project_kernel,
        grid_spec=pltpu.PrefetchScalarGridSpec(
            num_scalar_prefetch=1, grid=(1,), in_specs=[whole(x) for x in (rows, after, *projs)], out_specs=whole(out)),
        out_shape=out, name="project",
        cost_estimate=pl.CostEstimate(flops=2 * rows.size * len(projs) * LANES, transcendentals=0,
                                      bytes_accessed=4 * rows.size),
    )(at, rows, after, *projs)


def sums_kernel(drive_ref, w_re, w_im, c_re, c_im, push_ref, times_ref, acc_re, acc_im, sent_ref,
                stacked, carry):
    chunk = pl.program_id(0)
    blocks = push_ref.shape[0]

    @pl.when(chunk == 0)
    def _():
        carry[...] = jnp.zeros_like(carry)

    drive = drive_ref[...]
    twice = jnp.concatenate([drive, drive], axis=1)
    for b in range(blocks):
        cols = slice(b * LANES, (b + 1) * LANES)
        pushed = dot_t(twice, push_ref[b])
        p_re, p_im = pushed[:, :LANES], pushed[:, LANES:]
        wr, wi = w_re[:, cols], w_im[:, cols]
        high, low = high_low(wr * p_re - wi * p_im)
        stacked[b, :CHUNK, :LANES] = high
        stacked[b, CHUNK:, :LANES] = low
        high, low = high_low(wr * p_im + wi * p_re)
        stacked[b, :CHUNK, LANES:] = high
        stacked[b, CHUNK:, LANES:] = low
    lower = triangle(2)
    for b in range(blocks):
        cols = slice(b * LANES, (b + 1) * LANES)
        acc = jnp.dot(lower, stacked[b], preferred_element_type=F32)
        acc_re[:, cols] = acc[:, :LANES]
        acc_im[:, cols] = acc[:, LANES:]
        cr, ci = c_re[7:8, cols], c_im[7:8, cols]
        tr = acc[CHUNK - 1:, :LANES] + carry[b:b + 1, :]
        ti = acc[CHUNK - 1:, LANES:] + carry[blocks + b:blocks + b + 1, :]
        carry[b:b + 1, :] = cr * tr - ci * ti
        carry[blocks + b:blocks + b + 1, :] = cr * ti + ci * tr

    @pl.when(chunk == pl.num_programs(0) - 1)
    def _():
        message = jnp.concatenate([carry[...], times_ref[...]], axis=0)
        for k in range(sent_ref.shape[0]):
            sent_ref[k] = message


def sums(drive, w_re, w_im, c_re, c_im, push, times, peers):
    rows, width = w_re.shape
    blocks = width // LANES
    block = pl.BlockSpec((CHUNK, width), lambda c: (c, 0))
    last = pl.BlockSpec((8, width), lambda c: ((c + 1) * (CHUNK // 8) - 1, 0))
    big = jax.ShapeDtypeStruct((rows, width), F32)
    sent = jax.ShapeDtypeStruct((peers, 2 * blocks + 8, LANES), F32)
    return pl.pallas_call(
        sums_kernel, grid=(rows // CHUNK,),
        in_specs=[pl.BlockSpec((CHUNK, drive.shape[1]), lambda c: (c, 0)), block, block, last, last,
                  whole(push), whole(times)],
        out_specs=[block, block, whole(sent)],
        scratch_shapes=[pltpu.VMEM((blocks, 2 * CHUNK, 2 * LANES), BF16), pltpu.VMEM((2 * blocks, LANES), F32)],
        out_shape=[big, big, sent], name="sums",
        cost_estimate=pl.CostEstimate(flops=rows * width * 1500, transcendentals=0, bytes_accessed=rows * width * 16),
    )(drive, w_re, w_im, c_re, c_im, push, times)


def compose_kernel(at_ref, heard_ref, modes_ref, out_ref):
    blocks = modes_ref.shape[0] // 2
    rate = modes_ref[:blocks]
    turns = split_turns(modes_ref[blocks:])
    dr, di = jnp.ones(rate.shape, F32), jnp.zeros(rate.shape, F32)
    er, ei = jnp.zeros(rate.shape, F32), jnp.zeros(rate.shape, F32)
    count = heard_ref.shape[0]
    for k in range(count):
        @pl.when(at_ref[1] == k)
        def _(now=(er, ei, dr, di)):
            for j in range(4):
                out_ref[j * blocks:(j + 1) * blocks] = now[j]
        whole_time = heard_ref[k, 2 * blocks:2 * blocks + 1, :]
        coarse = jnp.round(whole_time)
        fine = (whole_time - coarse) + heard_ref[k, 2 * blocks + 1:2 * blocks + 2, :]
        xr, xi = decayed(coarse, fine, rate, turns)
        er, ei = (xr * er - xi * ei + heard_ref[k, :blocks], xr * ei + xi * er + heard_ref[k, blocks:2 * blocks])
        dr, di = xr * dr - xi * di, xr * di + xi * dr
    for j, value in enumerate((er, ei, dr, di)):
        out_ref[(4 + j) * blocks:(5 + j) * blocks] = value


def compose(at, heard, modes):
    out = jax.ShapeDtypeStruct((4 * modes.shape[0], LANES), F32)
    return pl.pallas_call(
        compose_kernel,
        grid_spec=pltpu.PrefetchScalarGridSpec(
            num_scalar_prefetch=1, grid=(1,), in_specs=[whole(heard), whole(modes)], out_specs=whole(out)),
        out_shape=out, name="compose",
    )(at, heard, modes)


def answer_kernel(near_ref, far_ref, acc_re, acc_im, c_re, c_im, read_ref, out_ref, high, low, carry):
    blocks = read_ref.shape[0]

    @pl.when(pl.program_id(0) == 0)
    def _():
        er, ei = near_ref[:blocks], near_ref[blocks:2 * blocks]
        dr, di = near_ref[2 * blocks:3 * blocks], near_ref[3 * blocks:4 * blocks]
        fr, fi = far_ref[:blocks], far_ref[blocks:]
        carry[:blocks] = dr * fr - di * fi + er
        carry[blocks:] = dr * fi + di * fr + ei

    for b in range(blocks):
        cols = slice(b * LANES, (b + 1) * LANES)
        tr = acc_re[:, cols] + carry[b:b + 1, :]
        ti = acc_im[:, cols] + carry[blocks + b:blocks + b + 1, :]
        cr, ci = c_re[:, cols], c_im[:, cols]
        sr = cr * tr - ci * ti
        si = cr * ti + ci * tr
        carry[b:b + 1, :] = sr[CHUNK - 1:]
        carry[blocks + b:blocks + b + 1, :] = si[CHUNK - 1:]
        high[b, :, :LANES], low[b, :, :LANES] = high_low(sr)
        high[b, :, LANES:], low[b, :, LANES:] = high_low(si)
    value = jnp.zeros((CHUNK, LANES), F32)
    for b in range(blocks):
        total = dot_t(high[b], read_ref[b])
        value = value + total[:, :LANES] + total[:, LANES:] + dot_t(low[b], read_ref[b, :LANES])
    inner = 0.7978845608 * (value + 0.044715 * (value * value * value))
    out_ref[...] = (0.5 * value * (1.0 + jnp.tanh(inner))).astype(BF16)


def answers(near, far, acc_re, acc_im, c_re, c_im, read):
    rows, width = acc_re.shape
    blocks = width // LANES
    block = pl.BlockSpec((CHUNK, width), lambda c: (c, 0))
    store = pltpu.VMEM((blocks, CHUNK, 2 * LANES), BF16)
    return pl.pallas_call(
        answer_kernel, grid=(rows // CHUNK,),
        in_specs=[whole(near), whole(far)] + [block] * 4 + [whole(read)],
        out_specs=pl.BlockSpec((CHUNK, LANES), lambda c: (c, 0)),
        scratch_shapes=[store, store, pltpu.VMEM((2 * blocks, LANES), F32)],
        out_shape=jax.ShapeDtypeStruct((rows, LANES), BF16), name="answers",
        cost_estimate=pl.CostEstimate(flops=rows * width * 1000, transcendentals=0, bytes_accessed=rows * width * 16),
    )(near, far, acc_re, acc_im, c_re, c_im, read)


def output_kernel(parts_ref, gain_ref, proj_ref, out_ref, shaped):
    pieces, _, part = parts_ref.shape

    @pl.when(pl.program_id(0) == 0)
    def _():
        total = jnp.zeros((parts_ref.shape[1], 1), F32)
        for k in range(pieces):
            values = parts_ref[k].astype(F32)
            total = total + jnp.sum(values * values, axis=1, keepdims=True)
        factor = lax.rsqrt(total * (1.0 / (pieces * part)) + 1e-06)
        for k in range(pieces):
            cols = slice(k * part, (k + 1) * part)
            shaped[:, cols] = (parts_ref[k].astype(F32) * factor * gain_ref[:, cols]).astype(BF16)

    out_ref[...] = jnp.dot(shaped[...], proj_ref[...], preferred_element_type=F32).astype(BF16)


def output(parts, gain, proj, tile=512):
    rows = parts.shape[1]
    width = proj.shape[1]
    return pl.pallas_call(
        output_kernel, grid=(width // tile,),
        in_specs=[whole(parts), whole(gain), pl.BlockSpec((proj.shape[0], tile), lambda n: (0, n))],
        out_specs=pl.BlockSpec((rows, tile), lambda n: (0, n)),
        scratch_shapes=[pltpu.VMEM((rows, proj.shape[0]), BF16)],
        out_shape=jax.ShapeDtypeStruct((rows, width), BF16), name="output",
    )(parts, gain, proj)


def rms_rows(values, gain):
    values = values.astype(F32)
    scaled = values * lax.rsqrt(jnp.mean(values * values, axis=-1, keepdims=True) + 1e-06)
    return (scaled * gain).astype(BF16)


def ring(count, by):
    return [(k, (k + by) % count) for k in range(count)]


def on_device(
    tokens, step, in_gain, in_proj, decay_rate, frequency, input_map, readout, out_gain, out_proj
):
    ways = lax.axis_size("tp")
    place = lax.axis_index(("zl", "core"))
    at = jnp.stack([lax.axis_index("tp"), place]).astype(jnp.int32)
    projs = [in_proj] + [lax.ppermute(in_proj, "tp", ring(ways, by)) for by in range(1, ways)]
    w_re, w_im, c_re, c_im, push, read, modes, times = tables(
        step.reshape(-1, CHUNK), decay_rate, frequency, input_map, readout
    )
    normed = rms_rows(tokens, in_gain)
    drive = lax.all_to_all(project(at, normed, times, projs), "tp", 0, 0, tiled=True)
    peers = lax.axis_size("zl") * lax.axis_size("core")
    acc_re, acc_im, sent = sums(
        drive.reshape(-1, drive.shape[-1]), w_re, w_im, c_re, c_im, push, times, peers
    )
    near = compose(at, lax.all_to_all(sent, ("zl", "core"), 0, 0, tiled=True), modes)
    half = modes.shape[0]
    quarter = half // 2
    er, ei, dr, di = (near[2 * half + k * quarter:2 * half + (k + 1) * quarter] for k in range(4))
    fr = jnp.zeros_like(er)
    fi = jnp.zeros_like(ei)
    for k in range(lax.axis_size("zh") - 1):
        leaves = jnp.concatenate([dr * fr - di * fi + er, dr * fi + di * fr + ei], axis=0)
        comes = lax.ppermute(leaves, "zh", [(k, k + 1)])
        fr, fi = fr + comes[:quarter], fi + comes[quarter:]
    far = jnp.concatenate([fr, fi], axis=0)
    answer = answers(near, far, acc_re, acc_im, c_re, c_im, read)
    parts = lax.all_to_all(answer.reshape(ways, -1, LANES), "tp", 0, 0, tiled=True)
    return output(parts, out_gain.reshape(1, -1), out_proj)


def solution(mesh):
    shape = mesh.shape
    chips = shape["sp"] // 2
    near = min(BLOCK, chips)
    devices = mesh.devices.reshape(shape["grp"], chips // near, near, 2, shape["tp"])
    fine_mesh = Mesh(devices, ("grp", "zh", "zl", "core", "tp"))
    rows = ("grp", "zh", "zl", "core", "tp")
    placed = (
        P(rows, None),
        P(("grp", "zh", "zl", "core")),
        P(),
        P(None, "tp"),
        P("tp", None),
        P("tp", None),
        P(None, "tp", None, None),
        P(None, "tp", None, None),
        P(),
        P(),
    )
    return jax.shard_map(
        on_device,
        mesh=fine_mesh,
        in_specs=placed,
        out_specs=P(rows, None),
        check_vma=False,
    )
```

time: 183 us -> 141 us (0.77)
  blocking collectives: 10.3 us -> 74.9 us
  starting transfers between devices: 73.7 us -> 15.8 us
  waiting for transfers between devices: 28.7 us -> 0.75 us
  local copies, waits for them, and re-layouts: 15.4 us -> 3.08 us
  matrix products: 10.5 us -> 0 us
  Pallas kernels: 32.5 us -> 38 us
  between operations: 4.44 us -> 0.14 us
    all_to_all x1 -> x3, blocking collectives: 10.3 us -> 74.9 us  [the longest x1 55.5 us: on_device(): lax.all_to_all(sent, ('zl', 'core'), 0, 0, tiled=True)]
    ppermute x8 -> x6, starting transfers between devices: 66.7 us -> 15.8 us  [the longest x3 12.5 us: on_device(): lax.ppermute(in_proj, 'tp', ring(ways, by))]
    all_to_all x1 -> x0, waiting for transfers between devices: 28.7 us -> none  [on_device(): heard = lax.all_to_all(sent, 'z', 0, 0, tiled=True)]
    dot_general x7 -> x0, matrix products: 10.5 us -> none  [the longest x4 7.12 us: driven(): return jnp.dot(normed, proj, preferred_element_type=F32).astype(BF16)]
    all_to_all x1 -> x0, starting transfers between devices: 6.93 us -> none  [on_device(): heard = lax.all_to_all(sent, 'z', 0, 0, tiled=True)]
    pallas_call x4 -> x6, Pallas kernels: 32.5 us -> 38 us  [the longest x1 9.34 us: tables(): pl.pallas_call(tables_kernel, grid=(chunks,), in_specs=[whole(x) for x in...]
    reshape x6 -> x0, local copies, waits for them, and re-layouts: 4.66 us -> none  [the longest x2 2.08 us: elapsed_parts(): return (coarse.reshape(-1, 1), fine.reshape(-1, 1), whole, left)]
    mul x7 -> x0, local copies, waits for them, and re-layouts: 3.76 us -> none  [the longest x4 1.99 us: spread(): small[:, :, None, :] * unit[:, None, :, None]]
  transfers between devices with their start and end apart: 9 -> 6, of which waited for: 1 -> 1; matrix products, arithmetic and copies ran while one was open for 15% -> 4% of each run, Pallas kernels for 5% -> 7%
where the time goes in v2:
time: 141 us; the launch traced here: 139 us
  blocking collectives  74.9 us (53%)
  Pallas kernels  38 us (27%)
  starting transfers between devices  15.8 us (11%)
  other arithmetic  6.34 us (4%)
  local copies, waits for them, and re-layouts  3.08 us (2%)
    all_to_all x1, blocking collectives, on_device(): lax.all_to_all(sent, ('zl', 'core'), 0, 0, tiled=True)  55.5 us
    ppermute x3, starting transfers between devices, on_device(): lax.ppermute(in_proj, 'tp', ring(ways, by))  12.5 us
    all_to_all x1, blocking collectives, on_device(): lax.all_to_all(project(at, normed, times, projs), 'tp', 0, 0, tiled=True)  9.67 us
    all_to_all x1, blocking collectives, on_device(): lax.all_to_all(answer.reshape(ways, -1, LANES), 'tp', 0, 0, tiled=True)  9.66 us
    pallas_call x1, Pallas kernels, tables(): pl.pallas_call(tables_kernel, grid=(chunks,), in_specs=[whole(x) for x in...  9.34 us
    pallas_call x1, Pallas kernels, sums(): pl.pallas_call(sums_kernel, grid=(rows // CHUNK,), in_specs=[pl.BlockSpec...  8.96 us
    pallas_call x1, Pallas kernels, answers(): pl.pallas_call(answer_kernel, grid=(rows // CHUNK,), in_specs=[whole(near...  8.07 us
    pallas_call x1, Pallas kernels, output(): pl.pallas_call(output_kernel, grid=(width // tile,), in_specs=[whole(part...  4.48 us
  transfers between devices with their start and end apart: 6, of which 1 were waited for; matrix products, arithmetic and copies ran while one was open for 4% of the time, Pallas kernels for 7%

profile of v2, /device:TPU:33, one launch (start us, length us, event | category | flops | bytes accessed | tf_op | source)
XLA Modules:
  0.0 139.0 jit_solution(9813535081955290362)
XLA Ops:
  0.0 5.9 %collective-permute-start.1 = (bf16[2048,128]{1,0:T(8,128)(2,1)}, bf16[2048,128]{1,0:T(8,128)(2,1)S(1)}, u32[]{:S(2)}, u32[]{:S(2)}) collective-permute-start(bf16[2048,128]{1,0:T(8,128)(2,1)} %refs_0_.1), channel_id=1, source_target_pairs={{0,2},{1,3},{2,0},{3,1},{4,6},{5,7},{6,4},{7,5},{8,10},{9,11},{10,... | collective-permute-start | bytes 1572872 | tf_op jit(solution)/shard_map/ppermute | solution.py:366
  5.9 2.4 %collective-permute-start = (bf16[2048,128]{1,0:T(8,128)(2,1)}, bf16[2048,128]{1,0:T(8,128)(2,1)S(1)}, u32[]{:S(2)}, u32[]{:S(2)}) collective-permute-start(bf16[2048,128]{1,0:T(8,128)(2,1)} %refs_0_.1), channel_id=1, source_target_pairs={{0,1},{1,2},{2,3},{3,0},{4,5},{5,6},{6,7},{7,4},{8,9},{9,10},{10,1... | collective-permute-start | bytes 1572872 | tf_op jit(solution)/shard_map/ppermute | solution.py:366
  8.3 4.2 %collective-permute-start.2 = (bf16[2048,128]{1,0:T(8,128)(2,1)}, bf16[2048,128]{1,0:T(8,128)(2,1)S(1)}, u32[]{:S(2)}, u32[]{:S(2)}) collective-permute-start(bf16[2048,128]{1,0:T(8,128)(2,1)} %refs_0_.1), channel_id=1, source_target_pairs={{0,3},{1,0},{2,1},{3,2},{4,7},{5,4},{6,5},{7,6},{8,11},{9,8},{10,9... | collective-permute-start | bytes 1572872 | tf_op jit(solution)/shard_map/ppermute | solution.py:366
  12.5 1.5 %fusion = f32[256]{0:T(256)S(1)} fusion(bf16[256,2048]{1,0:T(8,128)(2,1)} %param.10), kind=kLoop, calls=%fused_computation.2 | loop fusion | flops 1572608 | bytes 1049600 | tf_op jit(solution)/shard_map/reduce_sum | solution.py:352
  14.0 0.6 pad_add_fusion.at_ref
  14.7 1.9 %copy.11.map_ref = f32[2,8,64,16]{3,2,1,0:T(8,128)} copy(f32[2,8,64,16]{2,3,1,0:T(8,128)} %param.16) | data formatting | bytes 131072 | tf_op args[6]
  16.6 9.3 %tables.1 = (f32[1024,512]{1,0:T(8,128)}, f32[1024,512]{1,0:T(8,128)}, f32[1024,512]{1,0:T(8,128)}, f32[1024,512]{1,0:T(8,128)}, bf16[4,256,256]{2,1,0:T(8,128)(...) custom-call(f32[8,128]{1,0:T(8,128)} %bitcast.8, f32[8,64]{1,0:T(8,128)} %rate_ref.1, ...), custom_call_target="tpu_custom_call" | custom-call | flops 31457280 | bytes 8388608 | tf_op jit(solution)/shard_map/tables/pallas_call | solution.py:158
  25.9 1.3 fusion.2.rows_ref
  27.3 0.8 copy-done.1
  28.4 4.5 %project.1 = bf16[4,256,128]{2,1,0:T(8,128)(2,1)} custom-call(s32[2]{0:T(128)} %pad_add_fusion.at_ref, bf16[256,2048]{1,0:T(8,128)(2,1)} %fusion.2.rows_ref, f32[8,128]{1,0:T(8,128)} %get-tuple-element.16._.times_ref, bf16[2048,128]{1,0:T(8,128)(2,1)} %refs_0_.1, bf16[2048,128]{1,0:T(8,128)(2,1)} %copy-done.2, bf16[2048,128]{1,0:T(8,128)(2,1)} %copy-done.1, ...), custom_call_target="tpu_custom_call" | custom-call | flops 536870912 | bytes 2097152 | tf_op jit(solution)/shard_map/project/pallas_call | solution.py:175
  32.9 9.7 %all_to_all.15 = bf16[4,256,128]{2,1,0:T(8,128)(2,1)} all-to-all(bf16[4,256,128]{2,1,0:T(8,128)(2,1)} %project.1), channel_id=1, replica_groups=mesh['grp'=2,'zh'=4,'zl'=8,'core'=2,'tp'=4] {'tp'}, dimensions={0} | all-to-all | bytes 524288 | tf_op jit(solution)/shard_map/all_to_all | solution.py:371
  42.5 9.0 %sums.1 = (f32[1024,512]{1,0:T(8,128)}, f32[1024,512]{1,0:T(8,128)}, f32[16,16,128]{2,1,0:T(8,128)}) custom-call(bf16[1024,128]{1,0:T(8,128)(2,1)} %bitcast.6, f32[1024,512]{1,0:T(8,128)} %get-tuple-element.17.w_re, f32[1024,512]{1,0:T(8,128)} %get-tuple-element.18.w_im, f32[1024,512]{1,0:T(8,128)} %get-tuple-element.19.c_re, ...), custom_call_target="tpu_custom_call" | custom-call | flops 786432000 | bytes 8388608 | tf_op jit(solution)/shard_map/sums/pallas_call | solution.py:233
  51.5 55.5 %all_to_all.16.heard_ref = f32[16,16,128]{2,1,0:T(8,128)} all-to-all(f32[16,16,128]{2,1,0:T(8,128)} %get-tuple-element.22), channel_id=1, replica_groups=mesh['grp'=2,'zh'=4,'zl'=8,'core'=2,'tp'=4] {'zl','core'}, dimensions={0} | all-to-all | bytes 262144 | tf_op jit(solution)/shard_map/all_to_all | solution.py:376
  107.0 2.7 %compose.1.near_ref = f32[32,128]{1,0:T(8,128)} custom-call(s32[2]{0:T(128)} %pad_add_fusion.at_ref, f32[16,16,128]{2,1,0:T(8,128)} %all_to_all.16.heard_ref, f32[8,128]{1,0:T(8,128)} %get-tuple-element.23.modes_ref), custom_call_target="tpu_custom_call" | custom-call | tf_op jit(solution)/shard_map/compose/pallas_call | solution.py:268
  109.7 0.8 subtract_add_fusion.2
  110.5 2.1 %collective-permute-start.3 = (f32[8,128]{1,0:T(8,128)S(1)}, f32[8,128]{1,0:T(8,128)S(1)}, u32[]{:S(2)}, u32[]{:S(2)}) collective-permute-start(f32[8,128]{1,0:T(8,128)S(1)} %pad_maximum_fusion), channel_id=1, source_target_pairs={{0,64},{1,65},{2,66},{3,67},{4,68},{5,69},{6,70},{7,71},{8,72},{9,... | collective-permute-start | bytes 12296 | tf_op jit(solution)/shard_map/ppermute | solution.py:384
  112.5 0.7 collective-permute-done.3
  113.3 0.8 subtract_add_fusion.1
  114.1 0.7 collective-permute-start.4
  114.7 0.8 subtract_add_fusion
  115.5 0.7 collective-permute-start.5
  116.8 8.1 %answers.1 = bf16[1024,128]{1,0:T(8,128)(2,1)} custom-call(f32[32,128]{1,0:T(8,128)} %compose.1.near_ref, f32[8,128]{1,0:T(8,128)} %pad_maximum_fusion.3.far_ref, f32[1024,512]{1,0:T(8,128)} %get-tuple-element.24.acc_re, f32[1024,512]{1,0:T(8,128)} %get-tuple-element.25.acc_im, f32[1024,512]{1,0:T(8,128)} %get-tuple-element.19.c_re, ...), custom_call_target="tpu_custom_call" | custom-call | flops 524288000 | bytes 8388608 | tf_op jit(solution)/shard_map/answers/pallas_call | solution.py:311
  124.9 9.7 %all_to_all.17.parts_ref = bf16[4,256,128]{2,1,0:T(8,128)(2,1)} all-to-all(bf16[4,256,128]{2,1,0:T(8,128)(2,1)} %bitcast.7), channel_id=1, replica_groups=mesh['grp'=2,'zh'=4,'zl'=8,'core'=2,'tp'=4] {'tp'}, dimensions={0} | all-to-all | bytes 524288 | tf_op jit(solution)/shard_map/all_to_all | solution.py:388
  134.5 4.5 %output.1 = bf16[256,2048]{1,0:T(8,128)(2,1)} custom-call(bf16[4,256,128]{2,1,0:T(8,128)(2,1)} %all_to_all.17.parts_ref, f32[1,512]{1,0:T(1,128)} %bitcast.9, bf16[512,2048]{1,0:T(8,128)(2,1)} %proj_ref.1), custom_call_target="tpu_custom_call" | custom-call | tf_op jit(solution)/shard_map/output/pallas_call | solution.py:341
  (20 shorter events, 1.0 us)
Async XLA Ops:
  0.0 25.9 %copy-start = (bf16[256,2048]{1,0:T(8,128)(2,1)S(1)}, bf16[256,2048]{1,0:T(8,128)(2,1)}, u32[]{:S(2)}) copy-start(bf16[256,2048]{1,0:T(8,128)(2,1)} %param.10) | copy-start | bytes 3145732
  0.0 25.9 %copy-start.4 = (f32[2048]{0:T(1024)S(1)}, f32[2048]{0:T(1024)}, u32[]{:S(2)}) copy-start(f32[2048]{0:T(1024)} %param.12) | copy-start | bytes 24580
  0.0 27.2 %collective-permute-start.1 = (bf16[2048,128]{1,0:T(8,128)(2,1)}, bf16[2048,128]{1,0:T(8,128)(2,1)S(1)}, u32[]{:S(2)}, u32[]{:S(2)}) collective-permute-start(bf16[2048,128]{1,0:T(8,128)(2,1)} %refs_0_.1), channel_id=1, source_target_pairs={{0,2},{1,3},{2,0},{3,1},{4,6},{5,7},{6,4},{7,5},{8,10},{9,11},{10,... | collective-permute-start | bytes 1572872 | tf_op jit(solution)/shard_map/ppermute | solution.py:366
  5.9 21.3 %collective-permute-start = (bf16[2048,128]{1,0:T(8,128)(2,1)}, bf16[2048,128]{1,0:T(8,128)(2,1)S(1)}, u32[]{:S(2)}, u32[]{:S(2)}) collective-permute-start(bf16[2048,128]{1,0:T(8,128)(2,1)} %refs_0_.1), channel_id=1, source_target_pairs={{0,1},{1,2},{2,3},{3,0},{4,5},{5,6},{6,7},{7,4},{8,9},{9,10},{10,1... | collective-permute-start | bytes 1572872 | tf_op jit(solution)/shard_map/ppermute | solution.py:366
  8.3 18.9 %collective-permute-start.2 = (bf16[2048,128]{1,0:T(8,128)(2,1)}, bf16[2048,128]{1,0:T(8,128)(2,1)S(1)}, u32[]{:S(2)}, u32[]{:S(2)}) collective-permute-start(bf16[2048,128]{1,0:T(8,128)(2,1)} %refs_0_.1), channel_id=1, source_target_pairs={{0,3},{1,0},{2,1},{3,2},{4,7},{5,4},{6,5},{7,6},{8,11},{9,8},{10,9... | collective-permute-start | bytes 1572872 | tf_op jit(solution)/shard_map/ppermute | solution.py:366
  27.2 0.8 copy-start.1
  27.2 1.0 copy-start.2
  27.2 1.2 copy-start.3
  110.5 2.8 %collective-permute-start.3 = (f32[8,128]{1,0:T(8,128)S(1)}, f32[8,128]{1,0:T(8,128)S(1)}, u32[]{:S(2)}, u32[]{:S(2)}) collective-permute-start(f32[8,128]{1,0:T(8,128)S(1)} %pad_maximum_fusion), channel_id=1, source_target_pairs={{0,64},{1,65},{2,66},{3,67},{4,68},{5,69},{6,70},{7,71},{8,72},{9,... | collective-permute-start | bytes 12296 | tf_op jit(solution)/shard_map/ppermute | solution.py:384
  114.1 0.7 collective-permute-start.4
  115.5 0.7 collective-permute-start.5

commit v3 on v2

v3 whole, which is shorter than its diff:
```python
from functools import partial

import jax
import jax.numpy as jnp
from jax import lax
from jax.experimental import pallas as pl
from jax.experimental.pallas import tpu as pltpu
from jax.sharding import Mesh, PartitionSpec as P

CHUNK = 128
TILE = 512
LANES = 128
BLOCK = 4
F32 = jnp.float32
BF16 = jnp.bfloat16
TWO_PI_HIGH = 6.28125
TWO_PI_LOW = 0.0019353071795864769
INV_TWO_PI = 0.15915494309189535
SIN = (6.2831854820251465, -41.3416862487793, 81.60456085205078, -76.69428253173828,
       41.96574020385742, -14.708574295043945, 3.0096182823181152)
COS = (1.0, -19.739208221435547, 64.9393539428711, -85.45588684082031, 60.23442077636719,
       -26.364990234375, 7.6985273361206055, -1.3503994941711426)


def polynomial(x, factors):
    total = factors[-1] * x + factors[-2]
    for factor in factors[-3::-1]:
        total = total * x + factor
    return total


def split_turns(freq):
    plain = freq * INV_TWO_PI
    high = jnp.round(plain * 8192.0) * (1.0 / 8192.0)
    rest = (freq - high * TWO_PI_HIGH) - high * TWO_PI_LOW
    return high, rest * INV_TWO_PI, plain


def rotation(coarse, fine, turns, again=False):
    high, rest, plain = turns
    whole = coarse * high
    part = (whole - jnp.round(whole)) + (coarse * rest + fine * plain)
    if again:
        part = part - jnp.round(part)
    square = part * part
    return polynomial(square, COS), part * polynomial(square, SIN)


def decayed(coarse, fine, rate, turns):
    cosine, sine = rotation(coarse, fine, turns, again=True)
    magnitude = jnp.exp(-rate * (coarse + fine))
    return magnitude * cosine, magnitude * sine


def high_low(x):
    high = x.astype(BF16)
    return high, (x - high.astype(F32)).astype(BF16)


def dot_t(a, b):
    return lax.dot_general(a, b, (((1,), (1,)), ((), ())), preferred_element_type=F32)


def whole(array):
    return pl.BlockSpec(array.shape, lambda *at: (0,) * array.ndim)


def iota(shape, dim):
    return lax.broadcasted_iota(jnp.int32, shape, dim)


def triangle(repeat=1):
    shape = (CHUNK, repeat * CHUNK)
    return jnp.where((iota(shape, 1) % CHUNK) <= iota(shape, 0), 1.0, 0.0).astype(BF16)


def selection(shape, shift):
    return jnp.where(iota(shape, 1) == iota(shape, 0) + shift, 1.0, 0.0).astype(BF16)


def moved(rows, piece, cols):
    kept = dot_t(rows, piece).astype(BF16)
    return jnp.dot(kept, cols, preferred_element_type=F32)


def tables_kernel(tokens_ref, gain_ref, step_ref, rate_ref, freq_ref, map_ref, readout_ref,
                  normed_ref, w_re, w_im, c_re, c_im,
                  end_re, end_im, push_ref, read_ref, modes_ref, times_ref):
    chunk = pl.program_id(0)
    blocks = modes_ref.shape[0] // 2
    per_block, entries = rate_ref.shape[0] // blocks, rate_ref.shape[1]

    @pl.when(chunk == 0)
    def _():
        times_ref[...] = jnp.zeros_like(times_ref)
        for b in range(blocks):
            mine = range(per_block * b, per_block * (b + 1))
            modes_ref[b:b + 1, :] = jnp.concatenate([rate_ref[g:g + 1, :] for g in mine], axis=1)
            modes_ref[blocks + b:blocks + b + 1, :] = jnp.concatenate([freq_ref[g:g + 1, :] for g in mine], axis=1)

    for b in range(blocks):
        @pl.when(chunk == b)
        def _(b=b):
            members = map_ref.shape[2]
            for part in range(2):
                sign = 1.0 if part == 0 else -1.0
                pushes, reads = [0.0, 0.0], [0.0, 0.0]
                for j in range(per_block):
                    g = per_block * b + j
                    seat = selection((entries, LANES), entries * j)
                    seat_t = selection((LANES, entries), -entries * j)
                    place = selection((members, LANES), members * g)
                    place_t = selection((LANES, members), -members * g)
                    for k, piece in enumerate(high_low(map_ref[part, g])):
                        kept = jnp.dot(place_t, piece, preferred_element_type=F32).astype(BF16)
                        pushes[k] = pushes[k] + jnp.dot(kept, seat, preferred_element_type=F32)
                    for k, piece in enumerate(high_low(sign * readout_ref[part, g])):
                        reads[k] = reads[k] + moved(seat_t, piece, place)
                for k in range(2):
                    push_ref[b, k * LANES:(k + 1) * LANES, part * LANES:(part + 1) * LANES] = pushes[k].astype(BF16)
                    read_ref[b, part * LANES:(part + 1) * LANES, k * LANES:(k + 1) * LANES] = reads[k].astype(BF16)

    tokens = tokens_ref[...].astype(F32)
    mean = jnp.mean(tokens * tokens, axis=1, keepdims=True)
    normed_ref[...] = (tokens * lax.rsqrt(mean + 1e-06) * gain_ref[...]).astype(BF16)

    lower = triangle()
    steps = jnp.broadcast_to(step_ref[pl.ds(chunk, 1), :], (CHUNK, CHUNK))
    grid = jnp.round(steps * 8192.0) * (1.0 / 8192.0)

    def running(values):
        high, low = high_low(values)
        return dot_t(lower, high) + dot_t(lower, low)

    run = running(grid)
    coarse = jnp.round(run * 8.0) * 0.125
    fine = (run - coarse) + running(steps - grid)
    times_ref[0:1, :] += coarse[CHUNK - 1:]
    times_ref[1:2, :] += fine[CHUNK - 1:]
    elapsed = coarse + fine
    first = iota((CHUNK, LANES), 0) == 0
    for b in range(blocks):
        cols = slice(b * LANES, (b + 1) * LANES)
        rate = modes_ref[b:b + 1, :]
        freq = modes_ref[blocks + b:blocks + b + 1, :]
        cosine, sine = rotation(coarse, fine, split_turns(freq))
        exponent = rate * elapsed
        shrink = jnp.exp(-exponent)
        c_re[:, cols] = shrink * cosine
        c_im[:, cols] = shrink * sine
        end_re[:, cols] = (shrink * cosine)[CHUNK - 8:]
        end_im[:, cols] = (shrink * sine)[CHUNK - 8:]
        grow = jnp.exp(exponent)
        g_re = grow * cosine
        g_im = -(grow * sine)
        d_re = jnp.where(first, 1.0, pltpu.roll(g_re, 1, 0)) - g_re
        d_im = jnp.where(first, 0.0, pltpu.roll(g_im, 1, 0)) - g_im
        scale = 1.0 / (rate * rate + freq * freq)
        l_re, l_im = -rate * scale, -freq * scale
        w_re[:, cols] = d_re * l_re - d_im * l_im
        w_im[:, cols] = d_re * l_im + d_im * l_re


def tables(tokens, gain, step, rate, freq, input_map, readout):
    width = rate.size
    blocks = width // LANES
    chunks = step.shape[0]
    rows = chunks * CHUNK
    part = pl.BlockSpec((tokens.shape[0] // chunks, tokens.shape[1]), lambda c: (c, 0))
    block = pl.BlockSpec((CHUNK, width), lambda c: (c, 0))
    big = jax.ShapeDtypeStruct((rows, width), F32)
    end = jax.ShapeDtypeStruct((8 * chunks, width), F32)
    last = pl.BlockSpec((8, width), lambda c: (c, 0))
    matrix = jax.ShapeDtypeStruct((blocks, 2 * LANES, 2 * LANES), BF16)
    modes = jax.ShapeDtypeStruct((2 * blocks, LANES), F32)
    times = jax.ShapeDtypeStruct((8, LANES), F32)
    small = [matrix, matrix, modes, times]
    return pl.pallas_call(
        tables_kernel, grid=(chunks,),
        in_specs=[part, whole(gain)] + [whole(x) for x in (step, rate, freq, input_map, readout)],
        out_specs=[part] + [block] * 4 + [last] * 2 + [whole(x) for x in small], out_shape=[jax.ShapeDtypeStruct(tokens.shape, BF16)] + [big] * 4 + [end] * 2 + small, name="tables",
        cost_estimate=pl.CostEstimate(flops=rows * width * 60, transcendentals=0, bytes_accessed=rows * width * 16),
    )(tokens, gain, step, rate, freq, input_map, readout)


def project_kernel(at_ref, rows_ref, *refs):
    *projs, out_ref = refs
    ways = len(projs)
    width = projs[0].shape[1]
    rows = rows_ref[...]
    for back in range(0, ways, 2):
        pair = jnp.concatenate([projs[back][...], projs[back + 1][...]], axis=1)
        both = jnp.dot(rows, pair, preferred_element_type=F32).astype(BF16)
        for k in range(2):
            out_ref[(at_ref[0] - back - k + ways) % ways] = both[:, k * width:(k + 1) * width]


def project(at, rows, projs, tile=256):
    width = projs[0].shape[1]
    out = jax.ShapeDtypeStruct((len(projs), rows.shape[0], width), BF16)
    return pl.pallas_call(
        project_kernel,
        grid_spec=pltpu.PrefetchScalarGridSpec(
            num_scalar_prefetch=1, grid=(rows.shape[0] // tile,),
            in_specs=[pl.BlockSpec((tile, rows.shape[1]), lambda k, at: (k, 0))]
            + [whole(x) for x in projs],
            out_specs=pl.BlockSpec((len(projs), tile, width), lambda k, at: (0, k, 0))),
        out_shape=out, name="project",
        cost_estimate=pl.CostEstimate(flops=2 * rows.size * len(projs) * width, transcendentals=0,
                                      bytes_accessed=4 * rows.size),
    )(at, rows, *projs)


def ends_kernel(drive_ref, w_re, w_im, c_re, c_im, push_ref, times_ref, stacked, sent_ref, carry):
    chunk = pl.program_id(0)
    blocks = push_ref.shape[0]

    @pl.when(chunk == 0)
    def _():
        carry[...] = jnp.zeros_like(carry)

    drive = drive_ref[...]
    twice = jnp.concatenate([drive, drive], axis=1)
    for b in range(blocks):
        cols = slice(b * LANES, (b + 1) * LANES)
        pushed = jnp.dot(twice, push_ref[b], preferred_element_type=F32)
        er, ei = carry[b:b + 1, :], carry[blocks + b:blocks + b + 1, :]
        for k in range(TILE // CHUNK):
            rows = slice(k * CHUNK, (k + 1) * CHUNK)
            p_re, p_im = pushed[rows, :LANES], pushed[rows, LANES:]
            wr, wi = w_re[rows, cols], w_im[rows, cols]
            x_re = wr * p_re - wi * p_im
            x_im = wr * p_im + wi * p_re
            stacked[k, b, :CHUNK, :LANES], stacked[k, b, CHUNK:, :LANES] = high_low(x_re)
            stacked[k, b, :CHUNK, LANES:], stacked[k, b, CHUNK:, LANES:] = high_low(x_im)
            last = 8 * k + 7
            cr, ci = c_re[last:last + 1, cols], c_im[last:last + 1, cols]
            tr = jnp.sum(x_re, axis=0, keepdims=True) + er
            ti = jnp.sum(x_im, axis=0, keepdims=True) + ei
            er, ei = cr * tr - ci * ti, cr * ti + ci * tr
        carry[b:b + 1, :] = er
        carry[blocks + b:blocks + b + 1, :] = ei

    @pl.when(chunk == pl.num_programs(0) - 1)
    def _():
        message = jnp.concatenate([carry[...], times_ref[...]], axis=0)
        for k in range(sent_ref.shape[0]):
            sent_ref[k] = message


def ends(drive, w_re, w_im, d_re, d_im, push, times, peers):
    rows, width = w_re.shape
    blocks = width // LANES
    chunks = TILE // CHUNK
    block = pl.BlockSpec((TILE, width), lambda c: (c, 0))
    last = pl.BlockSpec((8 * chunks, width), lambda c: (c, 0))
    stacked = jax.ShapeDtypeStruct((rows // CHUNK, blocks, 2 * CHUNK, 2 * LANES), BF16)
    sent = jax.ShapeDtypeStruct((peers, 2 * blocks + 8, LANES), F32)
    return pl.pallas_call(
        ends_kernel, grid=(rows // TILE,),
        in_specs=[pl.BlockSpec((TILE, drive.shape[1]), lambda c: (c, 0)), block, block, last, last,
                  whole(push), whole(times)],
        out_specs=[pl.BlockSpec((chunks, *stacked.shape[1:]), lambda c: (c, 0, 0, 0)), whole(sent)],
        scratch_shapes=[pltpu.VMEM((2 * blocks, LANES), F32)],
        out_shape=[stacked, sent], name="ends",
        cost_estimate=pl.CostEstimate(flops=rows * width * 500, transcendentals=0, bytes_accessed=rows * width * 16),
    )(drive, w_re, w_im, d_re, d_im, push, times)


def read_states(high, low, read):
    total = jnp.dot(high, read, preferred_element_type=F32)
    return total[:, :LANES] + total[:, LANES:] + jnp.dot(low, read[:, :LANES], preferred_element_type=F32)


def local_kernel(stacked, c_re, c_im, read_ref, out_ref, high, low, carry):
    blocks = read_ref.shape[0]

    @pl.when(pl.program_id(0) == 0)
    def _():
        carry[...] = jnp.zeros_like(carry)

    lower = triangle(2)
    for b in range(blocks):
        cols = slice(b * LANES, (b + 1) * LANES)
        er, ei = carry[b:b + 1, :], carry[blocks + b:blocks + b + 1, :]
        for k in range(TILE // CHUNK):
            rows = slice(k * CHUNK, (k + 1) * CHUNK)
            acc = jnp.dot(lower, stacked[k, b], preferred_element_type=F32)
            tr, ti = acc[:, :LANES] + er, acc[:, LANES:] + ei
            cr, ci = c_re[rows, cols], c_im[rows, cols]
            sr = cr * tr - ci * ti
            si = cr * ti + ci * tr
            er, ei = sr[CHUNK - 1:], si[CHUNK - 1:]
            high[b, rows, :LANES], low[b, rows, :LANES] = high_low(sr)
            high[b, rows, LANES:], low[b, rows, LANES:] = high_low(si)
        carry[b:b + 1, :] = er
        carry[blocks + b:blocks + b + 1, :] = ei
    value = jnp.zeros((TILE, LANES), F32)
    for b in range(blocks):
        value = value + read_states(high[b], low[b], read_ref[b])
    out_ref[...] = value


def scratches(blocks):
    store = pltpu.VMEM((blocks, TILE, 2 * LANES), BF16)
    return [store, store, pltpu.VMEM((2 * blocks, LANES), F32)]


def local(stacked, c_re, c_im, read):
    rows, width = c_re.shape
    block = pl.BlockSpec((TILE, width), lambda c: (c, 0))
    return pl.pallas_call(
        local_kernel, grid=(rows // TILE,),
        in_specs=[pl.BlockSpec((TILE // CHUNK, *stacked.shape[1:]), lambda c: (c, 0, 0, 0)), block, block, whole(read)],
        out_specs=pl.BlockSpec((TILE, LANES), lambda c: (c, 0)),
        scratch_shapes=scratches(width // LANES),
        out_shape=jax.ShapeDtypeStruct((rows, LANES), F32), name="local",
        cost_estimate=pl.CostEstimate(flops=rows * width * 1500, transcendentals=0, bytes_accessed=rows * width * 16),
    )(stacked, c_re, c_im, read)


def compose_kernel(at_ref, heard_ref, modes_ref, _, out_ref):
    blocks = modes_ref.shape[0] // 2
    rate = modes_ref[:blocks]
    turns = split_turns(modes_ref[blocks:])
    dr, di = jnp.ones(rate.shape, F32), jnp.zeros(rate.shape, F32)
    er, ei = jnp.zeros(rate.shape, F32), jnp.zeros(rate.shape, F32)
    near = (er, ei, dr, di)
    for k in range(heard_ref.shape[0]):
        near = [jnp.where(at_ref[1] == k, new, old) for new, old in zip((er, ei, dr, di), near)]
        whole_time = heard_ref[k, 2 * blocks:2 * blocks + 1, :]
        coarse = jnp.round(whole_time)
        fine = (whole_time - coarse) + heard_ref[k, 2 * blocks + 1:2 * blocks + 2, :]
        xr, xi = decayed(coarse, fine, rate, turns)
        er, ei = (xr * er - xi * ei + heard_ref[k, :blocks], xr * ei + xi * er + heard_ref[k, blocks:2 * blocks])
        dr, di = xr * dr - xi * di, xr * di + xi * dr
    for j, value in enumerate(near):
        out_ref[j * blocks:(j + 1) * blocks] = value
    for j, value in enumerate((er, ei, dr, di)):
        out_ref[(4 + j) * blocks:(5 + j) * blocks] = value


def compose(at, heard, modes, after):
    out = jax.ShapeDtypeStruct((4 * modes.shape[0], LANES), F32)
    return pl.pallas_call(
        compose_kernel,
        grid_spec=pltpu.PrefetchScalarGridSpec(
            num_scalar_prefetch=1, grid=(1,), in_specs=[whole(heard), whole(modes), pl.BlockSpec((8, LANES), lambda c, at: (0, 0))],
            out_specs=whole(out)),
        out_shape=out, name="compose",
    )(at, heard, modes, after)


def answer_kernel(near_ref, far_ref, local_ref, c_re, c_im, read_ref, out_ref, high, low, carry):
    blocks = read_ref.shape[0]

    @pl.when(pl.program_id(0) == 0)
    def _():
        er, ei = near_ref[:blocks], near_ref[blocks:2 * blocks]
        dr, di = near_ref[2 * blocks:3 * blocks], near_ref[3 * blocks:4 * blocks]
        fr, fi = far_ref[:blocks], far_ref[blocks:]
        carry[:blocks] = dr * fr - di * fi + er
        carry[blocks:] = dr * fi + di * fr + ei

    for b in range(blocks):
        cols = slice(b * LANES, (b + 1) * LANES)
        er, ei = carry[b:b + 1, :], carry[blocks + b:blocks + b + 1, :]
        for k in range(TILE // CHUNK):
            rows = slice(k * CHUNK, (k + 1) * CHUNK)
            cr, ci = c_re[rows, cols], c_im[rows, cols]
            sr = cr * er - ci * ei
            si = cr * ei + ci * er
            er, ei = sr[CHUNK - 1:], si[CHUNK - 1:]
            high[b, rows, :LANES], low[b, rows, :LANES] = high_low(sr)
            high[b, rows, LANES:], low[b, rows, LANES:] = high_low(si)
        carry[b:b + 1, :] = er
        carry[blocks + b:blocks + b + 1, :] = ei
    value = local_ref[...]
    for b in range(blocks):
        value = value + read_states(high[b], low[b], read_ref[b])
    inner = 0.7978845608 * (value + 0.044715 * (value * value * value))
    out_ref[...] = (0.5 * value * (1.0 + jnp.tanh(inner))).astype(BF16)


def answers(near, far, locals_, c_re, c_im, read):
    rows, width = c_re.shape
    block = pl.BlockSpec((TILE, width), lambda c: (c, 0))
    narrow = pl.BlockSpec((TILE, LANES), lambda c: (c, 0))
    return pl.pallas_call(
        answer_kernel, grid=(rows // TILE,),
        in_specs=[whole(near), whole(far), narrow, block, block, whole(read)],
        out_specs=narrow, scratch_shapes=scratches(width // LANES),
        out_shape=jax.ShapeDtypeStruct((rows, LANES), BF16), name="answers",
        cost_estimate=pl.CostEstimate(flops=rows * width * 1000, transcendentals=0, bytes_accessed=rows * width * 16),
    )(near, far, locals_, c_re, c_im, read)


def ring(count, by):
    return [(k, (k + by) % count) for k in range(count)]


def on_device(
    tokens, step, in_gain, in_proj, decay_rate, frequency, input_map, readout, out_gain, out_proj
):
    ways = lax.axis_size("tp")
    place = lax.axis_index(("zl", "core"))
    at = jnp.stack([lax.axis_index("tp"), place]).astype(jnp.int32)
    projs = [in_proj] + [lax.ppermute(in_proj, "tp", ring(ways, by)) for by in range(1, ways)]
    normed, w_re, w_im, c_re, c_im, d_re, d_im, push, read, modes, times = tables(
        tokens, in_gain.reshape(1, -1), step.reshape(-1, CHUNK), decay_rate, frequency,
        jnp.swapaxes(input_map, 2, 3), readout,
    )
    drive = lax.all_to_all(project(at, normed, projs), "tp", 0, 0, tiled=True)
    peers = lax.axis_size("zl") * lax.axis_size("core")
    stacked, sent = ends(
        drive.reshape(-1, drive.shape[-1]), w_re, w_im, d_re, d_im, push, times, peers
    )
    heard = lax.all_to_all(sent, ("zl", "core"), 0, 0, tiled=True)
    own = local(stacked, c_re, c_im, read)
    near = compose(at, heard, modes, own)
    half = modes.shape[0]
    quarter = half // 2
    er, ei, dr, di = (near[2 * half + k * quarter:2 * half + (k + 1) * quarter] for k in range(4))
    er, ei, dr, di = lax.optimization_barrier((er, ei, dr, di))
    fr = jnp.zeros_like(er)
    fi = jnp.zeros_like(ei)
    for k in range(lax.axis_size("zh") - 1):
        leaves = jnp.concatenate([dr * fr - di * fi + er, dr * fi + di * fr + ei], axis=0)
        comes = lax.ppermute(leaves, "zh", [(k, k + 1)])
        fr, fi = fr + comes[:quarter], fi + comes[quarter:]
    far = jnp.concatenate([fr, fi], axis=0)
    answer = answers(near, far, own, c_re, c_im, read)
    parts = lax.all_to_all(answer.reshape(ways, -1, LANES), "tp", 0, 0, tiled=True)
    values = parts.astype(F32)
    mean = jnp.sum(values * values, axis=(0, 2), keepdims=True) * (1.0 / (ways * LANES))
    shaped = (values * lax.rsqrt(mean + 1e-06) * out_gain.reshape(ways, 1, LANES)).astype(BF16)
    return jnp.einsum(
        "ktc,kcd->td", shaped, out_proj.reshape(ways, LANES, -1), preferred_element_type=F32
    ).astype(BF16)


def solution(mesh):
    shape = mesh.shape
    chips = shape["sp"] // 2
    near = min(BLOCK, chips)
    devices = mesh.devices.reshape(shape["grp"], chips // near, near, 2, shape["tp"])
    fine_mesh = Mesh(devices, ("grp", "zh", "zl", "core", "tp"))
    rows = ("grp", "zh", "zl", "core", "tp")
    placed = (
        P(rows, None),
        P(("grp", "zh", "zl", "core")),
        P(),
        P(None, "tp"),
        P("tp", None),
        P("tp", None),
        P(None, "tp", None, None),
        P(None, "tp", None, None),
        P(),
        P(),
    )
    return jax.shard_map(
        on_device,
        mesh=fine_mesh,
        in_specs=placed,
        out_specs=P(rows, None),
        check_vma=False,
    )
```

time: 141 us -> 121 us (0.86)
  blocking collectives: 74.9 us -> 18.6 us
  starting transfers between devices: 15.8 us -> 60.3 us
  other arithmetic: 6.34 us -> 1.56 us
  Pallas kernels: 38 us -> 34.3 us
  matrix products: 0 us -> 1.74 us
    all_to_all x2 -> x1, blocking collectives: 65.2 us -> 9.66 us  [on_device(): drive = lax.all_to_all(project(at, normed, projs), 'tp', 0, 0, tiled=True)]
    all_to_all x0 -> x1, starting transfers between devices: none -> 42.6 us  [on_device(): heard = lax.all_to_all(sent, ('zl', 'core'), 0, 0, tiled=True)]
    pallas_call x4, Pallas kernels: 30.9 us -> 28.2 us  [the longest x1 12.5 us: tables(): pl.pallas_call(tables_kernel, grid=(chunks,), in_specs=[part, whole(gain)...]
    add x3 -> x7, other arithmetic: 2.28 us -> 0.07 us  [on_device(): dr * fr - di * fi + er]
    ppermute x3 -> x7, starting transfers between devices: 3.4 us -> 5.27 us  [on_device(): comes = lax.ppermute(leaves, 'zh', [(k, k + 1)])]
    dot_general x0 -> x1, matrix products: none -> 1.74 us  [on_device(): jnp.einsum('ktc,kcd->td', shaped, out_proj.reshape(ways, LANES, -1), pref...]
    unnamed x11 -> x10, local copies, waits for them, and re-layouts: 3.08 us -> 1.58 us
  transfers between devices with their start and end apart: 6 -> 11, of which waited for: 1 -> 1; matrix products, arithmetic and copies ran while one was open for 4% -> 1% of each run, Pallas kernels for 7% -> 15%
where the time goes in v3:
time: 121 us; the launch traced here: 120 us
  starting transfers between devices  60.3 us (50%)
  Pallas kernels  34.3 us (28%)
  blocking collectives  18.6 us (15%)
  local copies, waits for them, and re-layouts  2.34 us (2%)
  matrix products  1.74 us (1%)
  other arithmetic  1.56 us (1%)
    all_to_all x1, starting transfers between devices, on_device(): heard = lax.all_to_all(sent, ('zl', 'core'), 0, 0, tiled=True)  42.6 us
    pallas_call x1, Pallas kernels, tables(): pl.pallas_call(tables_kernel, grid=(chunks,), in_specs=[part, whole(gain)...  12.5 us
    ppermute x3, starting transfers between devices, on_device(): lax.ppermute(in_proj, 'tp', ring(ways, by))  12.5 us
    all_to_all x1, blocking collectives, on_device(): drive = lax.all_to_all(project(at, normed, projs), 'tp', 0, 0, tiled=True)  9.66 us
    all_to_all x1, blocking collectives, on_device(): lax.all_to_all(answer.reshape(ways, -1, LANES), 'tp', 0, 0, tiled=True)  8.99 us
    pallas_call x1, Pallas kernels, local(): pl.pallas_call(local_kernel, grid=(rows // TILE,), in_specs=[pl.BlockSpec...  5.78 us
    ppermute x7, starting transfers between devices, on_device(): comes = lax.ppermute(leaves, 'zh', [(k, k + 1)])  5.27 us
    pallas_call x1, Pallas kernels, ends(): pl.pallas_call(ends_kernel, grid=(rows // TILE,), in_specs=[pl.BlockSpec(...  5.17 us
  transfers between devices with their start and end apart: 11, of which 1 were waited for; matrix products, arithmetic and copies ran while one was open for 1% of the time, Pallas kernels for 15%

profile of v3, /device:TPU:33, one launch (start us, length us, event | category | flops | bytes accessed | tf_op | source)
XLA Modules:
  0.0 119.9 jit_solution(3406622973209619361)
XLA Ops:
  0.0 5.9 %collective-permute-start.1 = (bf16[2048,128]{1,0:T(8,128)(2,1)}, bf16[2048,128]{1,0:T(8,128)(2,1)S(1)}, u32[]{:S(2)}, u32[]{:S(2)}) collective-permute-start(bf16[2048,128]{1,0:T(8,128)(2,1)} %refs_0_.1), channel_id=1, source_target_pairs={{0,2},{1,3},{2,0},{3,1},{4,6},{5,7},{6,4},{7,5},{8,10},{9,11},{10,... | collective-permute-start | bytes 1572872 | tf_op jit(solution)/shard_map/ppermute | solution.py:408
  5.9 2.4 %collective-permute-start = (bf16[2048,128]{1,0:T(8,128)(2,1)}, bf16[2048,128]{1,0:T(8,128)(2,1)S(1)}, u32[]{:S(2)}, u32[]{:S(2)}) collective-permute-start(bf16[2048,128]{1,0:T(8,128)(2,1)} %refs_0_.1), channel_id=1, source_target_pairs={{0,1},{1,2},{2,3},{3,0},{4,5},{5,6},{6,7},{7,4},{8,9},{9,10},{10,1... | collective-permute-start | bytes 1572872 | tf_op jit(solution)/shard_map/ppermute | solution.py:408
  8.3 4.2 %collective-permute-start.2 = (bf16[2048,128]{1,0:T(8,128)(2,1)}, bf16[2048,128]{1,0:T(8,128)(2,1)}, u32[]{:S(2)}, u32[]{:S(2)}) collective-permute-start(bf16[2048,128]{1,0:T(8,128)(2,1)} %refs_0_.1), channel_id=1, source_target_pairs={{0,3},{1,0},{2,1},{3,2},{4,7},{5,4},{6,5},{7,6},{8,11},{9,8},{10,9... | collective-permute-start | bytes 1572872 | tf_op jit(solution)/shard_map/ppermute | solution.py:408
  12.5 12.5 %tables.1 = (bf16[256,2048]{1,0:T(8,128)(2,1)}, f32[1024,512]{1,0:T(8,128)}, f32[1024,512]{1,0:T(8,128)}, f32[1024,512]{1,0:T(8,128)}, f32[1024,512]{1,0:T(8,128...) custom-call(bf16[256,2048]{1,0:T(8,128)(2,1)} %tokens_ref.1, ...), custom_call_target="tpu_custom_call" | custom-call | flops 31457280 | bytes 8388608 | tf_op jit(solution)/shard_map/tables/pallas_call | solution.py:178
  25.0 0.7 pad_add_fusion.at_ref
  25.6 0.8 copy-done.1
  26.6 3.9 %project.1 = bf16[4,256,128]{2,1,0:T(8,128)(2,1)} custom-call(s32[2]{0:T(128)} %pad_add_fusion.at_ref, bf16[256,2048]{1,0:T(8,128)(2,1)} %get-tuple-element.22.rows_ref, bf16[2048,128]{1,0:T(8,128)(2,1)} %refs_0_.1, bf16[2048,128]{1,0:T(8,128)(2,1)} %copy-done.2, bf16[2048,128]{1,0:T(8,128)(2,1)} %copy-done.1, bf16[2048,128]{1,0:T(8,128)(2,1)} %collective-permute-done.2.refs_3_), custom_call_target="tpu_custom_call" | custom-call | flops 536870912 | bytes 2097152 | tf_op jit(solution)/shard_map/project/pallas_call | solution.py:201
  30.5 9.7 %all_to_all.15 = bf16[4,256,128]{2,1,0:T(8,128)(2,1)} all-to-all(bf16[4,256,128]{2,1,0:T(8,128)(2,1)} %project.1), channel_id=1, replica_groups=mesh['grp'=2,'zh'=8,'zl'=4,'core'=2,'tp'=4] {'tp'}, dimensions={0} | all-to-all | bytes 524288 | tf_op jit(solution)/shard_map/all_to_all | solution.py:413
  40.2 5.2 %ends.1 = (bf16[8,4,256,256]{3,2,1,0:T(8,128)(2,1)}, f32[8,16,128]{2,1,0:T(8,128)}) custom-call(bf16[1024,128]{1,0:T(8,128)(2,1)} %bitcast.15, f32[1024,512]{1,0:T(8,128)} %get-tuple-element.23.w_re, f32[1024,512]{1,0:T(8,128)} %get-tuple-element.24.w_im, f32[64,512]{1,0:T(8,128)} %get-tuple-element.25.c_re, f32[64,512]{1,0:T(8,128)} %get-tuple-element.26.c_im, ...), custom_call_target="tpu_custom_call" | custom-call | flops 262144000 | bytes 8388608 | tf_op jit(solution)/shard_map/ends/pallas_call | solution.py:259
  45.3 42.6 %all-to-all-start.1 = ((f32[8,16,128]{2,1,0:T(8,128)}), f32[8,16,128]{2,1,0:T(8,128)S(1)}, u32[]{:S(2)}, u32[]{:S(2)}) async-start(f32[8,16,128]{2,1,0:T(8,128)} %get-tuple-element.29), calls=%async_computation.1 | async-start | bytes 131072 | tf_op jit(solution)/shard_map/all_to_all | solution.py:418
  87.9 5.8 %local.1._.local_ref = f32[1024,128]{1,0:T(8,128)} custom-call(bf16[8,4,256,256]{3,2,1,0:T(8,128)(2,1)} %get-tuple-element.31.stacked, f32[1024,512]{1,0:T(8,128)} %get-tuple-element.32.c_re, f32[1024,512]{1,0:T(8,128)} %get-tuple-element.33.c_im, bf16[4,256,256]{2,1,0:T(8,128)(2,1)} %get-tuple-element.34.read_ref), custom_call_target="tpu_custom_call" | custom-call | flops 786432000 | bytes 8388608 | tf_op jit(solution)/shard_map/local/pallas_call | solution.py:312
  94.3 2.2 %compose.1.near_ref = f32[32,128]{1,0:T(8,128)} custom-call(s32[2]{0:T(128)} %pad_add_fusion.at_ref, f32[8,16,128]{2,1,0:T(8,128)} %copy-done.3, f32[8,128]{1,0:T(8,128)} %get-tuple-element.30.modes_ref, f32[1024,128]{1,0:T(8,128)} %local.1._.local_ref), custom_call_target="tpu_custom_call" | custom-call | tf_op jit(solution)/shard_map/compose/pallas_call | solution.py:345
  96.5 0.8 fusion.7
  97.3 1.3 %collective-permute-start.3 = (f32[8,128]{1,0:T(8,128)S(1)}, f32[8,128]{1,0:T(8,128)S(1)}, u32[]{:S(2)}, u32[]{:S(2)}) collective-permute-start(f32[8,128]{1,0:T(8,128)S(1)} %pad_maximum_fusion), channel_id=1, source_target_pairs={{0,32},{1,33},{2,34},{3,35},{4,36},{5,37},{6,38},{7,39},{8,40},{9,... | collective-permute-start | bytes 12296 | tf_op jit(solution)/shard_map/ppermute | solution.py:429
  98.6 0.7 collective-permute-done.3
  99.4 0.7 collective-permute-start.4
  100.1 0.7 collective-permute-start.5
  100.8 0.7 collective-permute-start.6
  101.5 0.7 collective-permute-start.7
  102.3 0.7 collective-permute-start.8
  103.0 0.7 collective-permute-start.9
  104.3 4.8 %answers.1 = bf16[1024,128]{1,0:T(8,128)(2,1)} custom-call(f32[32,128]{1,0:T(8,128)} %compose.1.near_ref, f32[8,128]{1,0:T(8,128)} %pad_maximum_fusion.7.far_ref, f32[1024,128]{1,0:T(8,128)} %local.1._.local_ref, f32[1024,512]{1,0:T(8,128)} %get-tuple-element.32.c_re, f32[1024,512]{1,0:T(8,128)} %get-tuple-element.33.c_im, ...), custom_call_target="tpu_custom_call" | custom-call | flops 524288000 | bytes 8388608 | tf_op jit(solution)/shard_map/answers/pallas_call | solution.py:389
  109.0 9.0 %all_to_all.16 = bf16[4,256,128]{2,1,0:T(8,128)(2,1)S(1)} all-to-all(bf16[4,256,128]{2,1,0:T(8,128)(2,1)} %bitcast.16), channel_id=1, replica_groups=mesh['grp'=2,'zh'=8,'zl'=4,'core'=2,'tp'=4] {'tp'}, dimensions={0} | all-to-all | bytes 524288 | tf_op jit(solution)/shard_map/all_to_all | solution.py:433
  118.2 1.7 %fusion = bf16[256,2048]{1,0:T(8,128)(2,1)} fusion(bf16[4,128,2048]{2,1,0:T(8,128)(2,1)S(1)} %bitcast.14, bf16[4,256,128]{2,1,0:T(8,128)(2,1)S(1)} %all_to_all.16, f32[4,128]{1,0:T(4,128)S(1)} %bitcast.20, f32[256]{0:T(256)S(1)} %add_rsqrt_fusion), kind=kOutput, calls=%fused_computation.1 | convolution fusion | flops 537919488 | bytes 3410944 | tf_op jit(solution)/shard_map/ktc,kcd->td/dot_general | solution.py:437
  (40 shorter events, 1.7 us)
Async XLA Ops:
  0.0 118.2 %copy-start = (bf16[512,2048]{1,0:T(8,128)(2,1)S(1)}, bf16[512,2048]{1,0:T(8,128)(2,1)}, u32[]{:S(2)}) copy-start(bf16[512,2048]{1,0:T(8,128)(2,1)} %param.19) | copy-start | bytes 6291460
  0.0 25.6 %collective-permute-start.1 = (bf16[2048,128]{1,0:T(8,128)(2,1)}, bf16[2048,128]{1,0:T(8,128)(2,1)S(1)}, u32[]{:S(2)}, u32[]{:S(2)}) collective-permute-start(bf16[2048,128]{1,0:T(8,128)(2,1)} %refs_0_.1), channel_id=1, source_target_pairs={{0,2},{1,3},{2,0},{3,1},{4,6},{5,7},{6,4},{7,5},{8,10},{9,11},{10,... | collective-permute-start | bytes 1572872 | tf_op jit(solution)/shard_map/ppermute | solution.py:408
  5.9 19.7 %collective-permute-start = (bf16[2048,128]{1,0:T(8,128)(2,1)}, bf16[2048,128]{1,0:T(8,128)(2,1)S(1)}, u32[]{:S(2)}, u32[]{:S(2)}) collective-permute-start(bf16[2048,128]{1,0:T(8,128)(2,1)} %refs_0_.1), channel_id=1, source_target_pairs={{0,1},{1,2},{2,3},{3,0},{4,5},{5,6},{6,7},{7,4},{8,9},{9,10},{10,1... | collective-permute-start | bytes 1572872 | tf_op jit(solution)/shard_map/ppermute | solution.py:408
  8.3 17.3 %collective-permute-start.2 = (bf16[2048,128]{1,0:T(8,128)(2,1)}, bf16[2048,128]{1,0:T(8,128)(2,1)}, u32[]{:S(2)}, u32[]{:S(2)}) collective-permute-start(bf16[2048,128]{1,0:T(8,128)(2,1)} %refs_0_.1), channel_id=1, source_target_pairs={{0,3},{1,0},{2,1},{3,2},{4,7},{5,4},{6,5},{7,6},{8,11},{9,8},{10,9... | collective-permute-start | bytes 1572872 | tf_op jit(solution)/shard_map/ppermute | solution.py:408
  25.6 0.8 copy-start.1
  25.6 1.0 copy-start.2
  45.3 48.4 %all-to-all-start.1 = ((f32[8,16,128]{2,1,0:T(8,128)}), f32[8,16,128]{2,1,0:T(8,128)S(1)}, u32[]{:S(2)}, u32[]{:S(2)}) async-start(f32[8,16,128]{2,1,0:T(8,128)} %get-tuple-element.29), calls=%async_computation.1 | async-start | bytes 131072 | tf_op jit(solution)/shard_map/all_to_all | solution.py:418
  93.7 0.6 copy-start.3
  97.3 2.0 %collective-permute-start.3 = (f32[8,128]{1,0:T(8,128)S(1)}, f32[8,128]{1,0:T(8,128)S(1)}, u32[]{:S(2)}, u32[]{:S(2)}) collective-permute-start(f32[8,128]{1,0:T(8,128)S(1)} %pad_maximum_fusion), channel_id=1, source_target_pairs={{0,32},{1,33},{2,34},{3,35},{4,36},{5,37},{6,38},{7,39},{8,40},{9,... | collective-permute-start | bytes 12296 | tf_op jit(solution)/shard_map/ppermute | solution.py:429
  99.4 0.7 collective-permute-start.4
  100.1 0.7 collective-permute-start.5
  100.8 0.7 collective-permute-start.6
  101.5 0.7 collective-permute-start.7
  102.3 0.7 collective-permute-start.8
  103.0 0.7 collective-permute-start.9
  104.3 13.9 %copy-start.4 = (f32[512]{0:T(512)S(1)}, f32[512]{0:T(512)}, u32[]{:S(2)}) copy-start(f32[512]{0:T(512)} %param.18) | copy-start | bytes 6148

commit v4 on v3

v4 whole, which is shorter than its diff:
```python
from functools import partial

import jax
import jax.numpy as jnp
from jax import lax
from jax.experimental import pallas as pl
from jax.experimental.pallas import tpu as pltpu
from jax.sharding import Mesh, PartitionSpec as P

CHUNK = 128
TILE = 1024
GRANT = 24 * 1024 * 1024
LANES = 128
BLOCK = 4
F32 = jnp.float32
BF16 = jnp.bfloat16
TWO_PI_HIGH = 6.28125
TWO_PI_LOW = 0.0019353071795864769
INV_TWO_PI = 0.15915494309189535
SIN = (6.2831854820251465, -41.3416862487793, 81.60456085205078, -76.69428253173828,
       41.96574020385742, -14.708574295043945, 3.0096182823181152)
COS = (1.0, -19.739208221435547, 64.9393539428711, -85.45588684082031, 60.23442077636719,
       -26.364990234375, 7.6985273361206055, -1.3503994941711426)


def polynomial(x, factors):
    total = factors[-1] * x + factors[-2]
    for factor in factors[-3::-1]:
        total = total * x + factor
    return total


def split_turns(freq):
    plain = freq * INV_TWO_PI
    high = jnp.round(plain * 8192.0) * (1.0 / 8192.0)
    rest = (freq - high * TWO_PI_HIGH) - high * TWO_PI_LOW
    return high, rest * INV_TWO_PI, plain


def rotation(coarse, fine, turns, again=False):
    high, rest, plain = turns
    whole = coarse * high
    part = (whole - jnp.round(whole)) + (coarse * rest + fine * plain)
    if again:
        part = part - jnp.round(part)
    square = part * part
    return polynomial(square, COS), part * polynomial(square, SIN)


def decayed(coarse, fine, rate, turns):
    cosine, sine = rotation(coarse, fine, turns, again=True)
    magnitude = jnp.exp(-rate * (coarse + fine))
    return magnitude * cosine, magnitude * sine


def high_low(x):
    high = x.astype(BF16)
    return high, (x - high.astype(F32)).astype(BF16)


def dot_t(a, b):
    return lax.dot_general(a, b, (((1,), (1,)), ((), ())), preferred_element_type=F32)


def whole(array):
    return pl.BlockSpec(array.shape, lambda *at: (0,) * array.ndim)


ONCHIP = pl.BlockSpec(memory_space=pltpu.VMEM)


def onchip(x):
    return pltpu.with_memory_space_constraint(x, pltpu.VMEM)


def settings():
    return pltpu.CompilerParams(vmem_limit_bytes=GRANT)


def iota(shape, dim):
    return lax.broadcasted_iota(jnp.int32, shape, dim)


def triangle(repeat=1):
    shape = (CHUNK, repeat * CHUNK)
    return jnp.where((iota(shape, 1) % CHUNK) <= iota(shape, 0), 1.0, 0.0).astype(BF16)


def selection(shape, shift):
    return jnp.where(iota(shape, 1) == iota(shape, 0) + shift, 1.0, 0.0).astype(BF16)


def moved(rows, piece, cols):
    kept = jnp.dot(rows, piece, preferred_element_type=F32).astype(BF16)
    return jnp.dot(kept, cols, preferred_element_type=F32)


def tables_kernel(tokens_ref, gain_ref, step_ref, rate_ref, freq_ref, map_ref, readout_ref,
                  normed_ref, w_re, w_im, c_re, c_im,
                  end_re, end_im, push_ref, read_ref, modes_ref, times_ref, ready):
    chunk = pl.program_id(0)
    blocks = modes_ref.shape[0] // 2
    per_block, entries = rate_ref.shape[0] // blocks, rate_ref.shape[1]

    @pl.when(chunk == 0)
    def _():
        times_ref[...] = jnp.zeros_like(times_ref)
        for b in range(blocks):
            mine = range(per_block * b, per_block * (b + 1))
            modes_ref[b:b + 1, :] = jnp.concatenate([rate_ref[g:g + 1, :] for g in mine], axis=1)
            modes_ref[blocks + b:blocks + b + 1, :] = jnp.concatenate([freq_ref[g:g + 1, :] for g in mine], axis=1)

    block, part = chunk // 2, chunk % 2
    members = map_ref.shape[2]
    sign = (1 - 2 * part).astype(F32)
    pushes, reads = [0.0, 0.0], [0.0, 0.0]
    for j in range(per_block):
        g = per_block * block + j
        seat = selection((entries, LANES), entries * j)
        seat_t = selection((LANES, entries), -entries * j)
        place = selection((members, LANES), members * g)
        place_t = selection((LANES, members), -members * g)
        for k, piece in enumerate(high_low(map_ref[part, g])):
            pushes[k] = pushes[k] + moved(place_t, piece, seat)
        for k, piece in enumerate(high_low(sign * readout_ref[part, g])):
            kept = dot_t(seat_t, piece).astype(BF16)
            reads[k] = reads[k] + jnp.dot(kept, place, preferred_element_type=F32)
    for k in range(2):
        push_ref[block, part, k * LANES:(k + 1) * LANES, :] = pushes[k].astype(BF16)
        read_ref[block, part, :, k * LANES:(k + 1) * LANES] = reads[k].astype(BF16)

    tokens = tokens_ref[...].astype(F32)
    mean = jnp.mean(tokens * tokens, axis=1, keepdims=True)
    share = tokens.shape[0]
    normed_ref[pl.ds(pl.multiple_of(chunk * share, share), share), :] = (tokens * lax.rsqrt(mean + 1e-06) * gain_ref[...]).astype(BF16)

    lower = iota((CHUNK, CHUNK), 1) <= iota((CHUNK, CHUNK), 0)
    ones = jnp.ones((2 * CHUNK, LANES), BF16)

    def running(values):
        kept = [jnp.where(lower, x.astype(F32), 0.0).astype(BF16) for x in high_low(values)]
        return jnp.dot(jnp.concatenate(kept, axis=1), ones, preferred_element_type=F32)

    def timed(which):
        steps = jnp.broadcast_to(step_ref[pl.ds(which, 1), :], (CHUNK, CHUNK))
        grid = jnp.round(steps * 8192.0) * (1.0 / 8192.0)
        run = running(grid)
        coarse = jnp.round(run * 8.0) * 0.125
        return coarse, (run - coarse) + running(steps - grid)

    @pl.when(chunk == 0)
    def _():
        ready[0, 0], ready[0, 1] = timed(0)

    now = pl.ds(pl.multiple_of(chunk * CHUNK, CHUNK), CHUNK)
    end = pl.ds(pl.multiple_of(chunk * 8, 8), 8)
    coarse, fine = ready[chunk % 2, 0], ready[chunk % 2, 1]
    following = timed(jnp.minimum(chunk + 1, pl.num_programs(0) - 1))
    times_ref[0:1, :] += coarse[CHUNK - 1:]
    times_ref[1:2, :] += fine[CHUNK - 1:]
    elapsed = coarse + fine
    first = iota((CHUNK, LANES), 0) == 0
    for b in range(blocks):
        cols = slice(b * LANES, (b + 1) * LANES)
        rate = modes_ref[b:b + 1, :]
        freq = modes_ref[blocks + b:blocks + b + 1, :]
        cosine, sine = rotation(coarse, fine, split_turns(freq))
        exponent = rate * elapsed
        shrink = jnp.exp(-exponent)
        c_re[now, cols] = shrink * cosine
        c_im[now, cols] = shrink * sine
        end_re[end, cols] = (shrink * cosine)[CHUNK - 8:]
        end_im[end, cols] = (shrink * sine)[CHUNK - 8:]
        grow = jnp.exp(exponent)
        g_re = grow * cosine
        g_im = -(grow * sine)
        d_re = jnp.where(first, 1.0, pltpu.roll(g_re, 1, 0)) - g_re
        d_im = jnp.where(first, 0.0, pltpu.roll(g_im, 1, 0)) - g_im
        scale = 1.0 / (rate * rate + freq * freq)
        l_re, l_im = -rate * scale, -freq * scale
        w_re[now, cols] = d_re * l_re - d_im * l_im
        w_im[now, cols] = d_re * l_im + d_im * l_re
    ready[(chunk + 1) % 2, 0], ready[(chunk + 1) % 2, 1] = following


def tables(tokens, gain, step, rate, freq, input_map, readout):
    width = rate.size
    blocks = width // LANES
    chunks = step.shape[0]
    rows = chunks * CHUNK
    part = pl.BlockSpec((tokens.shape[0] // chunks, tokens.shape[1]), lambda c: (c, 0))
    out = [pltpu.VMEM(tokens.shape, BF16)] + [pltpu.VMEM((rows, width), F32)] * 4
    out += [pltpu.VMEM((8 * chunks, width), F32)] * 2
    out += [pltpu.VMEM((blocks, 2, 2 * LANES, LANES), BF16), pltpu.VMEM((blocks, 2, LANES, 2 * LANES), BF16)]
    out += [pltpu.VMEM((2 * blocks, LANES), F32), pltpu.VMEM((8, LANES), F32)]
    return pl.pallas_call(
        tables_kernel, grid=(chunks,),
        in_specs=[part, whole(gain)] + [whole(x) for x in (step, rate, freq, input_map, readout)],
        out_specs=[ONCHIP] * len(out), out_shape=out, name="tables", compiler_params=settings(),
        scratch_shapes=[pltpu.VMEM((2, 2, CHUNK, LANES), F32)],
        cost_estimate=pl.CostEstimate(flops=rows * width * 60, transcendentals=0, bytes_accessed=rows * width * 16),
    )(*(pltpu.with_memory_space_constraint(x, pltpu.HBM) for x in (tokens, gain, step, rate, freq, input_map, readout)))


def project_kernel(at_ref, rows_ref, *refs):
    *projs, out_ref = refs
    ways = len(projs)
    width = projs[0].shape[1]
    rows = rows_ref[...]
    for back in range(0, ways, 2):
        pair = jnp.concatenate([projs[back][...], projs[back + 1][...]], axis=1)
        both = jnp.dot(rows, pair, preferred_element_type=F32).astype(BF16)
        for k in range(2):
            out_ref[(at_ref[0] - back - k + ways) % ways] = both[:, k * width:(k + 1) * width]


def project(at, rows, projs):
    width = projs[0].shape[1]
    return pl.pallas_call(
        project_kernel,
        grid_spec=pltpu.PrefetchScalarGridSpec(
            num_scalar_prefetch=1, grid=(1,), in_specs=[ONCHIP] * (1 + len(projs)), out_specs=ONCHIP),
        out_shape=pltpu.VMEM((len(projs), rows.shape[0], width), BF16), name="project", compiler_params=settings(),
        cost_estimate=pl.CostEstimate(flops=2 * rows.size * len(projs) * width, transcendentals=0,
                                      bytes_accessed=4 * rows.size),
    )(at, onchip(rows), *(onchip(x) for x in projs))


def ends_kernel(drive_ref, w_re, w_im, d_re, d_im, push_ref, times_ref, stacked, sent_ref):
    blocks = push_ref.shape[0]
    tiles = drive_ref.shape[0] // TILE
    ends_re, ends_im = [], []
    for b in range(blocks):
        cols = slice(b * LANES, (b + 1) * LANES)
        push = jnp.concatenate([push_ref[b, 0], push_ref[b, 1]], axis=1)
        er = ei = jnp.zeros((1, LANES), F32)
        for tile in range(tiles):
            drive = drive_ref[tile * TILE:(tile + 1) * TILE, :]
            pushed = jnp.dot(jnp.concatenate([drive, drive], axis=1), push, preferred_element_type=F32)
            for j in range(TILE // CHUNK):
                k = tile * (TILE // CHUNK) + j
                rows = slice(k * CHUNK, (k + 1) * CHUNK)
                part = pushed[j * CHUNK:(j + 1) * CHUNK]
                p_re, p_im = part[:, :LANES], part[:, LANES:]
                wr, wi = w_re[rows, cols], w_im[rows, cols]
                x_re = wr * p_re - wi * p_im
                x_im = wr * p_im + wi * p_re
                stacked[k, b, :CHUNK, :LANES], stacked[k, b, CHUNK:, :LANES] = high_low(x_re)
                stacked[k, b, :CHUNK, LANES:], stacked[k, b, CHUNK:, LANES:] = high_low(x_im)
                last = 8 * k + 7
                cr, ci = d_re[last:last + 1, cols], d_im[last:last + 1, cols]
                tr = jnp.sum(x_re, axis=0, keepdims=True) + er
                ti = jnp.sum(x_im, axis=0, keepdims=True) + ei
                er, ei = cr * tr - ci * ti, cr * ti + ci * tr
        ends_re.append(er)
        ends_im.append(ei)
    message = jnp.concatenate(ends_re + ends_im + [times_ref[...]], axis=0)
    for k in range(sent_ref.shape[0]):
        sent_ref[k] = message


def ends(drive, w_re, w_im, d_re, d_im, push, times, peers):
    rows, width = w_re.shape
    blocks = width // LANES
    return pl.pallas_call(
        ends_kernel, in_specs=[ONCHIP] * 7, out_specs=[ONCHIP] * 2, compiler_params=settings(),
        out_shape=[pltpu.VMEM((rows // CHUNK, blocks, 2 * CHUNK, 2 * LANES), BF16),
                   pltpu.VMEM((peers, 2 * blocks + 8, LANES), F32)], name="ends",
        cost_estimate=pl.CostEstimate(flops=rows * width * 500, transcendentals=0, bytes_accessed=rows * width * 16),
    )(*(onchip(x) for x in (drive, w_re, w_im, d_re, d_im, push, times)))


def read_states(high, low, read):
    total = jnp.dot(high, read, preferred_element_type=F32)
    return total[:, :LANES] + total[:, LANES:] + jnp.dot(low, read[:, :LANES], preferred_element_type=F32)


def read_of(read_ref, b):
    return jnp.concatenate([read_ref[b, 0], read_ref[b, 1]], axis=0)


def local_kernel(stacked, c_re, c_im, read_ref, _, out_ref, high, low):
    blocks = read_ref.shape[0]
    lower = triangle(2)
    carry = [jnp.zeros((1, LANES), F32)] * (2 * blocks)
    for tile in range(c_re.shape[0] // TILE):
        value = jnp.zeros((TILE, LANES), F32)
        for b in range(blocks):
            cols = slice(b * LANES, (b + 1) * LANES)
            er, ei = carry[2 * b:2 * b + 2]
            for j in range(TILE // CHUNK):
                k = tile * (TILE // CHUNK) + j
                rows = slice(k * CHUNK, (k + 1) * CHUNK)
                here = slice(j * CHUNK, (j + 1) * CHUNK)
                acc = jnp.dot(lower, stacked[k, b], preferred_element_type=F32)
                tr, ti = acc[:, :LANES] + er, acc[:, LANES:] + ei
                cr, ci = c_re[rows, cols], c_im[rows, cols]
                sr = cr * tr - ci * ti
                si = cr * ti + ci * tr
                er, ei = sr[CHUNK - 1:], si[CHUNK - 1:]
                high[b, here, :LANES], low[b, here, :LANES] = high_low(sr)
                high[b, here, LANES:], low[b, here, LANES:] = high_low(si)
            carry[2 * b], carry[2 * b + 1] = er, ei
        for b in range(blocks):
            value = value + read_states(high[b], low[b], read_of(read_ref, b))
        out_ref[tile * TILE:(tile + 1) * TILE, :] = value


def scratches(blocks):
    store = pltpu.VMEM((blocks, TILE, 2 * LANES), BF16)
    return [store, store]


def local(stacked, c_re, c_im, read, after):
    rows, width = c_re.shape
    return pl.pallas_call(
        local_kernel, in_specs=[ONCHIP] * 5, out_specs=ONCHIP, scratch_shapes=scratches(width // LANES),
        out_shape=pltpu.VMEM((rows, LANES), F32), name="local", compiler_params=settings(),
        cost_estimate=pl.CostEstimate(flops=rows * width * 1500, transcendentals=0, bytes_accessed=rows * width * 16),
    )(*(onchip(x) for x in (stacked, c_re, c_im, read, after)))


def compose_kernel(at_ref, heard_ref, modes_ref, out_ref, end_ref, decay_ref):
    blocks = modes_ref.shape[0] // 2
    rate = modes_ref[:blocks]
    turns = split_turns(modes_ref[blocks:])
    dr, di = jnp.ones(rate.shape, F32), jnp.zeros(rate.shape, F32)
    er, ei = jnp.zeros(rate.shape, F32), jnp.zeros(rate.shape, F32)
    near = (er, ei, dr, di)
    for k in range(heard_ref.shape[0]):
        near = [jnp.where(at_ref[0] == k, new, old) for new, old in zip((er, ei, dr, di), near)]
        whole_time = heard_ref[k, 2 * blocks:2 * blocks + 1, :]
        coarse = jnp.round(whole_time)
        fine = (whole_time - coarse) + heard_ref[k, 2 * blocks + 1:2 * blocks + 2, :]
        xr, xi = decayed(coarse, fine, rate, turns)
        er, ei = (xr * er - xi * ei + heard_ref[k, :blocks], xr * ei + xi * er + heard_ref[k, blocks:2 * blocks])
        dr, di = xr * dr - xi * di, xr * di + xi * dr
    for j, value in enumerate(near):
        out_ref[j * blocks:(j + 1) * blocks] = value
    end_ref[:blocks], end_ref[blocks:] = er, ei
    decay_ref[:blocks], decay_ref[blocks:] = dr, di


def compose(at, heard, modes):
    one = pltpu.VMEM(modes.shape, F32)
    return pl.pallas_call(
        compose_kernel,
        grid_spec=pltpu.PrefetchScalarGridSpec(
            num_scalar_prefetch=1, grid=(1,), in_specs=[ONCHIP] * 2, out_specs=[ONCHIP] * 3),
        out_shape=[pltpu.VMEM((2 * modes.shape[0], LANES), F32), one, one], name="compose",
        compiler_params=settings(),
    )(at, *(onchip(x) for x in (heard, modes)))


def link_kernel(far_ref, comes_ref, end_ref, decay_ref, next_ref, leaves_ref):
    blocks = far_ref.shape[0] // 2
    far = far_ref[...] + comes_ref[...]
    fr, fi = far[:blocks], far[blocks:]
    dr, di = decay_ref[:blocks], decay_ref[blocks:]
    next_ref[...] = far
    leaves_ref[...] = end_ref[...] + jnp.concatenate([dr * fr - di * fi, dr * fi + di * fr], axis=0)


def link(far, comes, end, decay):
    out = pltpu.VMEM(far.shape, F32)
    return pl.pallas_call(
        link_kernel, in_specs=[ONCHIP] * 4, out_specs=[ONCHIP] * 2, out_shape=[out, out], name="link",
        compiler_params=settings(),
    )(*(onchip(x) for x in (far, comes, end, decay)))


def answer_kernel(near_ref, far_ref, local_ref, c_re, c_im, d_re, d_im, read_ref, out_ref, high, low):
    blocks = read_ref.shape[0]
    er, ei = near_ref[:blocks], near_ref[blocks:2 * blocks]
    dr, di = near_ref[2 * blocks:3 * blocks], near_ref[3 * blocks:4 * blocks]
    fr, fi = far_ref[:blocks], far_ref[blocks:]
    start_re = dr * fr - di * fi + er
    start_im = dr * fi + di * fr + ei
    carry = [x[b:b + 1] for b in range(blocks) for x in (start_re, start_im)]
    for tile in range(c_re.shape[0] // TILE):
        for b in range(blocks):
            cols = slice(b * LANES, (b + 1) * LANES)
            er, ei = carry[2 * b:2 * b + 2]
            for j in range(TILE // CHUNK):
                k = tile * (TILE // CHUNK) + j
                rows = slice(k * CHUNK, (k + 1) * CHUNK)
                here = slice(j * CHUNK, (j + 1) * CHUNK)
                cr, ci = c_re[rows, cols], c_im[rows, cols]
                sr = cr * er - ci * ei
                si = cr * ei + ci * er
                high[b, here, :LANES], low[b, here, :LANES] = high_low(sr)
                high[b, here, LANES:], low[b, here, LANES:] = high_low(si)
                last = 8 * k + 7
                cr, ci = d_re[last:last + 1, cols], d_im[last:last + 1, cols]
                er, ei = cr * er - ci * ei, cr * ei + ci * er
            carry[2 * b], carry[2 * b + 1] = er, ei
        value = local_ref[tile * TILE:(tile + 1) * TILE, :]
        for b in range(blocks):
            value = value + read_states(high[b], low[b], read_of(read_ref, b))
        inner = 0.7978845608 * (value + 0.044715 * (value * value * value))
        out_ref[tile * TILE:(tile + 1) * TILE, :] = (0.5 * value * (1.0 + jnp.tanh(inner))).astype(BF16)


def answers(near, far, own, c_re, c_im, d_re, d_im, read):
    rows, width = c_re.shape
    return pl.pallas_call(
        answer_kernel, in_specs=[ONCHIP] * 8, out_specs=ONCHIP, scratch_shapes=scratches(width // LANES),
        out_shape=pltpu.VMEM((rows, LANES), BF16), name="answers", compiler_params=settings(),
        cost_estimate=pl.CostEstimate(flops=rows * width * 1000, transcendentals=0, bytes_accessed=rows * width * 16),
    )(*(onchip(x) for x in (near, far, own, c_re, c_im, d_re, d_im, read)))


def ring(count, by):
    return [(k, (k + by) % count) for k in range(count)]


def on_device(
    tokens, step, in_gain, in_proj, decay_rate, frequency, input_map, readout, out_gain, out_proj
):
    ways = lax.axis_size("tp")
    way = lax.axis_index("tp").astype(jnp.int32).reshape(1)
    place = lax.axis_index(("zl", "core")).astype(jnp.int32).reshape(1)
    step, way, place = lax.optimization_barrier((step, way, place))
    projs = [in_proj] + [lax.ppermute(in_proj, "tp", ring(ways, by)) for by in range(1, ways)]
    normed, w_re, w_im, c_re, c_im, d_re, d_im, push, read, modes, times = tables(
        tokens, in_gain.reshape(1, -1), step.reshape(-1, CHUNK), decay_rate, frequency,
        jnp.swapaxes(input_map, 2, 3), readout,
    )
    drive = lax.all_to_all(project(way, normed, projs), "tp", 0, 0, tiled=True)
    peers = lax.axis_size("zl") * lax.axis_size("core")
    stacked, sent = ends(
        drive.reshape(-1, drive.shape[-1]), w_re, w_im, d_re, d_im, push, times, peers
    )
    heard = lax.all_to_all(sent, ("zl", "core"), 0, 0, tiled=True)
    own = local(stacked, c_re, c_im, read, heard)
    near, end, decay = compose(place, heard, modes)
    far, leaves = jnp.zeros_like(end), end
    for k in range(lax.axis_size("zh") - 1):
        comes = lax.ppermute(leaves, "zh", [(k, k + 1)])
        far, leaves = link(far, comes, end, decay)
    answer = answers(near, far, own, c_re, c_im, d_re, d_im, read)
    parts = lax.all_to_all(answer.reshape(ways, -1, LANES), "tp", 0, 0, tiled=True)
    values = parts.astype(F32)
    mean = jnp.sum(values * values, axis=(0, 2), keepdims=True) * (1.0 / (ways * LANES))
    shaped = (values * lax.rsqrt(mean + 1e-06) * out_gain.reshape(ways, 1, LANES)).astype(BF16)
    return jnp.einsum(
        "ktc,kcd->td", shaped, out_proj.reshape(ways, LANES, -1), preferred_element_type=F32
    ).astype(BF16)


def solution(mesh):
    shape = mesh.shape
    chips = shape["sp"] // 2
    near = min(BLOCK, chips)
    devices = mesh.devices.reshape(shape["grp"], chips // near, near, 2, shape["tp"])
    fine_mesh = Mesh(devices, ("grp", "zh", "zl", "core", "tp"))
    rows = ("grp", "zh", "zl", "core", "tp")
    placed = (
        P(rows, None),
        P(("grp", "zh", "zl", "core")),
        P(),
        P(None, "tp"),
        P("tp", None),
        P("tp", None),
        P(None, "tp", None, None),
        P(None, "tp", None, None),
        P(),
        P(),
    )
    return jax.shard_map(
        on_device,
        mesh=fine_mesh,
        in_specs=placed,
        out_specs=P(rows, None),
        check_vma=False,
    )
```

time: 121 us -> 107 us (0.88)
  blocking collectives: 18.6 us -> 63.6 us
  starting transfers between devices: 60.3 us -> 17.1 us
  Pallas kernels: 34.3 us -> 18.8 us
  waiting for transfers between devices: 0.76 us -> 3.42 us
  other arithmetic: 1.56 us -> 0.14 us
  local copies, waits for them, and re-layouts: 2.34 us -> 1.05 us
    all_to_all x1 -> x2, blocking collectives: 9.66 us -> 55.6 us  [the longest x1 47.7 us: on_device(): heard = lax.all_to_all(sent, ('zl', 'core'), 0, 0, tiled=True)]
    all_to_all x1 -> x0, starting transfers between devices: 42.6 us -> none  [on_device(): heard = lax.all_to_all(sent, ('zl', 'core'), 0, 0, tiled=True)]
    pallas_call x3 -> x10, Pallas kernels: 15.7 us -> 6.61 us  [the longest x1 2.24 us: local(): pl.pallas_call(local_kernel, in_specs=[ONCHIP] * 5, out_specs=ONCHIP, scr...]
    ppermute x3, waiting for transfers between devices: 0.01 us -> 2.67 us  [on_device(): lax.ppermute(in_proj, 'tp', ring(ways, by))]
    pallas_call x1, Pallas kernels: 3.92 us -> 1.77 us  [project(): pl.pallas_call(project_kernel, grid_spec=pltpu.PrefetchScalarGridSpec(num...]
    pallas_call x1, Pallas kernels: 2.19 us -> 0.09 us  [compose(): pl.pallas_call(compose_kernel, grid_spec=pltpu.PrefetchScalarGridSpec(num...]
    pallas_call x1, Pallas kernels: 12.5 us -> 10.4 us  [tables(): pl.pallas_call(tables_kernel, grid=(chunks,), in_specs=[part, whole(gain)...]
  transfers between devices with their start and end apart: 11 -> 10, of which waited for: 1 -> 2; matrix products, arithmetic and copies ran while one was open for 1% -> 0% of each run, Pallas kernels for 15% -> 12%
where the time goes in v4:
time: 107 us; the launch traced here: 106 us
  blocking collectives  63.6 us (59%)
  Pallas kernels  18.8 us (18%)
  starting transfers between devices  17.1 us (16%)
  waiting for transfers between devices  3.42 us (3%)
  matrix products  1.74 us (2%)
    all_to_all x1, blocking collectives, on_device(): heard = lax.all_to_all(sent, ('zl', 'core'), 0, 0, tiled=True)  47.7 us
    ppermute x3, starting transfers between devices, on_device(): lax.ppermute(in_proj, 'tp', ring(ways, by))  11.8 us
    pallas_call x1, Pallas kernels, tables(): pl.pallas_call(tables_kernel, grid=(chunks,), in_specs=[part, whole(gain)...  10.4 us
    all_to_all x1, blocking collectives, on_device(): drive = lax.all_to_all(project(way, normed, projs), 'tp', 0, 0, tiled=True)  7.95 us
    all_to_all x1, blocking collectives, on_device(): lax.all_to_all(answer.reshape(ways, -1, LANES), 'tp', 0, 0, tiled=True)  7.95 us
    ppermute x7, starting transfers between devices, on_device(): comes = lax.ppermute(leaves, 'zh', [(k, k + 1)])  5.27 us
    ppermute x3, waiting for transfers between devices, on_device(): lax.ppermute(in_proj, 'tp', ring(ways, by))  2.67 us
    pallas_call x1, Pallas kernels, local(): pl.pallas_call(local_kernel, in_specs=[ONCHIP] * 5, out_specs=ONCHIP, scr...  2.24 us
  transfers between devices with their start and end apart: 10, of which 2 were waited for; matrix products, arithmetic and copies ran while one was open for 0% of the time, Pallas kernels for 12%

profile of v4, /device:TPU:33, one launch (start us, length us, event | category | flops | bytes accessed | tf_op | source)
XLA Modules:
  0.0 106.1 jit_solution(876528803519465542)
XLA Ops:
  0.0 4.2 %collective-permute-start = (bf16[2048,128]{1,0:T(8,128)(2,1)}, bf16[2048,128]{1,0:T(8,128)(2,1)S(1)}, u32[]{:S(2)}, u32[]{:S(2)}) collective-permute-start(bf16[2048,128]{1,0:T(8,128)(2,1)} %refs_0_.1), channel_id=1, source_target_pairs={{0,1},{1,2},{2,3},{3,0},{4,5},{5,6},{6,7},{7,4},{8,9},{9,10},{10,1... | collective-permute-start | bytes 1572872 | tf_op jit(solution)/shard_map/ppermute | solution.py:424
  4.2 4.7 %collective-permute-start.1 = (bf16[2048,128]{1,0:T(8,128)(2,1)}, bf16[2048,128]{1,0:T(8,128)(2,1)S(1)}, u32[]{:S(2)}, u32[]{:S(2)}) collective-permute-start(bf16[2048,128]{1,0:T(8,128)(2,1)} %refs_0_.1), channel_id=1, source_target_pairs={{0,2},{1,3},{2,0},{3,1},{4,6},{5,7},{6,4},{7,5},{8,10},{9,11},{10,... | collective-permute-start | bytes 1572872 | tf_op jit(solution)/shard_map/ppermute | solution.py:424
  8.9 3.0 %collective-permute-start.2 = (bf16[2048,128]{1,0:T(8,128)(2,1)}, bf16[2048,128]{1,0:T(8,128)(2,1)}, u32[]{:S(2)}, u32[]{:S(2)}) collective-permute-start(bf16[2048,128]{1,0:T(8,128)(2,1)} %refs_0_.1), channel_id=1, source_target_pairs={{0,3},{1,0},{2,1},{3,2},{4,7},{5,4},{6,5},{7,6},{8,11},{9,8},{10,9... | collective-permute-start | bytes 1572872 | tf_op jit(solution)/shard_map/ppermute | solution.py:424
  11.9 10.4 %tables.1 = (bf16[256,2048]{1,0:T(8,128)(2,1)S(1)}, f32[1024,512]{1,0:T(8,128)S(1)}, f32[1024,512]{1,0:T(8,128)S(1)}, f32[1024,512]{1,0:T(8,128)S(1)}, f32[1024,...) custom-call(bf16[256,2048]{1,0:T(8,128)(2,1)} %tokens_ref.1, ...), custom_call_target="tpu_custom_call" | custom-call | flops 31457280 | bytes 8388608 | tf_op jit(solution)/shard_map/tables/pallas_call | solution.py:196
  22.3 2.7 %collective-permute-done.1.refs_2_ = bf16[2048,128]{1,0:T(8,128)(2,1)S(1)} collective-permute-done((bf16[2048,128]{1,0:T(8,128)(2,1)}, bf16[2048,128]{1,0:T(8,128)(2,1)S(1)}, u32[]{:S(2)}, u32[]{:S(2)}) %collective-permute-start.1) | collective-permute-done | bytes 524320 | tf_op jit(solution)/shard_map/ppermute | solution.py:424
  25.0 1.0 copy-done.1
  26.0 1.8 %project.1 = bf16[4,256,128]{2,1,0:T(8,128)(2,1)S(1)} custom-call(s32[1]{0:T(128)} %bitcast.at_ref, bf16[256,2048]{1,0:T(8,128)(2,1)S(1)} %get-tuple-element.40.rows_ref, bf16[2048,128]{1,0:T(8,128)(2,1)S(1)} %copy-done.1, bf16[2048,128]{1,0:T(8,128)(2,1)S(1)} %collective-permute-done.refs_1_, bf16[2048,128]{1,0:T(8,128)(2,1)S(1)} %collective-permute-done.1.refs_2_, ...), custom_call_target="tpu_custom_call" | custom-call | flops 536870912 | bytes 2097152 | tf_op jit(solution)/shard_map/project/pallas_call | solution.py:219
  27.8 7.9 %all_to_all.15 = bf16[4,256,128]{2,1,0:T(8,128)(2,1)S(1)} all-to-all(bf16[4,256,128]{2,1,0:T(8,128)(2,1)S(1)} %project.1), channel_id=1, replica_groups=mesh['grp'=2,'zh'=8,'zl'=4,'core'=2,'tp'=4] {'tp'}, dimensions={0} | all-to-all | bytes 524288 | tf_op jit(solution)/shard_map/all_to_all | solution.py:429
  35.7 1.7 %ends.1 = (bf16[8,4,256,256]{3,2,1,0:T(8,128)(2,1)S(1)}, f32[8,16,128]{2,1,0:T(8,128)S(1)}) custom-call(bf16[1024,128]{1,0:T(8,128)(2,1)S(1)} %bitcast.16, f32[1024,512]{1,0:T(8,128)S(1)} %get-tuple-element.41.w_re, f32[1024,512]{1,0:T(8,128)S(1)} %get-tuple-element.42.w_im, f32[64,512]{1,0:T(8,128)S(1)} %get-tuple-element.43.d_re, ...), custom_call_target="tpu_custom_call" | custom-call | flops 262144000 | bytes 8388608 | tf_op jit(solution)/shard_map/ends/pallas_call | solution.py:265
  37.4 47.7 %all_to_all.16.heard_ref._ = f32[8,16,128]{2,1,0:T(8,128)S(1)} all-to-all(f32[8,16,128]{2,1,0:T(8,128)S(1)} %get-tuple-element.47), channel_id=1, replica_groups=mesh['grp'=2,'zh'=8,'zl'=4,'core'=2,'tp'=4] {'zl','core'}, dimensions={0} | all-to-all | bytes 131072 | tf_op jit(solution)/shard_map/all_to_all | solution.py:434
  85.2 1.3 %collective-permute-start.3 = (f32[8,128]{1,0:T(8,128)S(1)}, f32[8,128]{1,0:T(8,128)S(1)}, u32[]{:S(2)}, u32[]{:S(2)}) collective-permute-start(f32[8,128]{1,0:T(8,128)S(1)} %get-tuple-element.50.end_ref), channel_id=1, source_target_pairs={{0,32},{1,33},{2,34},{3,35},{4,36},{5,37},{6,38},{7,39},{8,40},{9,... | collective-permute-start | bytes 12296 | tf_op jit(solution)/shard_map/ppermute | solution.py:439
  86.5 0.7 collective-permute-done.3.comes_ref
  87.2 0.7 collective-permute-start.4
  87.9 0.7 collective-permute-start.5
  88.6 0.7 collective-permute-start.6
  89.3 0.7 collective-permute-start.7
  90.0 0.7 collective-permute-start.8
  90.7 0.7 collective-permute-start.9
  91.4 2.2 %local.1.local_ref = f32[1024,128]{1,0:T(8,128)S(1)} custom-call(bf16[8,4,256,256]{3,2,1,0:T(8,128)(2,1)S(1)} %get-tuple-element.65.stacked, f32[1024,512]{1,0:T(8,128)S(1)} %get-tuple-element.66.c_re, f32[1024,512]{1,0:T(8,128)S(1)} %get-tuple-element.67.c_im, bf16[4,2,128,256]{3,2,1,0:T(8,128)(2,1)S(1)} %get-tuple-element.68.read_ref, ...), custom_call_target="tpu_custom_call" | custom-call | flops 786432000 | bytes 8388608 | tf_op jit(solution)/shard_map/local/pallas_call | solution.py:316
  93.6 0.6 link.13
  94.2 2.0 %answers.1 = bf16[1024,128]{1,0:T(8,128)(2,1)S(1)} custom-call(f32[16,128]{1,0:T(8,128)S(1)} %get-tuple-element.49.near_ref, f32[8,128]{1,0:T(8,128)S(1)} %get-tuple-element.64.far_ref, f32[1024,128]{1,0:T(8,128)S(1)} %local.1.local_ref, f32[1024,512]{1,0:T(8,128)S(1)} %get-tuple-element.66.c_re, f32[1024,512]{1,0:T(8,128)S(1)} %get-tuple-element.67.c_im, ...), custom_call_target="tpu_custom_call" | custom-call | flops 524288000 | bytes 8388608 | tf_op jit(solution)/shard_map/answers/pallas_call | solution.py:406
  96.3 7.9 %all_to_all.17 = bf16[4,256,128]{2,1,0:T(8,128)(2,1)S(1)} all-to-all(bf16[4,256,128]{2,1,0:T(8,128)(2,1)S(1)} %bitcast.15), channel_id=1, replica_groups=mesh['grp'=2,'zh'=8,'zl'=4,'core'=2,'tp'=4] {'tp'}, dimensions={0} | all-to-all | bytes 524288 | tf_op jit(solution)/shard_map/all_to_all | solution.py:442
  104.2 0.1 fusion.1
  104.4 1.7 %fusion = bf16[256,2048]{1,0:T(8,128)(2,1)} fusion(bf16[4,128,2048]{2,1,0:T(8,128)(2,1)S(1)} %bitcast.14, bf16[4,256,128]{2,1,0:T(8,128)(2,1)S(1)} %all_to_all.17, f32[4,128]{1,0:T(4,128)S(1)} %bitcast.20, f32[256]{0:T(256)S(1)} %add_rsqrt_fusion), kind=kOutput, calls=%fused_computation.1 | convolution fusion | flops 537919488 | bytes 3410944 | tf_op jit(solution)/shard_map/ktc,kcd->td/dot_general | solution.py:446
  (22 shorter events, 0.2 us)
Async XLA Ops:
  0.0 104.4 %copy-start = (bf16[512,2048]{1,0:T(8,128)(2,1)S(1)}, bf16[512,2048]{1,0:T(8,128)(2,1)}, u32[]{:S(2)}) copy-start(bf16[512,2048]{1,0:T(8,128)(2,1)} %param.19) | copy-start | bytes 6291460
  0.0 22.3 %collective-permute-start = (bf16[2048,128]{1,0:T(8,128)(2,1)}, bf16[2048,128]{1,0:T(8,128)(2,1)S(1)}, u32[]{:S(2)}, u32[]{:S(2)}) collective-permute-start(bf16[2048,128]{1,0:T(8,128)(2,1)} %refs_0_.1), channel_id=1, source_target_pairs={{0,1},{1,2},{2,3},{3,0},{4,5},{5,6},{6,7},{7,4},{8,9},{9,10},{10,1... | collective-permute-start | bytes 1572872 | tf_op jit(solution)/shard_map/ppermute | solution.py:424
  4.2 20.7 %collective-permute-start.1 = (bf16[2048,128]{1,0:T(8,128)(2,1)}, bf16[2048,128]{1,0:T(8,128)(2,1)S(1)}, u32[]{:S(2)}, u32[]{:S(2)}) collective-permute-start(bf16[2048,128]{1,0:T(8,128)(2,1)} %refs_0_.1), channel_id=1, source_target_pairs={{0,2},{1,3},{2,0},{3,1},{4,6},{5,7},{6,4},{7,5},{8,10},{9,11},{10,... | collective-permute-start | bytes 1572872 | tf_op jit(solution)/shard_map/ppermute | solution.py:424
  8.9 16.0 %collective-permute-start.2 = (bf16[2048,128]{1,0:T(8,128)(2,1)}, bf16[2048,128]{1,0:T(8,128)(2,1)}, u32[]{:S(2)}, u32[]{:S(2)}) collective-permute-start(bf16[2048,128]{1,0:T(8,128)(2,1)} %refs_0_.1), channel_id=1, source_target_pairs={{0,3},{1,0},{2,1},{3,2},{4,7},{5,4},{6,5},{7,6},{8,11},{9,8},{10,9... | collective-permute-start | bytes 1572872 | tf_op jit(solution)/shard_map/ppermute | solution.py:424
  25.0 1.0 copy-start.1
  85.2 2.0 %collective-permute-start.3 = (f32[8,128]{1,0:T(8,128)S(1)}, f32[8,128]{1,0:T(8,128)S(1)}, u32[]{:S(2)}, u32[]{:S(2)}) collective-permute-start(f32[8,128]{1,0:T(8,128)S(1)} %get-tuple-element.50.end_ref), channel_id=1, source_target_pairs={{0,32},{1,33},{2,34},{3,35},{4,36},{5,37},{6,38},{7,39},{8,40},{9,... | collective-permute-start | bytes 12296 | tf_op jit(solution)/shard_map/ppermute | solution.py:439
  87.2 0.7 collective-permute-start.4
  87.9 0.7 collective-permute-start.5
  88.6 0.7 collective-permute-start.6
  89.3 0.7 collective-permute-start.7
  90.0 0.7 collective-permute-start.8
  90.7 2.9 %collective-permute-start.9 = (f32[8,128]{1,0:T(8,128)S(1)}, f32[8,128]{1,0:T(8,128)S(1)}, u32[]{:S(2)}, u32[]{:S(2)}) collective-permute-start(f32[8,128]{1,0:T(8,128)S(1)} %get-tuple-element.63), channel_id=1, source_target_pairs={{192,224},{193,225},{194,226},{195,227},{196,228},{197,229},{198,2... | collective-permute-start | bytes 12296 | tf_op jit(solution)/shard_map/ppermute | solution.py:439
  94.2 10.1 %copy-start.2 = (f32[512]{0:T(512)S(1)}, f32[512]{0:T(512)}, u32[]{:S(2)}) copy-start(f32[512]{0:T(512)} %param.18) | copy-start | bytes 6148

commit v5 on v4

--- a/solution.py
+++ b/solution.py
@@ -95,8 +95,8 @@
     return jnp.dot(kept, cols, preferred_element_type=F32)
 
 
-def tables_kernel(tokens_ref, gain_ref, step_ref, rate_ref, freq_ref, map_ref, readout_ref,
-                  normed_ref, w_re, w_im, c_re, c_im,
+def tables_kernel(tokens_ref, proj_ref, gain_ref, step_ref, rate_ref, freq_ref, map_ref, readout_ref,
+                  normed_ref, kept_ref, w_re, w_im, c_re, c_im,
                   end_re, end_im, push_ref, read_ref, modes_ref, times_ref, ready):
     chunk = pl.program_id(0)
     blocks = modes_ref.shape[0] // 2
@@ -133,6 +133,9 @@
     mean = jnp.mean(tokens * tokens, axis=1, keepdims=True)
     share = tokens.shape[0]
     normed_ref[pl.ds(pl.multiple_of(chunk * share, share), share), :] = (tokens * lax.rsqrt(mean + 1e-06) * gain_ref[...]).astype(BF16)
+
+    deep = proj_ref.shape[0]
+    kept_ref[pl.ds(pl.multiple_of(chunk * deep, deep), deep), :] = proj_ref[...]
 
     lower = iota((CHUNK, CHUNK), 1) <= iota((CHUNK, CHUNK), 0)
     ones = jnp.ones((2 * CHUNK, LANES), BF16)
@@ -183,23 +186,24 @@
     ready[(chunk + 1) % 2, 0], ready[(chunk + 1) % 2, 1] = following
 
 
-def tables(tokens, gain, step, rate, freq, input_map, readout):
+def tables(tokens, proj, gain, step, rate, freq, input_map, readout):
     width = rate.size
     blocks = width // LANES
     chunks = step.shape[0]
     rows = chunks * CHUNK
     part = pl.BlockSpec((tokens.shape[0] // chunks, tokens.shape[1]), lambda c: (c, 0))
-    out = [pltpu.VMEM(tokens.shape, BF16)] + [pltpu.VMEM((rows, width), F32)] * 4
+    slab = pl.BlockSpec((proj.shape[0] // chunks, proj.shape[1]), lambda c: (c, 0))
+    out = [pltpu.VMEM(tokens.shape, BF16), pltpu.VMEM(proj.shape, BF16)] + [pltpu.VMEM((rows, width), F32)] * 4
     out += [pltpu.VMEM((8 * chunks, width), F32)] * 2
     out += [pltpu.VMEM((blocks, 2, 2 * LANES, LANES), BF16), pltpu.VMEM((blocks, 2, LANES, 2 * LANES), BF16)]
     out += [pltpu.VMEM((2 * blocks, LANES), F32), pltpu.VMEM((8, LANES), F32)]
     return pl.pallas_call(
         tables_kernel, grid=(chunks,),
-        in_specs=[part, whole(gain)] + [whole(x) for x in (step, rate, freq, input_map, readout)],
+        in_specs=[part, slab, whole(gain)] + [whole(x) for x in (step, rate, freq, input_map, readout)],
         out_specs=[ONCHIP] * len(out), out_shape=out, name="tables", compiler_params=settings(),
         scratch_shapes=[pltpu.VMEM((2, 2, CHUNK, LANES), F32)],
         cost_estimate=pl.CostEstimate(flops=rows * width * 60, transcendentals=0, bytes_accessed=rows * width * 16),
-    )(*(pltpu.with_memory_space_constraint(x, pltpu.HBM) for x in (tokens, gain, step, rate, freq, input_map, readout)))
+    )(*(pltpu.with_memory_space_constraint(x, pltpu.HBM) for x in (tokens, proj, gain, step, rate, freq, input_map, readout)))
 
 
 def project_kernel(at_ref, rows_ref, *refs):
@@ -279,45 +283,9 @@
     return jnp.concatenate([read_ref[b, 0], read_ref[b, 1]], axis=0)
 
 
-def local_kernel(stacked, c_re, c_im, read_ref, _, out_ref, high, low):
-    blocks = read_ref.shape[0]
-    lower = triangle(2)
-    carry = [jnp.zeros((1, LANES), F32)] * (2 * blocks)
-    for tile in range(c_re.shape[0] // TILE):
-        value = jnp.zeros((TILE, LANES), F32)
-        for b in range(blocks):
-            cols = slice(b * LANES, (b + 1) * LANES)
-            er, ei = carry[2 * b:2 * b + 2]
-            for j in range(TILE // CHUNK):
-                k = tile * (TILE // CHUNK) + j
-                rows = slice(k * CHUNK, (k + 1) * CHUNK)
-                here = slice(j * CHUNK, (j + 1) * CHUNK)
-                acc = jnp.dot(lower, stacked[k, b], preferred_element_type=F32)
-                tr, ti = acc[:, :LANES] + er, acc[:, LANES:] + ei
-                cr, ci = c_re[rows, cols], c_im[rows, cols]
-                sr = cr * tr - ci * ti
-                si = cr * ti + ci * tr
-                er, ei = sr[CHUNK - 1:], si[CHUNK - 1:]
-                high[b, here, :LANES], low[b, here, :LANES] = high_low(sr)
-                high[b, here, LANES:], low[b, here, LANES:] = high_low(si)
-            carry[2 * b], carry[2 * b + 1] = er, ei
-        for b in range(blocks):
-            value = value + read_states(high[b], low[b], read_of(read_ref, b))
-        out_ref[tile * TILE:(tile + 1) * TILE, :] = value
-
-
 def scratches(blocks):
     store = pltpu.VMEM((blocks, TILE, 2 * LANES), BF16)
     return [store, store]
-
-
-def local(stacked, c_re, c_im, read, after):
-    rows, width = c_re.shape
-    return pl.pallas_call(
-        local_kernel, in_specs=[ONCHIP] * 5, out_specs=ONCHIP, scratch_shapes=scratches(width // LANES),
-        out_shape=pltpu.VMEM((rows, LANES), F32), name="local", compiler_params=settings(),
-        cost_estimate=pl.CostEstimate(flops=rows * width * 1500, transcendentals=0, bytes_accessed=rows * width * 16),
-    )(*(onchip(x) for x in (stacked, c_re, c_im, read, after)))
 
 
 def compose_kernel(at_ref, heard_ref, modes_ref, out_ref, end_ref, decay_ref):
@@ -369,14 +337,16 @@
     )(*(onchip(x) for x in (far, comes, end, decay)))
 
 
-def answer_kernel(near_ref, far_ref, local_ref, c_re, c_im, d_re, d_im, read_ref, out_ref, high, low):
+def answer_kernel(near_ref, far_ref, comes_ref, stacked, c_re, c_im, read_ref, out_ref, high, low):
     blocks = read_ref.shape[0]
     er, ei = near_ref[:blocks], near_ref[blocks:2 * blocks]
     dr, di = near_ref[2 * blocks:3 * blocks], near_ref[3 * blocks:4 * blocks]
-    fr, fi = far_ref[:blocks], far_ref[blocks:]
+    far = far_ref[...] + comes_ref[...]
+    fr, fi = far[:blocks], far[blocks:]
     start_re = dr * fr - di * fi + er
     start_im = dr * fi + di * fr + ei
     carry = [x[b:b + 1] for b in range(blocks) for x in (start_re, start_im)]
+    lower = triangle(2)
     for tile in range(c_re.shape[0] // TILE):
         for b in range(blocks):
             cols = slice(b * LANES, (b + 1) * LANES)
@@ -385,29 +355,29 @@
                 k = tile * (TILE // CHUNK) + j
                 rows = slice(k * CHUNK, (k + 1) * CHUNK)
                 here = slice(j * CHUNK, (j + 1) * CHUNK)
+                acc = jnp.dot(lower, stacked[k, b], preferred_element_type=F32)
+                tr, ti = acc[:, :LANES] + er, acc[:, LANES:] + ei
                 cr, ci = c_re[rows, cols], c_im[rows, cols]
-                sr = cr * er - ci * ei
-                si = cr * ei + ci * er
+                sr = cr * tr - ci * ti
+                si = cr * ti + ci * tr
+                er, ei = sr[CHUNK - 1:], si[CHUNK - 1:]
                 high[b, here, :LANES], low[b, here, :LANES] = high_low(sr)
                 high[b, here, LANES:], low[b, here, LANES:] = high_low(si)
-                last = 8 * k + 7
-                cr, ci = d_re[last:last + 1, cols], d_im[last:last + 1, cols]
-                er, ei = cr * er - ci * ei, cr * ei + ci * er
             carry[2 * b], carry[2 * b + 1] = er, ei
-        value = local_ref[tile * TILE:(tile + 1) * TILE, :]
+        value = jnp.zeros((TILE, LANES), F32)
         for b in range(blocks):
             value = value + read_states(high[b], low[b], read_of(read_ref, b))
         inner = 0.7978845608 * (value + 0.044715 * (value * value * value))
         out_ref[tile * TILE:(tile + 1) * TILE, :] = (0.5 * value * (1.0 + jnp.tanh(inner))).astype(BF16)
 
 
-def answers(near, far, own, c_re, c_im, d_re, d_im, read):
+def answers(near, far, comes, stacked, c_re, c_im, read):
     rows, width = c_re.shape
     return pl.pallas_call(
-        answer_kernel, in_specs=[ONCHIP] * 8, out_specs=ONCHIP, scratch_shapes=scratches(width // LANES),
+        answer_kernel, in_specs=[ONCHIP] * 7, out_specs=ONCHIP, scratch_shapes=scratches(width // LANES),
         out_shape=pltpu.VMEM((rows, LANES), BF16), name="answers", compiler_params=settings(),
-        cost_estimate=pl.CostEstimate(flops=rows * width * 1000, transcendentals=0, bytes_accessed=rows * width * 16),
-    )(*(onchip(x) for x in (near, far, own, c_re, c_im, d_re, d_im, read)))
+        cost_estimate=pl.CostEstimate(flops=rows * width * 1500, transcendentals=0, bytes_accessed=rows * width * 16),
+    )(*(onchip(x) for x in (near, far, comes, stacked, c_re, c_im, read)))
 
 
 def ring(count, by):
@@ -421,24 +391,25 @@
     way = lax.axis_index("tp").astype(jnp.int32).reshape(1)
     place = lax.axis_index(("zl", "core")).astype(jnp.int32).reshape(1)
     step, way, place = lax.optimization_barrier((step, way, place))
-    projs = [in_proj] + [lax.ppermute(in_proj, "tp", ring(ways, by)) for by in range(1, ways)]
-    normed, w_re, w_im, c_re, c_im, d_re, d_im, push, read, modes, times = tables(
-        tokens, in_gain.reshape(1, -1), step.reshape(-1, CHUNK), decay_rate, frequency,
+    projs = [lax.ppermute(in_proj, "tp", ring(ways, by)) for by in range(1, ways)]
+    normed, kept, w_re, w_im, c_re, c_im, d_re, d_im, push, read, modes, times = tables(
+        tokens, in_proj, in_gain.reshape(1, -1), step.reshape(-1, CHUNK), decay_rate, frequency,
         jnp.swapaxes(input_map, 2, 3), readout,
     )
-    drive = lax.all_to_all(project(way, normed, projs), "tp", 0, 0, tiled=True)
+    drive = lax.all_to_all(project(way, normed, [kept, *projs]), "tp", 0, 0, tiled=True)
     peers = lax.axis_size("zl") * lax.axis_size("core")
     stacked, sent = ends(
         drive.reshape(-1, drive.shape[-1]), w_re, w_im, d_re, d_im, push, times, peers
     )
     heard = lax.all_to_all(sent, ("zl", "core"), 0, 0, tiled=True)
-    own = local(stacked, c_re, c_im, read, heard)
     near, end, decay = compose(place, heard, modes)
-    far, leaves = jnp.zeros_like(end), end
-    for k in range(lax.axis_size("zh") - 1):
+    far, comes, leaves = jnp.zeros_like(end), jnp.zeros_like(end), end
+    steps = lax.axis_size("zh") - 1
+    for k in range(steps):
         comes = lax.ppermute(leaves, "zh", [(k, k + 1)])
-        far, leaves = link(far, comes, end, decay)
-    answer = answers(near, far, own, c_re, c_im, d_re, d_im, read)
+        if k < steps - 1:
+            far, leaves = link(far, comes, end, decay)
+    answer = answers(near, far, comes, stacked, c_re, c_im, read)
     parts = lax.all_to_all(answer.reshape(ways, -1, LANES), "tp", 0, 0, tiled=True)
     values = parts.astype(F32)
     mean = jnp.sum(values * values, axis=(0, 2), keepdims=True) * (1.0 / (ways * LANES))

time: 107 us -> 103 us (0.963)
  Pallas kernels: 18.8 us -> 16.3 us
    pallas_call x3 -> x2, Pallas kernels: 14.7 us -> 12.7 us  [the longest x1 10.5 us: tables(): pl.pallas_call(tables_kernel, grid=(chunks,), in_specs=[part, slab, whole...]
  transfers between devices with their start and end apart: 10 -> 10, of which waited for: 2 -> 2; matrix products, arithmetic and copies ran while one was open for 0% -> 0% of each run, Pallas kernels for 12% -> 10%
where the time goes in v5:
time: 103 us; the launch traced here: 102 us
  blocking collectives  63.6 us (62%)
  starting transfers between devices  17.1 us (17%)
  Pallas kernels  16.3 us (16%)
  waiting for transfers between devices  3.33 us (3%)
  matrix products  1.74 us (2%)
    all_to_all x1, blocking collectives, on_device(): heard = lax.all_to_all(sent, ('zl', 'core'), 0, 0, tiled=True)  47.7 us
    ppermute x3, starting transfers between devices, on_device(): lax.ppermute(in_proj, 'tp', ring(ways, by))  11.8 us
    pallas_call x1, Pallas kernels, tables(): pl.pallas_call(tables_kernel, grid=(chunks,), in_specs=[part, slab, whole...  10.5 us
    all_to_all x1, blocking collectives, on_device(): lax.all_to_all(answer.reshape(ways, -1, LANES), 'tp', 0, 0, tiled=True)  7.95 us
    all_to_all x1, blocking collectives, on_device(): lax.all_to_all(project(way, normed, [kept, *projs]), 'tp', 0, 0, tiled=True)  7.95 us
    ppermute x7, starting transfers between devices, on_device(): comes = lax.ppermute(leaves, 'zh', [(k, k + 1)])  5.27 us
    ppermute x3, waiting for transfers between devices, on_device(): lax.ppermute(in_proj, 'tp', ring(ways, by))  2.58 us
    pallas_call x1, Pallas kernels, answers(): pl.pallas_call(answer_kernel, in_specs=[ONCHIP] * 7, out_specs=ONCHIP, sc...  2.25 us
  transfers between devices with their start and end apart: 10, of which 2 were waited for; matrix products, arithmetic and copies ran while one was open for 0% of the time, Pallas kernels for 10%

profile of v5, /device:TPU:33, one launch (start us, length us, event | category | flops | bytes accessed | tf_op | source)
XLA Modules:
  0.0 102.4 jit_solution(8319358616288407029)
XLA Ops:
  0.0 4.2 %collective-permute-start = (bf16[2048,128]{1,0:T(8,128)(2,1)}, bf16[2048,128]{1,0:T(8,128)(2,1)S(1)}, u32[]{:S(2)}, u32[]{:S(2)}) collective-permute-start(bf16[2048,128]{1,0:T(8,128)(2,1)} %proj_ref.1), channel_id=1, source_target_pairs={{0,1},{1,2},{2,3},{3,0},{4,5},{5,6},{6,7},{7,4},{8,9},{9,10},{10,1... | collective-permute-start | bytes 1572872 | tf_op jit(solution)/shard_map/ppermute | solution.py:394
  4.2 4.7 %collective-permute-start.1 = (bf16[2048,128]{1,0:T(8,128)(2,1)}, bf16[2048,128]{1,0:T(8,128)(2,1)S(1)}, u32[]{:S(2)}, u32[]{:S(2)}) collective-permute-start(bf16[2048,128]{1,0:T(8,128)(2,1)} %proj_ref.1), channel_id=1, source_target_pairs={{0,2},{1,3},{2,0},{3,1},{4,6},{5,7},{6,4},{7,5},{8,10},{9,11},{10,... | collective-permute-start | bytes 1572872 | tf_op jit(solution)/shard_map/ppermute | solution.py:394
  8.9 3.0 %collective-permute-start.2 = (bf16[2048,128]{1,0:T(8,128)(2,1)}, bf16[2048,128]{1,0:T(8,128)(2,1)}, u32[]{:S(2)}, u32[]{:S(2)}) collective-permute-start(bf16[2048,128]{1,0:T(8,128)(2,1)} %proj_ref.1), channel_id=1, source_target_pairs={{0,3},{1,0},{2,1},{3,2},{4,7},{5,4},{6,5},{7,6},{8,11},{9,8},{10,9... | collective-permute-start | bytes 1572872 | tf_op jit(solution)/shard_map/ppermute | solution.py:394
  11.9 10.5 %tables.1 = (bf16[256,2048]{1,0:T(8,128)(2,1)S(1)}, bf16[2048,128]{1,0:T(8,128)(2,1)S(1)}, f32[1024,512]{1,0:T(8,128)S(1)}, f32[1024,512]{1,0:T(8,128)S(1)}, f32...) custom-call(bf16[256,2048]{1,0:T(8,128)(2,1)} %tokens_ref.1, ...), custom_call_target="tpu_custom_call" | custom-call | flops 31457280 | bytes 8388608 | tf_op jit(solution)/shard_map/tables/pallas_call | solution.py:200
  22.4 2.6 %collective-permute-done.1.refs_2_ = bf16[2048,128]{1,0:T(8,128)(2,1)S(1)} collective-permute-done((bf16[2048,128]{1,0:T(8,128)(2,1)}, bf16[2048,128]{1,0:T(8,128)(2,1)S(1)}, u32[]{:S(2)}, u32[]{:S(2)}) %collective-permute-start.1) | collective-permute-done | bytes 524320 | tf_op jit(solution)/shard_map/ppermute | solution.py:394
  24.9 0.0 collective-permute-done.2.refs_3_
  24.9 1.8 %project.1 = bf16[4,256,128]{2,1,0:T(8,128)(2,1)S(1)} custom-call(s32[1]{0:T(128)} %bitcast.at_ref, bf16[256,2048]{1,0:T(8,128)(2,1)S(1)} %get-tuple-element.40.rows_ref, bf16[2048,128]{1,0:T(8,128)(2,1)S(1)} %get-tuple-element.41.refs_0_, bf16[2048,128]{1,0:T(8,128)(2,1)S(1)} %collective-permute-done.refs_1_, ...), custom_call_target="tpu_custom_call" | custom-call | flops 536870912 | bytes 2097152 | tf_op jit(solution)/shard_map/project/pallas_call | solution.py:223
  26.7 7.9 %all_to_all.15 = bf16[4,256,128]{2,1,0:T(8,128)(2,1)S(1)} all-to-all(bf16[4,256,128]{2,1,0:T(8,128)(2,1)S(1)} %project.1), channel_id=1, replica_groups=mesh['grp'=2,'zh'=8,'zl'=4,'core'=2,'tp'=4] {'tp'}, dimensions={0} | all-to-all | bytes 524288 | tf_op jit(solution)/shard_map/all_to_all | solution.py:399
  34.7 1.6 %ends.1 = (bf16[8,4,256,256]{3,2,1,0:T(8,128)(2,1)S(1)}, f32[8,16,128]{2,1,0:T(8,128)S(1)}) custom-call(bf16[1024,128]{1,0:T(8,128)(2,1)S(1)} %bitcast.15, f32[1024,512]{1,0:T(8,128)S(1)} %get-tuple-element.42.w_re, f32[1024,512]{1,0:T(8,128)S(1)} %get-tuple-element.43.w_im, f32[64,512]{1,0:T(8,128)S(1)} %get-tuple-element.44.d_re, ...), custom_call_target="tpu_custom_call" | custom-call | flops 262144000 | bytes 8388608 | tf_op jit(solution)/shard_map/ends/pallas_call | solution.py:269
  36.3 47.7 %all_to_all.16.heard_ref = f32[8,16,128]{2,1,0:T(8,128)S(1)} all-to-all(f32[8,16,128]{2,1,0:T(8,128)S(1)} %get-tuple-element.48), channel_id=1, replica_groups=mesh['grp'=2,'zh'=8,'zl'=4,'core'=2,'tp'=4] {'zl','core'}, dimensions={0} | all-to-all | bytes 131072 | tf_op jit(solution)/shard_map/all_to_all | solution.py:404
  84.0 0.1 compose.1
  84.0 1.3 %collective-permute-start.3 = (f32[8,128]{1,0:T(8,128)S(1)}, f32[8,128]{1,0:T(8,128)S(1)}, u32[]{:S(2)}, u32[]{:S(2)}) collective-permute-start(f32[8,128]{1,0:T(8,128)S(1)} %get-tuple-element.51.end_ref), channel_id=1, source_target_pairs={{0,32},{1,33},{2,34},{3,35},{4,36},{5,37},{6,38},{7,39},{8,40},{9,... | collective-permute-start | bytes 12296 | tf_op jit(solution)/shard_map/ppermute | solution.py:409
  85.4 0.7 collective-permute-done.3.comes_ref
  86.1 0.7 collective-permute-start.4
  86.8 0.7 collective-permute-start.5
  87.5 0.7 collective-permute-start.6
  88.2 0.7 collective-permute-start.7
  88.9 0.7 collective-permute-start.8
  89.6 0.7 collective-permute-start.9
  90.3 0.0 copy-start.1
  90.3 2.2 %answers.1 = bf16[1024,128]{1,0:T(8,128)(2,1)S(1)} custom-call(f32[16,128]{1,0:T(8,128)S(1)} %get-tuple-element.50.near_ref, f32[8,128]{1,0:T(8,128)S(1)} %get-tuple-element.63.far_ref, f32[8,128]{1,0:T(8,128)S(1)} %collective-permute-done.9.comes_ref, bf16[8,4,256,256]{3,2,1,0:T(8,128)(2,1)S(1)} %get-tuple-element.65.stacked, ...), custom_call_target="tpu_custom_call" | custom-call | flops 786432000 | bytes 8388608 | tf_op jit(solution)/shard_map/answers/pallas_call | solution.py:376
  92.5 7.9 %all_to_all.17 = bf16[4,256,128]{2,1,0:T(8,128)(2,1)S(1)} all-to-all(bf16[4,256,128]{2,1,0:T(8,128)(2,1)S(1)} %bitcast.16), channel_id=1, replica_groups=mesh['grp'=2,'zh'=8,'zl'=4,'core'=2,'tp'=4] {'tp'}, dimensions={0} | all-to-all | bytes 524288 | tf_op jit(solution)/shard_map/all_to_all | solution.py:413
  100.5 0.1 fusion.1
  100.6 1.7 %fusion = bf16[256,2048]{1,0:T(8,128)(2,1)} fusion(bf16[4,128,2048]{2,1,0:T(8,128)(2,1)S(1)} %bitcast.14, bf16[4,256,128]{2,1,0:T(8,128)(2,1)S(1)} %all_to_all.17, f32[4,128]{1,0:T(4,128)S(1)} %bitcast.20, f32[256]{0:T(256)S(1)} %add_rsqrt_fusion), kind=kOutput, calls=%fused_computation.1 | convolution fusion | flops 537919488 | bytes 3410944 | tf_op jit(solution)/shard_map/ktc,kcd->td/dot_general | solution.py:417
  (18 shorter events, 0.1 us)
Async XLA Ops:
  0.0 100.6 %copy-start = (bf16[512,2048]{1,0:T(8,128)(2,1)S(1)}, bf16[512,2048]{1,0:T(8,128)(2,1)}, u32[]{:S(2)}) copy-start(bf16[512,2048]{1,0:T(8,128)(2,1)} %param.19) | copy-start | bytes 6291460
  0.0 22.4 %collective-permute-start = (bf16[2048,128]{1,0:T(8,128)(2,1)}, bf16[2048,128]{1,0:T(8,128)(2,1)S(1)}, u32[]{:S(2)}, u32[]{:S(2)}) collective-permute-start(bf16[2048,128]{1,0:T(8,128)(2,1)} %proj_ref.1), channel_id=1, source_target_pairs={{0,1},{1,2},{2,3},{3,0},{4,5},{5,6},{6,7},{7,4},{8,9},{9,10},{10,1... | collective-permute-start | bytes 1572872 | tf_op jit(solution)/shard_map/ppermute | solution.py:394
  4.2 20.7 %collective-permute-start.1 = (bf16[2048,128]{1,0:T(8,128)(2,1)}, bf16[2048,128]{1,0:T(8,128)(2,1)S(1)}, u32[]{:S(2)}, u32[]{:S(2)}) collective-permute-start(bf16[2048,128]{1,0:T(8,128)(2,1)} %proj_ref.1), channel_id=1, source_target_pairs={{0,2},{1,3},{2,0},{3,1},{4,6},{5,7},{6,4},{7,5},{8,10},{9,11},{10,... | collective-permute-start | bytes 1572872 | tf_op jit(solution)/shard_map/ppermute | solution.py:394
  8.9 16.0 %collective-permute-start.2 = (bf16[2048,128]{1,0:T(8,128)(2,1)}, bf16[2048,128]{1,0:T(8,128)(2,1)}, u32[]{:S(2)}, u32[]{:S(2)}) collective-permute-start(bf16[2048,128]{1,0:T(8,128)(2,1)} %proj_ref.1), channel_id=1, source_target_pairs={{0,3},{1,0},{2,1},{3,2},{4,7},{5,4},{6,5},{7,6},{8,11},{9,8},{10,9... | collective-permute-start | bytes 1572872 | tf_op jit(solution)/shard_map/ppermute | solution.py:394
  84.0 2.0 %collective-permute-start.3 = (f32[8,128]{1,0:T(8,128)S(1)}, f32[8,128]{1,0:T(8,128)S(1)}, u32[]{:S(2)}, u32[]{:S(2)}) collective-permute-start(f32[8,128]{1,0:T(8,128)S(1)} %get-tuple-element.51.end_ref), channel_id=1, source_target_pairs={{0,32},{1,33},{2,34},{3,35},{4,36},{5,37},{6,38},{7,39},{8,40},{9,... | collective-permute-start | bytes 12296 | tf_op jit(solution)/shard_map/ppermute | solution.py:409
  86.1 0.7 collective-permute-start.4
  86.8 0.7 collective-permute-start.5
  87.5 0.7 collective-permute-start.6
  88.2 0.7 collective-permute-start.7
  88.9 0.7 collective-permute-start.8
  89.6 0.7 collective-permute-start.9
  90.3 10.4 %copy-start.1 = (f32[512]{0:T(512)S(1)}, f32[512]{0:T(512)}, u32[]{:S(2)}) copy-start(f32[512]{0:T(512)} %param.18) | copy-start | bytes 6148
